TPU v7x, 256 devices: a whole 4x4x8 slice. The times are simulated.
256 devices in a mesh: ep: 16 (over y, x), tp: 16 (over z, core).
Axes of the slice: x: 4, y: 4, z: 8, core: 2. Of those that a mesh axis runs over, the one named last changes fastest.
Arguments:
- scan_source_values: bfloat16 [1024, 32768], P('tp', 'ep'), may hold values from -6 to 6
- switch_path_values: bfloat16 [1024, 32768], P('tp', 'ep'), may hold values from -6 to 6
- causal_filter_coefficients: bfloat16 [1024, 4], replicated, may hold values from -3 to 3
- scan_switch_blockmap: bfloat16 [16, 64, 64], replicated, may hold values from -0.75 to 0.75
- entry_switch_blockmap: bfloat16 [16, 64, 64], replicated, may hold values from -0.75 to 0.75
- feature_fading_speeds: float32 [1024], replicated, may hold values from 0 to 1
- spike_amount: float32 [32768], P('ep'), may hold values from -1 to 0
- final_linear_map: bfloat16 [1024, 2048], replicated, may hold values from -0.1875 to 0.1875
- dispatched_group_activity: bfloat16 [32768, 2048], P(('ep', 'tp')), may hold values from -6 to 6
- specialist_rmsgain: bfloat16 [2048], replicated, may hold values from 0.099609375 to 1.8984375
- selected_specialist_ids: int32 [32768, 2], P(('ep', 'tp')), may hold values from 0 to 15, all different within a row; in each aligned block of 128 rows (0 to 127, 128 to 255, ...) at most 24 rows name the same one
- selected_specialist_share: float32 [32768, 2], P(('ep', 'tp')), may hold values from 0.2 to 1
- specialist_switch_maps: bfloat16 [16, 2048, 2048], P('ep', None, 'tp'), may hold values from -0.3125 to 0.3125
- specialist_widen_maps: bfloat16 [16, 2048, 2048], P('ep', None, 'tp'), may hold values from -0.3125 to 0.3125
- specialist_shrink_maps: bfloat16 [16, 2048, 2048], P('ep', None, 'tp'), may hold values from -0.03125 to 0.03125
Outputs:
- scan_path_result: bfloat16 [32768, 2048], P(('ep', 'tp'))
- moe_out: bfloat16 [32768, 2048], P(('ep', 'tp'))
Inputs may be any that keep to these rules, and one draw needn't show every extreme that they name: `selected_specialist_ids`: each row names 2 different experts. Among the rows of one device no expert is named more than 24 times, and in every draw some device names some expert exactly 24 times.
All inputs are finite; a program needn't handle non-finite values.
Results may differ from a plain program's by a relative error of at most 0.0085.
Values may be sent and summed in bfloat16 or wider, within the bound.
No kernel may reach another device: no remote copies, remote signals or barrier semaphores. Data moves between devices by JAX's collectives and lax.ppermute only.
A program may use at most 128 MiB of HBM per device.

v0:
```python
import jax
import jax.numpy as jnp
from jax import lax
from jax.sharding import PartitionSpec as P

BLOCK = 64


def from_everyone(x, axis):
    copies = jnp.broadcast_to(x, (lax.axis_size(axis), *x.shape))
    return lax.all_to_all(copies, axis, split_axis=0, concat_axis=0, tiled=True)


def all_in_one(x, axis):
    leaves = jax.tree.leaves(x)
    sequence = sorted(range(len(leaves)), key=lambda k: -leaves[k].size)
    width = (1, *leaves[sequence[0]].shape)[-1]
    lines = [
        jnp.pad(leaves[k].reshape(-1), (0, -leaves[k].size % width)).reshape(-1, width)
        for k in sequence
    ]
    both, at, found = (from_everyone(jnp.concatenate(lines), axis), 0, {})
    for k, line in zip(sequence, lines):
        section = both[:, at : at + len(line)].reshape(len(both), -1)
        found[k] = section[:, : leaves[k].size].reshape(-1, *leaves[k].shape)
        at += len(line)
    numbers = iter(range(len(leaves)))
    return jax.tree.map(lambda _: found[next(numbers)], x)


def folded_in_pairs(pieces, combine):
    while len(jax.tree.leaves(pieces)[0]) > 1:
        pieces = jax.vmap(combine)(
            *(jax.tree.map(lambda part: part[side::2], pieces) for side in (0, 1))
        )
    return jax.tree.map(lambda part: part[0], pieces)


def prefix(x, axis, combine, identity):
    count, index = (lax.axis_size(axis), lax.axis_index(axis))
    passed = jnp.arange(count) < index

    def kept(part, zero, own):
        part = jnp.where(
            passed.reshape(-1, *(1 for _ in own.shape)), part, jnp.asarray(zero, own.dtype)
        )
        return part

    pieces = all_in_one(x, axis)
    return folded_in_pairs(jax.tree.map(kept, pieces, identity, x), combine)


def from_behind(x, axis, by):
    count = lax.axis_size(axis)
    pairs = [(i, i + by) for i in range(count) if 0 <= i + by < count]
    return lax.ppermute(x, axis, pairs)


def cut_along(x, dim, count):
    dims = x.shape
    blocks = x.reshape(*dims[:dim], count, dims[dim] // count, *dims[dim + 1 :])
    return jnp.moveaxis(blocks, dim, 0)


def cut_rows(length, count):
    hop = length // count
    if hop >= 8:
        hop -= hop % 8
    return [hop * k for k in range(1, count)]


def laid_out(blocks, dim):
    blocks = jnp.moveaxis(blocks, 0, dim)
    dims = blocks.shape
    return blocks.reshape(*dims[:dim], dims[dim] * dims[dim + 1], *dims[dim + 2 :])


def cut_exchange(x, axis, pieces, split_dim, concat_dim):
    blocks = cut_along(x, split_dim, lax.axis_size(axis))
    split_at = max(range(1, max(2, blocks.ndim - 1)), key=lambda d: blocks.shape[d])
    finished = []
    for section in jnp.split(blocks, cut_rows(blocks.shape[split_at], pieces), axis=split_at):
        if section.size:
            finished.append(lax.all_to_all(section, axis, split_axis=0, concat_axis=0, tiled=True))
    return laid_out(jnp.concatenate(finished, axis=split_at), concat_dim)


def sent_together(arrays, axis, dim, along):
    ends, at = ([], 0)
    for a in arrays[:-1]:
        at += a.shape[along]
        ends.append(at)
    both = jnp.concatenate(arrays, axis=along)
    return tuple(jnp.split(lax.all_gather(both, axis, axis=dim, tiled=True), ends, axis=along))


def combine_pairs(earlier, later):
    return (earlier[0] * later[0], later[0] * earlier[1] + later[1])


def expert_units(rows, gate_piece, up_piece):
    gate_pre = jnp.dot(rows, gate_piece, preferred_element_type=jnp.float32)
    up_pre = jnp.dot(rows, up_piece, preferred_element_type=jnp.float32)
    gate_cut = jnp.minimum(gate_pre, 7.0)
    up_cut = jnp.clip(up_pre, -7.0, 7.0)
    return ((up_cut + 1.0) * gate_cut * jax.nn.sigmoid(1.702 * gate_cut)).astype(jnp.bfloat16)


def down_product(units, down_piece):
    return lax.dot_general(
        units, down_piece, (((1,), (1,)), ((), ())), preferred_element_type=jnp.float32
    )


def segment_recurrence(decay, drive):
    channels, positions = decay.shape
    span = 16
    seg_count = positions // span
    decay_split = decay.reshape(channels, seg_count, span).transpose(0, 2, 1)
    drive_split = drive.reshape(channels, seg_count, span).transpose(0, 2, 1)
    run_state = jnp.zeros((channels, seg_count), jnp.float32)
    run_decay = jnp.ones((channels, seg_count), jnp.float32)
    state_list = []
    decay_list = []
    for offset in range(span):
        run_state = decay_split[:, offset] * run_state + drive_split[:, offset]
        run_decay = run_decay * decay_split[:, offset]
        state_list.append(run_state)
        decay_list.append(run_decay)
    local_state = jnp.stack(state_list, axis=1)
    local_decay = jnp.stack(decay_list, axis=1)
    decay_upto, state_upto = lax.associative_scan(combine_pairs, (run_decay, run_state), axis=1)
    decay_before = jnp.concatenate(
        [jnp.ones((channels, 1), jnp.float32), decay_upto[:, :-1]], axis=1
    )
    state_before = jnp.concatenate(
        [jnp.zeros((channels, 1), jnp.float32), state_upto[:, :-1]], axis=1
    )
    identity = (jnp.ones((channels,), jnp.float32), jnp.zeros((channels,), jnp.float32))
    carried = prefix((decay_upto[:, -1], state_upto[:, -1]), "ep", combine_pairs, identity)
    entering = state_before + decay_before * carried[1][:, None]
    state = local_state + local_decay * entering[:, None, :]
    return state.transpose(0, 2, 1).reshape(channels, positions)


def mixer_half(
    scan_source_values,
    switch_path_values,
    causal_filter_coefficients,
    scan_switch_blockmap,
    entry_switch_blockmap,
    feature_fading_speeds,
    spike_amount,
    final_linear_map,
):
    channels, positions = scan_source_values.shape
    tp_index = lax.axis_index("tp")
    first_chan = tp_index * channels
    conv_local = lax.dynamic_slice_in_dim(
        causal_filter_coefficients, first_chan, channels, 0
    ).astype(jnp.float32)
    tap_count = conv_local.shape[1]
    rim_cells = from_behind(scan_source_values[:, positions - tap_count + 1 :], "ep", 1)
    padded = jnp.concatenate([rim_cells, scan_source_values], axis=1).astype(jnp.float32)
    running = padded[:, 0:positions] * conv_local[:, 0:1]
    for shift_tap in range(1, tap_count):
        running = (
            running
            + padded[:, shift_tap : shift_tap + positions]
            * conv_local[:, shift_tap : shift_tap + 1]
        )
    conv_out = running.astype(jnp.bfloat16)
    block_count = channels // BLOCK
    rate_local = lax.dynamic_slice_in_dim(
        scan_switch_blockmap, tp_index * block_count, block_count, 0
    )
    input_local = lax.dynamic_slice_in_dim(
        entry_switch_blockmap, tp_index * block_count, block_count, 0
    )
    grouped = conv_out.reshape(block_count, BLOCK, positions)
    block_dims = (((1,), (1,)), ((0,), (0,)))
    scan_switch = jax.nn.sigmoid(
        lax.dot_general(
            rate_local, grouped, block_dims, preferred_element_type=jnp.float32
        ).reshape(channels, positions)
    )
    inflow = jax.nn.sigmoid(
        lax.dot_general(
            input_local, grouped, block_dims, preferred_element_type=jnp.float32
        ).reshape(channels, positions)
    )
    feature_fading = lax.dynamic_slice_in_dim(feature_fading_speeds, first_chan, channels, 0)
    fading_exponent = -8.0 * scan_switch * feature_fading[:, None] + spike_amount[None, :]
    drive = jnp.sqrt(-jnp.expm1(2.0 * fading_exponent)) * inflow * conv_out.astype(jnp.float32)
    state = segment_recurrence(jnp.exp(fading_exponent), drive)
    mix_hidden = (
        state * jax.nn.gelu(switch_path_values.astype(jnp.float32), approximate=True)
    ).astype(jnp.bfloat16)
    tp_count = lax.axis_size("tp")
    pieces = mix_hidden.reshape(channels, tp_count, positions // tp_count)
    return lax.dot_general(
        lax.all_to_all(pieces, "tp", split_axis=1, concat_axis=0, tiled=True)[:, 0, :],
        final_linear_map,
        (((0,), (0,)), ((), ())),
        preferred_element_type=jnp.float32,
    ).astype(jnp.bfloat16)


def expert_half(
    dispatched_group_activity,
    specialist_rmsgain,
    selected_specialist_ids,
    selected_specialist_share,
    specialist_switch_maps,
    specialist_widen_maps,
    specialist_shrink_maps,
):
    token_count, model_width = dispatched_group_activity.shape
    route_count = selected_specialist_ids.shape[1]
    expert_count = lax.axis_size("ep")
    slot_count = 3 * route_count * token_count // (2 * expert_count)
    values = dispatched_group_activity.astype(jnp.float32)
    scale = lax.rsqrt(jnp.mean(values * values, axis=1, keepdims=True) + 1e-06)
    normed = (values * scale * specialist_rmsgain.astype(jnp.float32)).astype(jnp.bfloat16)
    flat_ids = selected_specialist_ids.reshape(-1)
    one_hot = (flat_ids[:, None] == jnp.arange(expert_count, dtype=jnp.int32)[None, :]).astype(
        jnp.int32
    )
    slot_rank = jnp.sum((jnp.cumsum(one_hot, axis=0) - one_hot) * one_hot, axis=1)
    slot_place = flat_ids * slot_count + slot_rank
    owner_token = jnp.arange(token_count * route_count, dtype=jnp.int32) // route_count
    slot_token = (
        jnp.full((expert_count * slot_count,), token_count, jnp.int32)
        .at[slot_place]
        .set(owner_token)
    )
    padded_rows = jnp.concatenate([normed, jnp.zeros((1, model_width), jnp.bfloat16)], axis=0)
    outgoing = padded_rows[slot_token].reshape(expert_count, slot_count, model_width)
    arrived = cut_exchange(outgoing, "ep", 2, 0, 0).reshape(expert_count * slot_count, model_width)
    gate_shard = specialist_switch_maps[0]
    up_shard = specialist_widen_maps[0]
    down_shard = specialist_shrink_maps[0]
    gate_full, up_full, down_full = sent_together((gate_shard, up_shard, down_shard), "tp", 1, 0)
    result = down_product(expert_units(arrived, gate_full, up_full), down_full)
    outbound = result.astype(jnp.bfloat16).reshape(expert_count, slot_count, model_width)
    returned = lax.all_to_all(outbound, "ep", split_axis=0, concat_axis=0, tiled=True).reshape(
        expert_count * slot_count, model_width
    )
    chosen = returned[slot_place].reshape(token_count, route_count, model_width).astype(jnp.float32)
    return jnp.sum(chosen * selected_specialist_share[:, :, None], axis=1).astype(jnp.bfloat16)


def on_device(
    scan_source_values,
    switch_path_values,
    causal_filter_coefficients,
    scan_switch_blockmap,
    entry_switch_blockmap,
    feature_fading_speeds,
    spike_amount,
    final_linear_map,
    dispatched_group_activity,
    specialist_rmsgain,
    selected_specialist_ids,
    selected_specialist_share,
    specialist_switch_maps,
    specialist_widen_maps,
    specialist_shrink_maps,
):
    scan_path_result = mixer_half(
        scan_source_values,
        switch_path_values,
        causal_filter_coefficients,
        scan_switch_blockmap,
        entry_switch_blockmap,
        feature_fading_speeds,
        spike_amount,
        final_linear_map,
    )
    moe_out = expert_half(
        dispatched_group_activity,
        specialist_rmsgain,
        selected_specialist_ids,
        selected_specialist_share,
        specialist_switch_maps,
        specialist_widen_maps,
        specialist_shrink_maps,
    )
    return (scan_path_result, moe_out)


def solution(mesh):
    in_specs = (
        P("tp", "ep"),
        P("tp", "ep"),
        P(),
        P(),
        P(),
        P(),
        P("ep"),
        P(),
        P(("ep", "tp"), None),
        P(),
        P(("ep", "tp"), None),
        P(("ep", "tp"), None),
        P("ep", None, "tp"),
        P("ep", None, "tp"),
        P("ep", None, "tp"),
    )
    out_specs = (P(("ep", "tp"), None), P(("ep", "tp"), None))
    return jax.shard_map(
        on_device, mesh=mesh, in_specs=in_specs, out_specs=out_specs, check_vma=False
    )
```

profile of v0, /device:TPU:1, one launch (start us, length us, event | category | flops | bytes accessed | tf_op | source)
XLA Modules:
  0.0 230.1 jit_solution(9406618166542396886)
XLA Ops:
  7.3 2.7 %pad_maximum_fusion.1 = bf16[6144,128]{1,0:T(8,128)(2,1)} fusion(bf16[2048,128]{1,0:T(8,128)(2,1)} %bitcast.310, bf16[2048,128]{1,0:T(8,128)(2,1)} %bitcast.311, bf16[2048,128]{1,0:T(8,128)(2,1)} %bitcast.312), kind=kLoop, calls=%fused_computation.24 | loop fusion | flops 4718592 | bytes 3145728 | tf_op jit(solution)/shard_map/concatenate | solution.py:93
  10.1 3.9 %collective-permute-start = (bf16[64,3]{1,0:T(8,128)(2,1)S(1)}, bf16[64,3]{1,0:T(8,128)(2,1)S(1)}, u32[]{:S(2)}, u32[]{:S(2)}) collective-permute-start(bf16[64,3]{1,0:T(8,128)(2,1)S(1)} %slice.411), channel_id=1, source_target_pairs={{0,16},{16,32},{32,48},{48,64},{64,80},{80,96},{96,112},{112,128},... | collective-permute-start | bytes 1160 | tf_op jit(solution)/shard_map/ppermute | solution.py:56
  14.1 0.1 eq.29
  14.3 0.1 eq.25
  14.5 0.6 reduce-window.6
  15.0 0.2 slice_reduce_fusion
  15.4 0.1 mul.822
  15.6 0.2 fusion.25
  15.8 0.2 fusion.27
  16.1 1.4 scatter_custom_fusion
  17.6 2.5 %gather_fusion = bf16[384,2048]{1,0:T(8,128)(2,1)S(1)} fusion(bf16[129,2048]{1,0:T(8,128)(2,1)S(1)} %concatenate.73, s32[1024]{0:T(1024)S(1)} %pad_clamp_fusion.1), kind=kCustom, calls=%fused_computation | custom fusion | bytes 3147264 | tf_op jit(solution)/shard_map/gather | solution.py:238
  20.0 0.8 dynamic-slice_multiply_fusion
  20.8 0.7 dynamic-slice_convert_fusion
  21.6 1.0 split.21
  22.6 0.8 split.20
  23.5 0.1 maximum_convert_fusion
  23.7 0.5 fusion.36
  24.2 0.3 fusion.20
  24.5 0.3 copy.49
  24.9 0.3 exponential_bitcast_fusion
  25.2 0.9 fusion.74
  26.3 1.3 fusion.17
  27.6 0.3 copy.51
  27.9 0.3 copy.101
  28.2 0.1 bitcast_add_fusion
  29.9 0.7 reshape.178
  30.6 6.5 %all-to-all-start = ((f32[16,1,128]{2,1,0:T(1,128)}), f32[16,1,128]{2,1,0:T(1,128)S(1)}, u32[]{:S(2)}, u32[]{:S(2)}) async-start(f32[16,1,128]{2,1,0:T(1,128)} %reshape.178), calls=%async_computation | async-start | bytes 16384 | tf_op jit(solution)/shard_map/all_to_all | solution.py:11
  37.1 0.6 constant_dynamic-update-slice_fusion.31
  37.8 0.6 constant_dynamic-update-slice_fusion.30
  38.4 0.6 constant_dynamic-update-slice_fusion.29
  39.0 0.6 constant_dynamic-update-slice_fusion.28
  39.7 0.6 constant_dynamic-update-slice_fusion.27
  40.3 0.6 constant_dynamic-update-slice_fusion.26
  41.0 0.6 constant_dynamic-update-slice_fusion.25
  41.6 0.6 constant_dynamic-update-slice_fusion.24
  42.2 0.6 constant_dynamic-update-slice_fusion.23
  42.9 0.6 constant_dynamic-update-slice_fusion.22
  43.5 0.6 constant_dynamic-update-slice_fusion.21
  44.2 0.6 constant_dynamic-update-slice_fusion.20
  44.8 0.6 constant_dynamic-update-slice_fusion.19
  45.4 0.7 constant_dynamic-update-slice_fusion.18
  46.1 0.6 constant_dynamic-update-slice_fusion.17
  46.7 0.6 constant_dynamic-update-slice_fusion.16
  47.4 6.7 %all-to-all-start.2 = ((bf16[16,1,8,2048]{3,2,1,0:T(8,128)(2,1)}), bf16[16,1,8,2048]{3,2,1,0:T(8,128)(2,1)S(1)}, u32[]{:S(2)}, u32[]{:S(2)}) async-start(bf16[16,1,8,2048]{3,2,1,0:T(8,128)(2,1)} %split.20), calls=%async_computation.2 | async-start | bytes 1048576 | tf_op jit(solution)/shard_map/all_to_all | solution.py:84
  54.0 0.5 broadcast.206
  54.6 0.7 reduce.2
  55.7 8.4 %all-to-all-done.2 = bf16[16,1,8,2048]{3,2,1,0:T(8,128)(2,1)S(1)} async-done(((bf16[16,1,8,2048]{3,2,1,0:T(8,128)(2,1)}), bf16[16,1,8,2048]{3,2,1,0:T(8,128)(2,1)S(1)}, u32[]{:S(2)}, u32[]{:S(2)}) %all-to-all-start.2) | async-done | bytes 524320 | tf_op jit(solution)/shard_map/all_to_all | solution.py:84
  64.1 3.7 %all-to-all-start.3 = ((bf16[16,1,16,2048]{3,2,1,0:T(8,128)(2,1)}), bf16[16,1,16,2048]{3,2,1,0:T(8,128)(2,1)S(1)}, u32[]{:S(2)}, u32[]{:S(2)}) async-start(bf16[16,1,16,2048]{3,2,1,0:T(8,128)(2,1)} %split.21), calls=%async_computation.3 | async-start | bytes 2097152 | tf_op jit(solution)/shard_map/all_to_all | solution.py:84
  67.8 1.4 add_bitcast_fusion
  69.2 0.6 copy.70
  69.9 0.3 copy.71
  70.2 0.9 copy_bitcast_fusion.1
  71.1 11.6 %all-to-all-done.3 = bf16[16,1,16,2048]{3,2,1,0:T(8,128)(2,1)S(1)} async-done(((bf16[16,1,16,2048]{3,2,1,0:T(8,128)(2,1)}), bf16[16,1,16,2048]{3,2,1,0:T(8,128)(2,1)S(1)}, u32[]{:S(2)}, u32[]{:S(2)}) %all-to-all-start.3) | async-done | bytes 1048608 | tf_op jit(solution)/shard_map/all_to_all | solution.py:84
  82.7 12.0 %all-to-all-start.1 = ((bf16[64,16,128]{2,0,1:T(8,128)(2,1)}), bf16[64,16,128]{2,0,1:T(8,128)(2,1)S(1)}, u32[]{:S(2)}, u32[]{:S(2)}) async-start(bf16[64,16,128]{2,0,1:T(8,128)(2,1)} %copy_bitcast_fusion.1), calls=%async_computation.1 | async-start | bytes 524288 | tf_op jit(solution)/shard_map/all_to_all | solution.py:202
  94.7 0.2 pad_maximum_fusion
  94.9 66.8 %all-gather.2.cloned.1.call-done = bf16[6144,2048]{1,0:T(8,128)(2,1)} async-done(((bf16[6144,128]{1,0:T(8,128)(2,1)}), bf16[6144,2048]{1,0:T(8,128)(2,1)}) %all-gather.2.cloned.1.call-update) | async-done | bytes 25165840 | tf_op jit(solution)/shard_map/all_gather | solution.py:94
  161.7 8.4 %fusion.2 = f32[384,2048]{1,0:T(8,128)} fusion(bf16[384,2048]{1,0:T(8,128)(2,1)S(1)} %bitcast.289, bf16[6144,2048]{1,0:T(8,128)(2,1)} %all-gather.2.cloned.1.call-done), kind=kOutput, calls=%fused_computation.5 | convolution fusion | flops 3221225472 | bytes 13107200 | tf_op jit(solution)/shard_map/dot_general | solution.py:102
  170.1 15.3 %fusion.8 = bf16[384,2048]{1,0:T(8,128)(2,1)} fusion(bf16[6144,2048]{1,0:T(8,128)(2,1)} %all-gather.2.cloned.1.call-done, f32[384,2048]{1,0:T(8,128)} %fusion.2, bf16[384,2048]{1,0:T(8,128)(2,1)S(1)} %bitcast.290), kind=kOutput, calls=%fused_computation.10 | convolution fusion | flops 6451101696 | bytes 23068672 | tf_op jit(solution)/shard_map/dot_general | solution.py:110
  185.4 6.7 %all-to-all-start.4 = ((bf16[16,24,2048]{2,1,0:T(8,128)(2,1)}), bf16[16,24,2048]{2,1,0:T(8,128)(2,1)S(1)}, u32[]{:S(2)}, u32[]{:S(2)}) async-start(bf16[16,24,2048]{2,1,0:T(8,128)(2,1)} %bitcast.64), calls=%async_computation.4 | async-start | bytes 3145728 | tf_op jit(solution)/shard_map/all_to_all | solution.py:246
  192.2 3.7 %convolution_convert_fusion = bf16[128,2048]{1,0:T(8,128)(2,1)} fusion(bf16[1024,128]{1,0:T(8,128)(2,1)S(1)} %bitcast.306, bf16[1024,2048]{1,0:T(8,128)(2,1)} %param.22), kind=kOutput, calls=%fused_computation.11 | convolution fusion | flops 537133056 | bytes 4980736 | tf_op jit(solution)/shard_map/dot_general | solution.py:201
  195.9 20.7 %all-to-all-done.4 = bf16[16,24,2048]{2,1,0:T(8,128)(2,1)S(1)} async-done(((bf16[16,24,2048]{2,1,0:T(8,128)(2,1)}), bf16[16,24,2048]{2,1,0:T(8,128)(2,1)S(1)}, u32[]{:S(2)}, u32[]{:S(2)}) %all-to-all-start.4) | async-done | bytes 1572896 | tf_op jit(solution)/shard_map/all_to_all | solution.py:246
  216.6 1.4 gather_fusion.1
  218.0 1.3 reshape.149
  219.4 3.9 %multiply_reduce_fusion = bf16[128,2048]{1,0:T(8,128)(2,1)} fusion(f32[128,2,2048]{2,1,0:T(2,128)S(1)} %reshape.149, f32[128,2]{1,0:T(8,128)S(1)} %copy.79), kind=kLoop, calls=%fused_computation.22 | loop fusion | flops 786432 | bytes 2622464 | tf_op jit(solution)/shard_map/reduce_sum | solution.py:250
  (177 shorter events, 2.6 us)
Async XLA Ops:
  7.2 17.0 %copy-start = (bf16[16,64,64]{2,1,0:T(8,128)(2,1)S(1)}, bf16[16,64,64]{2,1,0:T(8,128)(2,1)}, u32[]{:S(2)}) copy-start(bf16[16,64,64]{2,1,0:T(8,128)(2,1)} %param.18) | copy-start | bytes 393220
  7.2 2.8 %copy-start.3 = (bf16[64,2048]{1,0:T(8,128)(2,1)S(1)}, bf16[64,2048]{1,0:T(8,128)(2,1)}, u32[]{:S(2)}) copy-start(bf16[64,2048]{1,0:T(8,128)(2,1)} %param.15) | copy-start | bytes 786436
  7.2 6.8 %copy-start.6 = (s32[128,2]{0,1:T(2,128)S(1)}, s32[128,2]{0,1:T(2,128)}, u32[]{:S(2)}) copy-start(s32[128,2]{0,1:T(2,128)} %param.25) | copy-start | bytes 3076
  7.2 8.3 %copy-start.7 = (bf16[2048]{0:T(1024)(128)(2,1)S(1)}, bf16[2048]{0:T(1024)(128)(2,1)}, u32[]{:S(2)}) copy-start(bf16[2048]{0:T(1024)(128)(2,1)} %param.24) | copy-start | bytes 12292
  7.2 8.3 %copy-start.2 = (bf16[128,2048]{1,0:T(8,128)(2,1)S(1)}, bf16[128,2048]{1,0:T(8,128)(2,1)}, u32[]{:S(2)}) copy-start(bf16[128,2048]{1,0:T(8,128)(2,1)} %param.23) | copy-start | bytes 1572868
  7.2 154.4 %all-gather.2.cloned.1.call-start = ((), (), s32[]{:S(2)}) async-start(), calls=%async_computation.5 | async-start | bytes 26738688 | tf_op jit(solution)/shard_map/all_gather | solution.py:94
  10.1 13.4 %collective-permute-start = (bf16[64,3]{1,0:T(8,128)(2,1)S(1)}, bf16[64,3]{1,0:T(8,128)(2,1)S(1)}, u32[]{:S(2)}, u32[]{:S(2)}) collective-permute-start(bf16[64,3]{1,0:T(8,128)(2,1)S(1)} %slice.411), channel_id=1, source_target_pairs={{0,16},{16,32},{32,48},{48,64},{64,80},{80,96},{96,112},{112,128},... | collective-permute-start | bytes 1160 | tf_op jit(solution)/shard_map/ppermute | solution.py:56
  20.0 3.4 %copy-start.5 = (f32[2048]{0:T(1024)S(1)}, f32[2048]{0:T(1024)}, u32[]{:S(2)}) copy-start(f32[2048]{0:T(1024)} %param.21) | copy-start | bytes 24580
  30.6 16.8 %all-to-all-start = ((f32[16,1,128]{2,1,0:T(1,128)}), f32[16,1,128]{2,1,0:T(1,128)S(1)}, u32[]{:S(2)}, u32[]{:S(2)}) async-start(f32[16,1,128]{2,1,0:T(1,128)} %reshape.178), calls=%async_computation | async-start | bytes 16384 | tf_op jit(solution)/shard_map/all_to_all | solution.py:11
  47.4 16.7 %all-to-all-start.2 = ((bf16[16,1,8,2048]{3,2,1,0:T(8,128)(2,1)}), bf16[16,1,8,2048]{3,2,1,0:T(8,128)(2,1)S(1)}, u32[]{:S(2)}, u32[]{:S(2)}) async-start(bf16[16,1,8,2048]{3,2,1,0:T(8,128)(2,1)} %split.20), calls=%async_computation.2 | async-start | bytes 1048576 | tf_op jit(solution)/shard_map/all_to_all | solution.py:84
  64.1 18.6 %all-to-all-start.3 = ((bf16[16,1,16,2048]{3,2,1,0:T(8,128)(2,1)}), bf16[16,1,16,2048]{3,2,1,0:T(8,128)(2,1)S(1)}, u32[]{:S(2)}, u32[]{:S(2)}) async-start(bf16[16,1,16,2048]{3,2,1,0:T(8,128)(2,1)} %split.21), calls=%async_computation.3 | async-start | bytes 2097152 | tf_op jit(solution)/shard_map/all_to_all | solution.py:84
  67.8 2.4 %copy-start.4 = (bf16[64,2048]{1,0:T(8,128)(2,1)S(1)}, bf16[64,2048]{1,0:T(8,128)(2,1)}, u32[]{:S(2)}) copy-start(bf16[64,2048]{1,0:T(8,128)(2,1)} %param.16) | copy-start | bytes 786436
  82.7 102.7 %all-to-all-start.1 = ((bf16[64,16,128]{2,0,1:T(8,128)(2,1)}), bf16[64,16,128]{2,0,1:T(8,128)(2,1)S(1)}, u32[]{:S(2)}, u32[]{:S(2)}) async-start(bf16[64,16,128]{2,0,1:T(8,128)(2,1)} %copy_bitcast_fusion.1), calls=%async_computation.1 | async-start | bytes 524288 | tf_op jit(solution)/shard_map/all_to_all | solution.py:202
  185.4 6.7 %copy-start.8 = (f32[128,2]{0,1:T(2,128)S(1)}, f32[128,2]{0,1:T(2,128)}, u32[]{:S(2)}) copy-start(f32[128,2]{0,1:T(2,128)} %param.26) | copy-start | bytes 3076
  185.4 31.2 %all-to-all-start.4 = ((bf16[16,24,2048]{2,1,0:T(8,128)(2,1)}), bf16[16,24,2048]{2,1,0:T(8,128)(2,1)S(1)}, u32[]{:S(2)}, u32[]{:S(2)}) async-start(bf16[16,24,2048]{2,1,0:T(8,128)(2,1)} %bitcast.64), calls=%async_computation.4 | async-start | bytes 3145728 | tf_op jit(solution)/shard_map/all_to_all | solution.py:246
  216.6 6.6 %copy-start.1 = (bf16[16,64,64]{2,1,0:T(8,128)(2,1)S(1)}, bf16[16,64,64]{2,1,0:T(8,128)(2,1)}, u32[]{:S(2)}) copy-start(bf16[16,64,64]{2,1,0:T(8,128)(2,1)} %param.18) | copy-start | bytes 393220
Sparse Core Ops, SparseCore 0:
  10.1 151.4 all-gather.1
where the time goes:
time: 231 us; the launch traced here: 230 us
  waiting for transfers between devices  108 us (47%)
  starting transfers between devices  39.4 us (17%)
  matrix products  29.1 us (13%)
  other arithmetic  23.6 us (10%)
  local copies, waits for them, and re-layouts  15.4 us (7%)
  between operations  15 us (6%)
    all_gather x1, waiting for transfers between devices, sent_together(): lax.all_gather(both, axis, axis=dim, tiled=True)  66.8 us
    all_to_all x1, waiting for transfers between devices, expert_half(): lax.all_to_all(outbound, 'ep', split_axis=0, concat_axis=0, tiled=True)  20.7 us
    all_to_all x2, waiting for transfers between devices, cut_exchange(): lax.all_to_all(section, axis, split_axis=0, concat_axis=0, tiled=True)  20 us
    dot_general x1, matrix products, down_product(): lax.dot_general(units, down_piece, (((1,), (1,)), ((), ())), preferred_el...  15.3 us
    all_to_all x1, starting transfers between devices, mixer_half(): lax.all_to_all(pieces, 'tp', split_axis=1, concat_axis=0, tiled=True)  12 us
    all_to_all x2, starting transfers between devices, cut_exchange(): lax.all_to_all(section, axis, split_axis=0, concat_axis=0, tiled=True)  10.3 us
    unnamed x16, other arithmetic  8.93 us
    dot_general x1, matrix products, expert_units(): gate_pre = jnp.dot(rows, gate_piece, preferred_element_type=jnp.float32)  8.43 us
  transfers between devices with their start and end apart: 7, of which 4 were waited for; matrix products, arithmetic and copies ran while one was open for 26% of the time, Pallas kernels for 0%

commit v1 on v0

v1 whole, which is shorter than its diff:
```python
import jax
import jax.numpy as jnp
from jax import lax
from jax.experimental import pallas as pl
from jax.experimental.pallas import tpu as pltpu
from jax.sharding import PartitionSpec as P


LANES = 128
TILES_AT_ONCE = 4
CUT = 512


def from_everyone(x, axis):
    copies = jnp.broadcast_to(x, (lax.axis_size(axis), *x.shape))
    return lax.all_to_all(copies, axis, split_axis=0, concat_axis=0, tiled=True)


def from_behind(x, axis, by):
    count = lax.axis_size(axis)
    pairs = [(i, i + by) for i in range(count) if 0 <= i + by < count]
    return lax.ppermute(x, axis, pairs)


def along_z(x, by):
    tp = lax.axis_size("tp")
    return lax.ppermute(x, "tp", [(i, (i + 2 * by) % tp) for i in range(tp)])


def other_core(x):
    tp = lax.axis_size("tp")
    return lax.ppermute(x, "tp", [(i, i ^ 1) for i in range(tp)])


def times(a, b):
    return jnp.dot(a, b, preferred_element_type=jnp.float32)


def times_t(a, b):
    return lax.dot_general(a, b, (((1,), (1,)), ((), ())), preferred_element_type=jnp.float32)


def cost(flops, moved):
    return pl.CostEstimate(flops=flops, bytes_accessed=moved, transcendentals=0)


def minus_expm1(v, exp_v):
    series = 1.0 + v * (1.0 / 9.0)
    for k in range(8, 1, -1):
        series = 1.0 + v * (1.0 / k) * series
    return jnp.where(v > -0.5, -v * series, 1.0 - exp_v)


def local_scan(x, halo, taps, rate_map, entry_map, fade, spike, group):
    channels, positions = x.shape
    block = rate_map.shape[1]

    def body(_, x_ref, halo_ref, taps_ref, rate_ref, entry_ref, fade_ref, spike_ref, decay_ref, state_ref, total_ref, map_ref):
        map_ref[:block] = rate_ref[0].astype(jnp.float32).T.astype(jnp.bfloat16)
        map_ref[block:] = entry_ref[0].astype(jnp.float32).T.astype(jnp.bfloat16)
        lane = lax.broadcasted_iota(jnp.int32, (channels, LANES), 1)
        tap = [taps_ref[:, k : k + 1].astype(jnp.float32) for k in range(4)]
        speed = -8.0 * fade_ref[...]

        def rolled(a):
            return [pltpu.roll(a, s, 1) for s in (1, 2, 3)]

        def steps(chunk, carry):
            decay_run, state_run, before = carry[0], carry[1], list(carry[2:])
            found = []
            for t in range(TILES_AT_ONCE):
                at = pl.ds(pl.multiple_of((chunk * TILES_AT_ONCE + t) * LANES, LANES), LANES)
                here = x_ref[:, at].astype(jnp.float32)
                moved = rolled(here)
                conv = here * tap[3]
                for s in (1, 2, 3):
                    conv = conv + tap[3 - s] * jnp.where(lane < s, before[s - 1], moved[s - 1])
                before = moved
                conv = conv.astype(jnp.bfloat16)
                gates = times(map_ref[...], conv)
                rate = jax.nn.sigmoid(gates[:block])
                inflow = jax.nn.sigmoid(gates[block:])
                exponent = rate * speed + spike_ref[:, at]
                decay = jnp.exp(exponent)
                share = minus_expm1(2.0 * exponent, decay * decay)
                root = jnp.where(share > 0.0, jnp.sqrt(share), 0.0)
                state = root * inflow * conv.astype(jnp.float32)
                k = 1
                while k < LANES:
                    inside = lane >= k
                    state = state + jnp.where(inside, decay * pltpu.roll(state, k, 1), 0.0)
                    decay = decay * jnp.where(inside, pltpu.roll(decay, k, 1), 1.0)
                    k *= 2
                found.append((at, decay, state))
            for at, decay, state in found:
                state = state + decay * state_run
                decay = decay * decay_run
                decay_ref[:, at] = decay
                state_ref[:, at] = state
                decay_run = jnp.broadcast_to(decay[:, LANES - 1 :], decay.shape)
                state_run = jnp.broadcast_to(state[:, LANES - 1 :], state.shape)
            return (decay_run, state_run, *before)

        one = jnp.ones((channels, LANES), jnp.float32)
        first = (one, jnp.zeros_like(one), *rolled(halo_ref[...].astype(jnp.float32)))
        last = lax.fori_loop(0, positions // (LANES * TILES_AT_ONCE), steps, first)
        ends = jnp.where(lane == 0, last[0], jnp.where(lane == 1, last[1], 0.0))
        total_ref[...] = ends.T[:8]

    whole = lambda *shape: pl.BlockSpec(shape, lambda i, g: (0,) * len(shape))
    return pl.pallas_call(
        body,
        grid_spec=pltpu.PrefetchScalarGridSpec(
            num_scalar_prefetch=1,
            grid=(1,),
            in_specs=[
                whole(channels, positions),
                whole(channels, LANES),
                pl.BlockSpec((channels, 4), lambda i, g: (g[0], 0)),
                pl.BlockSpec((1, block, block), lambda i, g: (g[0], 0, 0)),
                pl.BlockSpec((1, block, block), lambda i, g: (g[0], 0, 0)),
                pl.BlockSpec((channels, 1), lambda i, g: (g[0], 0)),
                whole(1, positions),
            ],
            out_specs=[
                whole(channels, positions),
                whole(channels, positions),
                whole(8, channels),
            ],
            scratch_shapes=[pltpu.VMEM((2 * block, block), jnp.bfloat16)],
        ),
        out_shape=[
            jax.ShapeDtypeStruct((channels, positions), jnp.float32),
            jax.ShapeDtypeStruct((channels, positions), jnp.float32),
            jax.ShapeDtypeStruct((8, channels), jnp.float32),
        ],
        cost_estimate=cost(4 * 10**9, 2 * 10**6),
        compiler_params=pltpu.CompilerParams(vmem_limit_bytes=12 * 2**20),
        name="local_scan",
    )(group, x, halo, taps, rate_map, entry_map, fade, spike)


def gated_states(decay, state, switch, totals, place, pieces):
    channels, positions = decay.shape
    width = positions // pieces

    def body(place_ref, decay_ref, state_ref, switch_ref, totals_ref, out_ref):
        entering = jnp.zeros((1, channels), jnp.float32)
        for b in range(totals.shape[0]):
            passed = b < place_ref[0]
            entering = jnp.where(
                passed, totals_ref[b, 0:1] * entering + totals_ref[b, 1:2], entering
            )
        entering = jnp.broadcast_to(entering, (LANES, channels)).T
        for p in range(pieces):
            at = slice(p * width, (p + 1) * width)
            whole = state_ref[:, at] + decay_ref[:, at] * entering
            gate = jax.nn.gelu(switch_ref[:, at].astype(jnp.float32), approximate=True)
            out_ref[p] = (whole * gate).astype(jnp.bfloat16)

    vmem = pl.BlockSpec(memory_space=pltpu.VMEM)
    return pl.pallas_call(
        body,
        in_specs=[pl.BlockSpec(memory_space=pltpu.SMEM)] + [vmem] * 4,
        out_specs=vmem,
        out_shape=jax.ShapeDtypeStruct((pieces, channels, width), jnp.bfloat16),
        cost_estimate=cost(10**9, 2 * 10**6),
        compiler_params=pltpu.CompilerParams(vmem_limit_bytes=12 * 2**20),
        name="gated_states",
    )(place, decay, state, switch, totals)


def mixer_half(
    scan_source_values,
    switch_path_values,
    causal_filter_coefficients,
    scan_switch_blockmap,
    entry_switch_blockmap,
    feature_fading_speeds,
    spike_amount,
    final_linear_map,
):
    halo = from_behind(scan_source_values[:, -LANES:], "ep", 1)
    decay, state, total = local_scan(
        scan_source_values,
        halo,
        causal_filter_coefficients,
        scan_switch_blockmap,
        entry_switch_blockmap,
        feature_fading_speeds[:, None],
        spike_amount[None, :],
        lax.axis_index("tp").astype(jnp.int32)[None],
    )
    pieces = gated_states(
        decay,
        state,
        switch_path_values,
        from_everyone(total, "ep"),
        lax.axis_index("ep").astype(jnp.int32)[None],
        lax.axis_size("tp"),
    )
    mixed = lax.all_to_all(pieces, "tp", split_axis=0, concat_axis=0, tiled=True)
    return lax.dot_general(
        mixed.reshape(-1, mixed.shape[2]),
        final_linear_map,
        (((0,), (0,)), ((), ())),
        preferred_element_type=jnp.float32,
    ).astype(jnp.bfloat16)


def token_rows(activity, gain, ids, share, experts, slots):
    tokens, width = activity.shape

    def body(act_ref, gain_ref, ids_ref, share_ref, rows_ref, back_ref):
        values = act_ref[...].astype(jnp.float32)
        scale = lax.rsqrt(jnp.mean(values * values, axis=1, keepdims=True) + 1e-06)
        normed = (values * scale * gain_ref[...].astype(jnp.float32)).astype(jnp.bfloat16)
        expert = lax.broadcasted_iota(jnp.int32, (experts, tokens), 0)
        earlier = lax.broadcasted_iota(jnp.int32, (tokens, tokens), 0)
        later = lax.broadcasted_iota(jnp.int32, (tokens, tokens), 1)
        ahead = (earlier < later).astype(jnp.float32).astype(jnp.bfloat16)
        slot = lax.broadcasted_iota(jnp.int32, (experts * slots, tokens), 0)
        count = jnp.zeros((experts, 1), jnp.float32)
        taken = jnp.zeros((experts * slots, tokens), jnp.float32)
        back = jnp.zeros((experts * slots, tokens), jnp.float32)
        for j in range(ids.shape[0]):
            mine = (expert == ids_ref[j : j + 1]).astype(jnp.float32)
            rank = times(mine.astype(jnp.bfloat16), ahead) + count
            rank = jnp.sum(mine * rank, axis=0, keepdims=True)
            count = count + jnp.sum(mine, axis=1, keepdims=True)
            here = slot == ids_ref[j : j + 1] * slots + rank.astype(jnp.int32)
            taken = taken + jnp.where(here, 1.0, 0.0)
            back = back + jnp.where(here, share_ref[j : j + 1], 0.0)
        rows_ref[...] = times(taken.astype(jnp.bfloat16), normed).astype(jnp.bfloat16)
        rest = back.T
        for k in range(3):
            part = rest.astype(jnp.bfloat16)
            back_ref[k] = part
            rest = rest - part.astype(jnp.float32)

    return pl.pallas_call(
        body,
        out_shape=[
            jax.ShapeDtypeStruct((experts * slots, width), jnp.bfloat16),
            jax.ShapeDtypeStruct((3, tokens, experts * slots), jnp.bfloat16),
        ],
        cost_estimate=cost(10**9, 2 * 10**6),
        compiler_params=pltpu.CompilerParams(vmem_limit_bytes=12 * 2**20),
        name="token_rows",
    )(activity, gain, ids, share)


def weighted_sum(back, results):
    parts, tokens, slots = back.shape
    width = results.shape[1]

    def body(back_ref, results_ref, out_ref):
        total = times(back_ref[0], results_ref[...])
        for k in range(1, parts):
            total = total + times(back_ref[k], results_ref[...])
        out_ref[...] = total.astype(jnp.bfloat16)

    return pl.pallas_call(
        body,
        out_shape=jax.ShapeDtypeStruct((tokens, width), jnp.bfloat16),
        cost_estimate=cost(2 * parts * tokens * slots * width, 2 * slots * width),
        compiler_params=pltpu.CompilerParams(vmem_limit_bytes=12 * 2**20),
        name="weighted_sum",
    )(back, results)


def near(x):
    return pltpu.with_memory_space_constraint(x, pltpu.VMEM)


def gated(gate_pre, up_pre):
    gate_cut = jnp.minimum(gate_pre, 7.0)
    up_cut = jnp.clip(up_pre, -7.0, 7.0)
    return ((up_cut + 1.0) * gate_cut * jax.nn.sigmoid(1.702 * gate_cut)).astype(jnp.bfloat16)


def expert_step(rows, shards, so_far, dtype):
    sets, count, width = len(rows), *rows[0].shape
    placed = pltpu.VMEM if dtype == jnp.float32 else jax.ShapeDtypeStruct
    hidden = shards[0][0][0].shape[1]
    operands, layout = [], []
    for shard in shards:
        layout.append([])
        for pieces in shard:
            layout[-1].append((len(operands), len(pieces)))
            operands += pieces

    def body(*refs):
        row_refs, weights = refs[:sets], refs[sets : sets + len(operands)]
        refs = refs[sets + len(operands) :]
        old, new = (refs[:sets], refs[sets:]) if so_far else ((), refs)

        def load(at):
            return jnp.concatenate([weights[at[0] + k][...] for k in range(at[1])], axis=0)

        def side_by_side(ats):
            return jnp.concatenate([load(at) for at in ats], axis=1)

        for k in range(sets):
            first = 0
            while first < len(shards):
                taken = layout[first : first + 2]
                base = old if first == 0 else new
                if len(taken) == 2:
                    gate_pre = times(row_refs[k][...], side_by_side([s[0] for s in taken]))
                    up_pre = times(row_refs[k][...], side_by_side([s[1] for s in taken]))
                else:
                    both = times(row_refs[k][...], side_by_side(taken[0][:2]))
                    gate_pre, up_pre = both[:, :hidden], both[:, hidden:]
                units = gated(gate_pre, up_pre)
                down = side_by_side([s[2] for s in taken])
                for at in range(0, width, CUT):
                    added = times_t(units, down[at : at + CUT])
                    if base:
                        added = base[k][:, at : at + CUT] + added
                    new[k][:, at : at + CUT] = added.astype(dtype)
                first += 2

    alias = {sets + len(operands) + k: k for k in range(sets)} if so_far and dtype == jnp.float32 else {}
    return pl.pallas_call(
        body,
        in_specs=[pl.BlockSpec(memory_space=pltpu.VMEM)] * (sets + len(operands) + len(so_far)),
        out_specs=[pl.BlockSpec(memory_space=pltpu.VMEM)] * sets,
        out_shape=[placed((count, width), dtype)] * sets,
        input_output_aliases=alias,
        cost_estimate=cost(
            2 * sets * count * 3 * width * hidden * len(shards), 6 * width * hidden * len(shards)
        ),
        compiler_params=pltpu.CompilerParams(vmem_limit_bytes=24 * 2**20),
    )(*map(near, rows), *operands, *map(near, so_far))


def z_ring(own):
    chips = lax.axis_size("tp") // 2
    up, down, found = own, own, []

    def moved(arrays, by):
        return [along_z(a, by) for a in arrays]

    for _ in range(1, chips // 2):
        up, down = moved(up, 1), moved(down, -1)
        found.append([[(a,) for a in up], [(a,) for a in down]])
    half = own[0].shape[0] // 2
    up = moved([a[:half] for a in up], 1)
    down = moved([a[half:] for a in down], -1)
    return found, list(zip(up, down))


def expert_half(
    dispatched_group_activity,
    specialist_rmsgain,
    selected_specialist_ids,
    selected_specialist_share,
    specialist_switch_maps,
    specialist_widen_maps,
    specialist_shrink_maps,
):
    token_count, model_width = dispatched_group_activity.shape
    route_count = selected_specialist_ids.shape[1]
    expert_count = lax.axis_size("ep")
    slot_count = 3 * route_count * token_count // (2 * expert_count)
    own = [specialist_switch_maps[0], specialist_widen_maps[0], specialist_shrink_maps[0]]
    found, opposite = z_ring(own)
    outgoing, back = token_rows(
        dispatched_group_activity,
        specialist_rmsgain[None, :],
        selected_specialist_ids.T,
        selected_specialist_share.T,
        expert_count,
        slot_count,
    )

    def exchange(rows):
        blocks = rows.reshape(expert_count, slot_count, model_width)
        return lax.all_to_all(blocks, "ep", split_axis=0, concat_axis=0, tiled=True).reshape(
            expert_count * slot_count, model_width
        )

    kept = exchange(outgoing)
    lent = other_core(kept)
    found[0].append([(a,) for a in own])
    partial = ()
    for shards in found:
        partial = expert_step((lent, kept), shards, tuple(partial), jnp.float32)
    (sent,) = expert_step((lent,), [opposite], partial[:1], jnp.bfloat16)
    back_home = other_core(sent)
    (mine,) = expert_step((kept,), [opposite], partial[1:], jnp.float32)
    result = (mine + back_home.astype(jnp.float32)).astype(jnp.bfloat16)
    return weighted_sum(back, exchange(result))


def on_device(
    scan_source_values,
    switch_path_values,
    causal_filter_coefficients,
    scan_switch_blockmap,
    entry_switch_blockmap,
    feature_fading_speeds,
    spike_amount,
    final_linear_map,
    dispatched_group_activity,
    specialist_rmsgain,
    selected_specialist_ids,
    selected_specialist_share,
    specialist_switch_maps,
    specialist_widen_maps,
    specialist_shrink_maps,
):
    scan_path_result = mixer_half(
        scan_source_values,
        switch_path_values,
        causal_filter_coefficients,
        scan_switch_blockmap,
        entry_switch_blockmap,
        feature_fading_speeds,
        spike_amount,
        final_linear_map,
    )
    moe_out = expert_half(
        dispatched_group_activity,
        specialist_rmsgain,
        selected_specialist_ids,
        selected_specialist_share,
        specialist_switch_maps,
        specialist_widen_maps,
        specialist_shrink_maps,
    )
    return (scan_path_result, moe_out)


def solution(mesh):
    in_specs = (
        P("tp", "ep"),
        P("tp", "ep"),
        P(),
        P(),
        P(),
        P(),
        P("ep"),
        P(),
        P(("ep", "tp"), None),
        P(),
        P(("ep", "tp"), None),
        P(("ep", "tp"), None),
        P("ep", None, "tp"),
        P("ep", None, "tp"),
        P("ep", None, "tp"),
    )
    out_specs = (P(("ep", "tp"), None), P(("ep", "tp"), None))
    return jax.shard_map(
        lambda *args: on_device(*args), mesh=mesh, in_specs=in_specs, out_specs=out_specs, check_vma=False
    )
```

time: 231 us -> 242 us (1.048)
  Pallas kernels: 0 us -> 28.7 us
  starting transfers between devices: 39.4 us -> 67.3 us
  matrix products: 29.1 us -> 3.86 us
  other arithmetic: 23.6 us -> 3.78 us
  between operations: 15 us -> 1.07 us
  local copies, waits for them, and re-layouts: 15.4 us -> 26.4 us
    ppermute x0 -> x26, waiting for transfers between devices: none -> 79.4 us  [the longest x24 79.4 us: along_z(): return lax.ppermute(x, 'tp', [(i, (i + 2 * by) % tp) for i in range(tp)])]
    all_gather x1 -> x0, waiting for transfers between devices: 66.8 us -> none  [sent_together(): lax.all_gather(both, axis, axis=dim, tiled=True)]
    ppermute x0 -> x26, starting transfers between devices: none -> 40.1 us  [the longest x24 29.9 us: along_z(): return lax.ppermute(x, 'tp', [(i, (i + 2 * by) % tp) for i in range(tp)])]
    pallas_call x0 -> x9, Pallas kernels: none -> 28.7 us  [the longest x5 19.5 us: expert_step(): pl.pallas_call(body, in_specs=[pl.BlockSpec(memory_space=pltpu.VMEM)] * (...]
    dot_general x5 -> x1, matrix products: 29.1 us -> 3.86 us  [mixer_half(): lax.dot_general(mixed.reshape(-1, mixed.shape[2]), final_linear_map, (((0...]
    unnamed x25 -> x87, local copies, waits for them, and re-layouts: 1.68 us -> 23.3 us
    all_to_all x4 -> x3, waiting for transfers between devices: 40.8 us -> 23.8 us  [the longest x2 23.1 us: exchange(): lax.all_to_all(blocks, 'ep', split_axis=0, concat_axis=0, tiled=True)]
    all_to_all x4 -> x3, starting transfers between devices: 29 us -> 17.5 us  [the longest x2 11.3 us: exchange(): lax.all_to_all(blocks, 'ep', split_axis=0, concat_axis=0, tiled=True)]
  transfers between devices with their start and end apart: 7 -> 31, of which waited for: 4 -> 12; matrix products, arithmetic and copies ran while one was open for 26% -> 5% of each run, Pallas kernels for 0% -> 9%
where the time goes in v1:
time: 242 us; the launch traced here: 241 us
  waiting for transfers between devices  110 us (45%)
  starting transfers between devices  67.3 us (28%)
  Pallas kernels  28.7 us (12%)
  local copies, waits for them, and re-layouts  26.4 us (11%)
  matrix products  3.86 us (2%)
  other arithmetic  3.78 us (2%)
    ppermute x24, waiting for transfers between devices, along_z(): return lax.ppermute(x, 'tp', [(i, (i + 2 * by) % tp) for i in range(tp)])  79.4 us
    ppermute x24, starting transfers between devices, along_z(): return lax.ppermute(x, 'tp', [(i, (i + 2 * by) % tp) for i in range(tp)])  29.9 us
    unnamed x87, local copies, waits for them, and re-layouts  23.3 us
    all_to_all x2, waiting for transfers between devices, exchange(): lax.all_to_all(blocks, 'ep', split_axis=0, concat_axis=0, tiled=True)  23.1 us
    pallas_call x5, Pallas kernels, expert_step(): pl.pallas_call(body, in_specs=[pl.BlockSpec(memory_space=pltpu.VMEM)] * (...  19.5 us
    all_to_all x2, starting transfers between devices, exchange(): lax.all_to_all(blocks, 'ep', split_axis=0, concat_axis=0, tiled=True)  11.3 us
    ppermute x2, starting transfers between devices, other_core(): return lax.ppermute(x, 'tp', [(i, i ^ 1) for i in range(tp)])  10.2 us
    all_to_all x1, waiting for transfers between devices, from_everyone(): return lax.all_to_all(copies, axis, split_axis=0, concat_axis=0, tiled=True)  6.45 us
  transfers between devices with their start and end apart: 31, of which 12 were waited for; matrix products, arithmetic and copies ran while one was open for 5% of the time, Pallas kernels for 9%

profile of v1, /device:TPU:1, one launch (start us, length us, event | category | flops | bytes accessed | tf_op | source)
XLA Modules:
  0.0 240.7 jit_solution(5973293359838016240)
XLA Ops:
  1.3 1.0 copy-done.25
  3.7 1.9 token_rows.1
  5.6 0.7 copy-done.20
  6.4 7.6 %all-to-all-start.2 = ((bf16[16,24,2048]{2,1,0:T(8,128)(2,1)}), bf16[16,24,2048]{2,1,0:T(8,128)(2,1)S(1)}, u32[]{:S(2)}, u32[]{:S(2)}) async-start(bf16[16,24,2048]{2,1,0:T(8,128)(2,1)} %bitcast.7), calls=%async_computation.2 | async-start | bytes 3145728 | tf_op jit(solution)/shard_map/all_to_all | solution.py:380
  14.0 1.7 collective-permute-start.1
  15.7 1.6 collective-permute-start.9
  17.3 2.5 %collective-permute-start.13 = (bf16[2048,128]{1,0:T(8,128)(2,1)S(1)}, bf16[2048,128]{1,0:T(8,128)(2,1)}, u32[]{:S(2)}, u32[]{:S(2)}) collective-permute-start(bf16[2048,128]{1,0:T(8,128)(2,1)S(1)} %bitcast.23), channel_id=1, source_target_pairs={{0,14},{1,15},{2,0},{3,1},{4,2},{5,3},{6,4},{7,5},{8,6},{9,7},{10,... | collective-permute-start | bytes 1572872 | tf_op jit(solution)/shard_map/ppermute | solution.py:27
  19.8 2.7 %collective-permute-start.21 = (bf16[2048,128]{1,0:T(8,128)(2,1)}, bf16[2048,128]{1,0:T(8,128)(2,1)S(1)}, u32[]{:S(2)}, u32[]{:S(2)}) collective-permute-start(bf16[2048,128]{1,0:T(8,128)(2,1)} %bitcast.11.refs_10_), channel_id=1, source_target_pairs={{0,14},{1,15},{2,0},{3,1},{4,2},{5,3},{6,4},{7,5},{8,6},{9,7},{10,... | collective-permute-start | bytes 1572872 | tf_op jit(solution)/shard_map/ppermute | solution.py:27
  22.5 8.8 %collective-permute-done.1.refs_2_ = bf16[2048,128]{1,0:T(8,128)(2,1)} collective-permute-done((bf16[2048,128]{1,0:T(8,128)(2,1)}, bf16[2048,128]{1,0:T(8,128)(2,1)}, u32[]{:S(2)}, u32[]{:S(2)}) %collective-permute-start.1) | collective-permute-done | bytes 524320 | tf_op jit(solution)/shard_map/ppermute | solution.py:27
  31.3 1.2 collective-permute-start.5
  32.4 10.1 %collective-permute-done.9.refs_3_ = bf16[2048,128]{1,0:T(8,128)(2,1)} collective-permute-done((bf16[2048,128]{1,0:T(8,128)(2,1)S(1)}, bf16[2048,128]{1,0:T(8,128)(2,1)}, u32[]{:S(2)}, u32[]{:S(2)}) %collective-permute-start.9) | collective-permute-done | bytes 524320 | tf_op jit(solution)/shard_map/ppermute | solution.py:27
  42.5 2.7 %collective-permute-start.14 = (bf16[2048,128]{1,0:T(8,128)(2,1)}, bf16[2048,128]{1,0:T(8,128)(2,1)S(1)}, u32[]{:S(2)}, u32[]{:S(2)}) collective-permute-start(bf16[2048,128]{1,0:T(8,128)(2,1)} %collective-permute-done.13.refs_6_), channel_id=1, source_target_pairs={{0,14},{1,15},{2,0},{3,1},{4,2},{5,3},{6,4},{7,5},{8,6},{9,7},{10,... | collective-permute-start | bytes 1572872 | tf_op jit(solution)/shard_map/ppermute | solution.py:27
  45.2 8.6 %collective-permute-done.17.refs_4_ = bf16[2048,128]{1,0:T(8,128)(2,1)} collective-permute-done((bf16[2048,128]{1,0:T(8,128)(2,1)}, bf16[2048,128]{1,0:T(8,128)(2,1)}, u32[]{:S(2)}, u32[]{:S(2)}) %collective-permute-start.17) | collective-permute-done | bytes 524320 | tf_op jit(solution)/shard_map/ppermute | solution.py:27
  54.6 2.8 %collective-permute-start.25 = (bf16[384,2048]{1,0:T(8,128)(2,1)S(1)}, bf16[384,2048]{1,0:T(8,128)(2,1)S(1)}, u32[]{:S(2)}, u32[]{:S(2)}) collective-permute-start(bf16[384,2048]{1,0:T(8,128)(2,1)S(1)} %bitcast.16), channel_id=1, source_target_pairs={{0,1},{1,0},{2,3},{3,2},{4,5},{5,4},{6,7},{7,6},{8,9},{9,8},{10,11... | collective-permute-start | bytes 4718600 | tf_op jit(solution)/shard_map/ppermute | solution.py:32
  57.3 7.5 %collective-permute-done.10.refs_3_ = bf16[2048,128]{1,0:T(8,128)(2,1)S(1)} collective-permute-done((bf16[2048,128]{1,0:T(8,128)(2,1)}, bf16[2048,128]{1,0:T(8,128)(2,1)S(1)}, u32[]{:S(2)}, u32[]{:S(2)}) %collective-permute-start.10) | collective-permute-done | bytes 524320 | tf_op jit(solution)/shard_map/ppermute | solution.py:27
  64.9 1.2 collective-permute-start.22
  66.1 1.2 collective-permute-start.6
  67.2 8.9 %collective-permute-done.18.refs_4_ = bf16[2048,128]{1,0:T(8,128)(2,1)S(1)} collective-permute-done((bf16[2048,128]{1,0:T(8,128)(2,1)}, bf16[2048,128]{1,0:T(8,128)(2,1)S(1)}, u32[]{:S(2)}, u32[]{:S(2)}) %collective-permute-start.18) | collective-permute-done | bytes 524320 | tf_op jit(solution)/shard_map/ppermute | solution.py:27
  76.1 11.3 %collective-permute-done.2.refs_2_ = bf16[2048,128]{1,0:T(8,128)(2,1)} collective-permute-done((bf16[2048,128]{1,0:T(8,128)(2,1)}, bf16[2048,128]{1,0:T(8,128)(2,1)}, u32[]{:S(2)}, u32[]{:S(2)}) %collective-permute-start.2) | collective-permute-done | bytes 524320 | tf_op jit(solution)/shard_map/ppermute | solution.py:27
  87.4 1.2 collective-permute-start.15
  88.9 2.4 collective-permute-start.23
  91.3 7.3 %collective-permute-done.11.refs_3_ = bf16[2048,128]{1,0:T(8,128)(2,1)S(1)} collective-permute-done((bf16[2048,128]{1,0:T(8,128)(2,1)S(1)}, bf16[2048,128]{1,0:T(8,128)(2,1)S(1)}, u32[]{:S(2)}, u32[]{:S(2)}) %collective-permute-start.11) | collective-permute-done | bytes 524320 | tf_op jit(solution)/shard_map/ppermute | solution.py:27
  98.6 2.7 %collective-permute-start.7 = (bf16[2048,128]{1,0:T(8,128)(2,1)S(1)}, bf16[2048,128]{1,0:T(8,128)(2,1)S(1)}, u32[]{:S(2)}, u32[]{:S(2)}) collective-permute-start(bf16[2048,128]{1,0:T(8,128)(2,1)S(1)} %collective-permute-done.6.refs_5_), channel_id=1, source_target_pairs={{0,14},{1,15},{2,0},{3,1},{4,2},{5,3},{6,4},{7,5},{8,6},{9,7},{10,... | collective-permute-start | bytes 1572872 | tf_op jit(solution)/shard_map/ppermute | solution.py:27
  101.3 8.5 %collective-permute-done.19.refs_4_ = bf16[2048,128]{1,0:T(8,128)(2,1)S(1)} collective-permute-done((bf16[2048,128]{1,0:T(8,128)(2,1)S(1)}, bf16[2048,128]{1,0:T(8,128)(2,1)S(1)}, u32[]{:S(2)}, u32[]{:S(2)}) %collective-permute-start.19) | collective-permute-done | bytes 524320 | tf_op jit(solution)/shard_map/ppermute | solution.py:27
  109.8 2.7 %collective-permute-start.16 = (bf16[1024,128]{1,0:T(8,128)(2,1)S(1)}, bf16[1024,128]{1,0:T(8,128)(2,1)S(1)}, u32[]{:S(2)}, u32[]{:S(2)}) collective-permute-start(bf16[1024,128]{1,0:T(8,128)(2,1)S(1)} %slice.31), channel_id=1, source_target_pairs={{0,14},{1,15},{2,0},{3,1},{4,2},{5,3},{6,4},{7,5},{8,6},{9,7},{10,... | collective-permute-start | bytes 786440 | tf_op jit(solution)/shard_map/ppermute | solution.py:27
  112.6 8.4 %collective-permute-done.3.refs_2_ = bf16[2048,128]{1,0:T(8,128)(2,1)S(1)} collective-permute-done((bf16[2048,128]{1,0:T(8,128)(2,1)}, bf16[2048,128]{1,0:T(8,128)(2,1)S(1)}, u32[]{:S(2)}, u32[]{:S(2)}) %collective-permute-start.3) | collective-permute-done | bytes 524320 | tf_op jit(solution)/shard_map/ppermute | solution.py:27
  121.1 2.7 %collective-permute-start.24 = (bf16[1024,128]{1,0:T(8,128)(2,1)S(1)}, bf16[1024,128]{1,0:T(8,128)(2,1)S(1)}, u32[]{:S(2)}, u32[]{:S(2)}) collective-permute-start(bf16[1024,128]{1,0:T(8,128)(2,1)S(1)} %slice.33), channel_id=1, source_target_pairs={{0,14},{1,15},{2,0},{3,1},{4,2},{5,3},{6,4},{7,5},{8,6},{9,7},{10,... | collective-permute-start | bytes 786440 | tf_op jit(solution)/shard_map/ppermute | solution.py:27
  124.0 1.4 copy-done.1
  125.4 7.3 %shard_map.158 = (f32[384,2048]{1,0:T(8,128)S(1)}, f32[384,2048]{1,0:T(8,128)S(1)}) custom-call(bf16[384,2048]{1,0:T(8,128)(2,1)S(1)} %collective-permute-done.25.refs_0_, bf16[384,2048]{1,0:T(8,128)(2,1)S(1)} %bitcast.17, bf16[2048,128]{1,0:T(8,128)(2,1)} %collective-permute-done.1.refs_2_, bf16[2048,128]{1,0:T(8,128)(2,1)} %collective-permute-done.9.refs_3_, ...), custom_call_target="tpu_custom_call" | custom-call | flops 3623878656 | bytes 4718592 | tf_op jit(solution)/shard_map/pallas_call | solution.py:325
  132.8 2.9 %collective-permute-start.8 = (bf16[1024,128]{1,0:T(8,128)(2,1)S(1)}, bf16[1024,128]{1,0:T(8,128)(2,1)S(1)}, u32[]{:S(2)}, u32[]{:S(2)}) collective-permute-start(bf16[1024,128]{1,0:T(8,128)(2,1)S(1)} %slice.29), channel_id=1, source_target_pairs={{0,14},{1,15},{2,0},{3,1},{4,2},{5,3},{6,4},{7,5},{8,6},{9,7},{10,... | collective-permute-start | bytes 786440 | tf_op jit(solution)/shard_map/ppermute | solution.py:27
  135.7 4.1 %shard_map.159 = (f32[384,2048]{1,0:T(8,128)S(1)}, f32[384,2048]{1,0:T(8,128)S(1)}) custom-call(bf16[384,2048]{1,0:T(8,128)(2,1)S(1)} %collective-permute-done.25.refs_0_, bf16[384,2048]{1,0:T(8,128)(2,1)S(1)} %bitcast.18, bf16[2048,128]{1,0:T(8,128)(2,1)} %collective-permute-done.2.refs_2_, ...), custom_call_target="tpu_custom_call", output_to_operand_aliasing={{0}: (8, {}), {1}: (9, {})} | custom-call | flops 2415919104 | bytes 3145728 | tf_op jit(solution)/shard_map/pallas_call | solution.py:325
  139.9 3.1 %shard_map.160 = (f32[384,2048]{1,0:T(8,128)S(1)}, f32[384,2048]{1,0:T(8,128)S(1)}) custom-call(bf16[384,2048]{1,0:T(8,128)(2,1)S(1)} %collective-permute-done.25.refs_0_, bf16[384,2048]{1,0:T(8,128)(2,1)S(1)} %bitcast.19, bf16[2048,128]{1,0:T(8,128)(2,1)S(1)} %collective-permute-done.3.refs_2_, ...), custom_call_target="tpu_custom_call", output_to_operand_aliasing={{0}: (8, {}), {1}: (9, {})} | custom-call | flops 2415919104 | bytes 3145728 | tf_op jit(solution)/shard_map/pallas_call | solution.py:325
  143.1 3.0 %shard_map.162 = bf16[384,2048]{1,0:T(8,128)(2,1)} custom-call(bf16[384,2048]{1,0:T(8,128)(2,1)S(1)} %collective-permute-done.25.refs_0_, bf16[1024,128]{1,0:T(8,128)(2,1)S(1)} %collective-permute-done.4.refs_1_, bf16[1024,128]{1,0:T(8,128)(2,1)S(1)} %collective-permute-done.8.refs_2_, bf16[1024,128]{1,0:T(8,128)(2,1)S(1)} %collective-permute-done.12.refs_3_, ...), custom_call_target="tpu_custom_call" | custom-call | flops 603979776 | bytes 1572864 | tf_op jit(solution)/shard_map/pallas_call | solution.py:325
  146.1 7.4 %collective-permute-start.26 = (bf16[384,2048]{1,0:T(8,128)(2,1)}, bf16[384,2048]{1,0:T(8,128)(2,1)}, u32[]{:S(2)}, u32[]{:S(2)}) collective-permute-start(bf16[384,2048]{1,0:T(8,128)(2,1)} %shard_map.162), channel_id=1, source_target_pairs={{0,1},{1,0},{2,3},{3,2},{4,5},{5,4},{6,7},{7,6},{8,9},{9,8},{10,11... | collective-permute-start | bytes 4718600 | tf_op jit(solution)/shard_map/ppermute | solution.py:32
  153.5 0.7 slice.21
  154.3 3.5 %collective-permute-start = (bf16[64,128]{1,0:T(8,128)(2,1)S(1)}, bf16[64,128]{1,0:T(8,128)(2,1)S(1)}, u32[]{:S(2)}, u32[]{:S(2)}) collective-permute-start(bf16[64,128]{1,0:T(8,128)(2,1)S(1)} %slice.21), channel_id=1, source_target_pairs={{0,16},{16,32},{32,48},{48,64},{64,80},{80,96},{96,112},{112,128},... | collective-permute-start | bytes 49160 | tf_op jit(solution)/shard_map/ppermute | solution.py:22
  157.8 1.0 copy.24.fade_ref
  158.8 0.9 copy.23.taps_ref
  159.7 1.0 copy-done.19
  160.7 0.9 copy-done.23
  161.7 0.9 copy-done.24
  162.6 0.9 copy-done.30
  163.6 0.9 copy-done.31
  164.5 5.2 %local_scan.1 = (f32[64,2048]{1,0:T(8,128)S(1)}, f32[64,2048]{1,0:T(8,128)S(1)}, f32[8,64]{1,0:T(8,128)S(1)}) custom-call(s32[1]{0:T(128)} %bitcast.1._, bf16[64,2048]{1,0:T(8,128)(2,1)S(1)} %copy-done.24, bf16[64,128]{1,0:T(8,128)(2,1)S(1)} %collective-permute-done.halo_ref, bf16[1024,4]{1,0:T(8,128)(2,1)S(1)} %copy-done.23, ...), custom_call_target="tpu_custom_call" | custom-call | flops 4000000000 | bytes 2000000 | tf_op jit(solution)/shard_map/local_scan/pallas_call | solution.py:111
  169.8 0.8 copy-done.36
  170.6 0.8 copy-done.38
  172.1 6.2 %all-to-all-start = ((f32[16,1,512]{2,1,0:T(1,128)}), f32[16,1,512]{2,1,0:T(1,128)S(1)}, u32[]{:S(2)}, u32[]{:S(2)}) async-start(f32[16,1,512]{2,1,0:T(1,128)} %reshape.24), calls=%async_computation | async-start | bytes 65536 | tf_op jit(solution)/shard_map/all_to_all | solution.py:16
  178.3 6.4 %all-to-all-done = f32[16,1,512]{2,1,0:T(1,128)S(1)} async-done(((f32[16,1,512]{2,1,0:T(1,128)}), f32[16,1,512]{2,1,0:T(1,128)S(1)}, u32[]{:S(2)}, u32[]{:S(2)}) %all-to-all-start) | async-done | bytes 32800 | tf_op jit(solution)/shard_map/all_to_all | solution.py:16
  186.0 0.9 copy-done.32
  187.0 1.0 copy-done.37
  188.0 1.0 copy-done.39
  190.1 6.3 %all-to-all-start.1 = ((bf16[16,64,128]{2,1,0:T(8,128)(2,1)}), bf16[16,64,128]{2,1,0:T(8,128)(2,1)}, u32[]{:S(2)}, u32[]{:S(2)}) async-start(bf16[16,64,128]{2,1,0:T(8,128)(2,1)} %copy-done.22), calls=%async_computation.1 | async-start | bytes 524288 | tf_op jit(solution)/shard_map/all_to_all | solution.py:202
  196.3 1.4 copy-done.2
  197.7 0.9 copy-done.4
  198.7 0.9 copy-done.6
  199.6 0.9 copy-done.8
  200.6 0.9 copy-done.10
  201.5 0.9 copy-done.12
  202.5 2.0 shard_map.161
  204.5 3.1 %add_convert_fusion = bf16[384,2048]{1,0:T(8,128)(2,1)} fusion(f32[384,2048]{1,0:T(8,128)S(1)} %shard_map.161, bf16[384,2048]{1,0:T(8,128)(2,1)} %collective-permute-done.26), kind=kLoop, calls=%fused_computation | loop fusion | flops 2359296 | bytes 6291456 | tf_op jit(solution)/shard_map/convert_element_type | solution.py:393
  208.2 3.7 %all-to-all-start.3 = ((bf16[16,24,2048]{2,1,0:T(8,128)(2,1)}), bf16[16,24,2048]{2,1,0:T(8,128)(2,1)S(1)}, u32[]{:S(2)}, u32[]{:S(2)}) async-start(bf16[16,24,2048]{2,1,0:T(8,128)(2,1)} %bitcast.28), calls=%async_computation.3 | async-start | bytes 3145728 | tf_op jit(solution)/shard_map/all_to_all | solution.py:380
  211.9 3.9 %convolution_convert_fusion = bf16[128,2048]{1,0:T(8,128)(2,1)} fusion(bf16[1024,128]{1,0:T(8,128)(2,1)} %bitcast.4, bf16[1024,2048]{1,0:T(8,128)(2,1)} %param.22), kind=kOutput, calls=%fused_computation.1 | convolution fusion | flops 537133056 | bytes 4980736 | tf_op jit(solution)/shard_map/dot_general | solution.py:203
  215.8 23.1 %all-to-all-done.3 = bf16[16,24,2048]{2,1,0:T(8,128)(2,1)S(1)} async-done(((bf16[16,24,2048]{2,1,0:T(8,128)(2,1)}), bf16[16,24,2048]{2,1,0:T(8,128)(2,1)S(1)}, u32[]{:S(2)}, u32[]{:S(2)}) %all-to-all-start.3) | async-done | bytes 1572896 | tf_op jit(solution)/shard_map/all_to_all | solution.py:380
  238.9 1.8 weighted_sum.1
  (108 shorter events, 7.1 us)
Async XLA Ops:
  1.3 1.0 copy-start.25
  3.7 11.9 %copy-start.26 = (bf16[1,2048,128]{2,1,0:T(8,128)(2,1)S(1)}, bf16[1,2048,128]{2,1,0:T(8,128)(2,1)}, u32[]{:S(2)}) copy-start(bf16[1,2048,128]{2,1,0:T(8,128)(2,1)} %param.28) | copy-start | bytes 1572868
  6.4 48.2 %all-to-all-start.2 = ((bf16[16,24,2048]{2,1,0:T(8,128)(2,1)}), bf16[16,24,2048]{2,1,0:T(8,128)(2,1)S(1)}, u32[]{:S(2)}, u32[]{:S(2)}) async-start(bf16[16,24,2048]{2,1,0:T(8,128)(2,1)} %bitcast.7), calls=%async_computation.2 | async-start | bytes 3145728 | tf_op jit(solution)/shard_map/all_to_all | solution.py:380
  14.0 17.3 %collective-permute-start.1 = (bf16[2048,128]{1,0:T(8,128)(2,1)}, bf16[2048,128]{1,0:T(8,128)(2,1)}, u32[]{:S(2)}, u32[]{:S(2)}) collective-permute-start(bf16[2048,128]{1,0:T(8,128)(2,1)} %bitcast.9.refs_8_), channel_id=1, source_target_pairs={{0,2},{1,3},{2,4},{3,5},{4,6},{5,7},{6,8},{7,9},{8,10},{9,11},{10,... | collective-permute-start | bytes 1572872 | tf_op jit(solution)/shard_map/ppermute | solution.py:27
  15.7 26.8 %collective-permute-start.9 = (bf16[2048,128]{1,0:T(8,128)(2,1)S(1)}, bf16[2048,128]{1,0:T(8,128)(2,1)}, u32[]{:S(2)}, u32[]{:S(2)}) collective-permute-start(bf16[2048,128]{1,0:T(8,128)(2,1)S(1)} %bitcast.22), channel_id=1, source_target_pairs={{0,2},{1,3},{2,4},{3,5},{4,6},{5,7},{6,8},{7,9},{8,10},{9,11},{10,... | collective-permute-start | bytes 1572872 | tf_op jit(solution)/shard_map/ppermute | solution.py:27
  17.3 25.2 %collective-permute-start.13 = (bf16[2048,128]{1,0:T(8,128)(2,1)S(1)}, bf16[2048,128]{1,0:T(8,128)(2,1)}, u32[]{:S(2)}, u32[]{:S(2)}) collective-permute-start(bf16[2048,128]{1,0:T(8,128)(2,1)S(1)} %bitcast.23), channel_id=1, source_target_pairs={{0,14},{1,15},{2,0},{3,1},{4,2},{5,3},{6,4},{7,5},{8,6},{9,7},{10,... | collective-permute-start | bytes 1572872 | tf_op jit(solution)/shard_map/ppermute | solution.py:27
  19.8 33.9 %collective-permute-start.17 = (bf16[2048,128]{1,0:T(8,128)(2,1)}, bf16[2048,128]{1,0:T(8,128)(2,1)}, u32[]{:S(2)}, u32[]{:S(2)}) collective-permute-start(bf16[2048,128]{1,0:T(8,128)(2,1)} %bitcast.11.refs_10_), channel_id=1, source_target_pairs={{0,2},{1,3},{2,4},{3,5},{4,6},{5,7},{6,8},{7,9},{8,10},{9,11},{10,... | collective-permute-start | bytes 1572872 | tf_op jit(solution)/shard_map/ppermute | solution.py:27
  19.8 33.9 %collective-permute-start.21 = (bf16[2048,128]{1,0:T(8,128)(2,1)}, bf16[2048,128]{1,0:T(8,128)(2,1)S(1)}, u32[]{:S(2)}, u32[]{:S(2)}) collective-permute-start(bf16[2048,128]{1,0:T(8,128)(2,1)} %bitcast.11.refs_10_), channel_id=1, source_target_pairs={{0,14},{1,15},{2,0},{3,1},{4,2},{5,3},{6,4},{7,5},{8,6},{9,7},{10,... | collective-permute-start | bytes 1572872 | tf_op jit(solution)/shard_map/ppermute | solution.py:27
  31.3 23.3 %collective-permute-start.5 = (bf16[2048,128]{1,0:T(8,128)(2,1)}, bf16[2048,128]{1,0:T(8,128)(2,1)}, u32[]{:S(2)}, u32[]{:S(2)}) collective-permute-start(bf16[2048,128]{1,0:T(8,128)(2,1)} %bitcast.9.refs_8_), channel_id=1, source_target_pairs={{0,14},{1,15},{2,0},{3,1},{4,2},{5,3},{6,4},{7,5},{8,6},{9,7},{10,... | collective-permute-start | bytes 1572872 | tf_op jit(solution)/shard_map/ppermute | solution.py:27
  42.5 22.4 %collective-permute-start.10 = (bf16[2048,128]{1,0:T(8,128)(2,1)}, bf16[2048,128]{1,0:T(8,128)(2,1)S(1)}, u32[]{:S(2)}, u32[]{:S(2)}) collective-permute-start(bf16[2048,128]{1,0:T(8,128)(2,1)} %collective-permute-done.9.refs_3_), channel_id=1, source_target_pairs={{0,2},{1,3},{2,4},{3,5},{4,6},{5,7},{6,8},{7,9},{8,10},{9,11},{10,... | collective-permute-start | bytes 1572872 | tf_op jit(solution)/shard_map/ppermute | solution.py:27
  42.5 23.5 %collective-permute-start.14 = (bf16[2048,128]{1,0:T(8,128)(2,1)}, bf16[2048,128]{1,0:T(8,128)(2,1)S(1)}, u32[]{:S(2)}, u32[]{:S(2)}) collective-permute-start(bf16[2048,128]{1,0:T(8,128)(2,1)} %collective-permute-done.13.refs_6_), channel_id=1, source_target_pairs={{0,14},{1,15},{2,0},{3,1},{4,2},{5,3},{6,4},{7,5},{8,6},{9,7},{10,... | collective-permute-start | bytes 1572872 | tf_op jit(solution)/shard_map/ppermute | solution.py:27
  53.7 22.4 %collective-permute-start.18 = (bf16[2048,128]{1,0:T(8,128)(2,1)}, bf16[2048,128]{1,0:T(8,128)(2,1)S(1)}, u32[]{:S(2)}, u32[]{:S(2)}) collective-permute-start(bf16[2048,128]{1,0:T(8,128)(2,1)} %collective-permute-done.17.refs_4_), channel_id=1, source_target_pairs={{0,2},{1,3},{2,4},{3,5},{4,6},{5,7},{6,8},{7,9},{8,10},{9,11},{10,... | collective-permute-start | bytes 1572872 | tf_op jit(solution)/shard_map/ppermute | solution.py:27
  53.8 33.7 %collective-permute-start.2 = (bf16[2048,128]{1,0:T(8,128)(2,1)}, bf16[2048,128]{1,0:T(8,128)(2,1)}, u32[]{:S(2)}, u32[]{:S(2)}) collective-permute-start(bf16[2048,128]{1,0:T(8,128)(2,1)} %collective-permute-done.1.refs_2_), channel_id=1, source_target_pairs={{0,2},{1,3},{2,4},{3,5},{4,6},{5,7},{6,8},{7,9},{8,10},{9,11},{10,... | collective-permute-start | bytes 1572872 | tf_op jit(solution)/shard_map/ppermute | solution.py:27
  54.5 69.3 %copy-start = (bf16[16,24,2048]{2,1,0:T(8,128)(2,1)}, bf16[16,24,2048]{2,1,0:T(8,128)(2,1)S(1)}, u32[]{:S(2)}) copy-start(bf16[16,24,2048]{2,1,0:T(8,128)(2,1)S(1)} %all-to-all-done.2) | copy-start | bytes 4718596
  54.6 69.4 %copy-start.27 = (bf16[1,2048,128]{2,1,0:T(8,128)(2,1)S(1)}, bf16[1,2048,128]{2,1,0:T(8,128)(2,1)}, u32[]{:S(2)}) copy-start(bf16[1,2048,128]{2,1,0:T(8,128)(2,1)} %param.28) | copy-start | bytes 1572868
  54.6 69.4 %copy-start.29 = (bf16[2048,128]{1,0:T(8,128)(2,1)S(1)}, bf16[2048,128]{1,0:T(8,128)(2,1)}, u32[]{:S(2)}) copy-start(bf16[2048,128]{1,0:T(8,128)(2,1)} %copy-done.28) | copy-start | bytes 1572868
  54.6 69.3 %collective-permute-start.25 = (bf16[384,2048]{1,0:T(8,128)(2,1)S(1)}, bf16[384,2048]{1,0:T(8,128)(2,1)S(1)}, u32[]{:S(2)}, u32[]{:S(2)}) collective-permute-start(bf16[384,2048]{1,0:T(8,128)(2,1)S(1)} %bitcast.16), channel_id=1, source_target_pairs={{0,1},{1,0},{2,3},{3,2},{4,5},{5,4},{6,7},{7,6},{8,9},{9,8},{10,11... | collective-permute-start | bytes 4718600 | tf_op jit(solution)/shard_map/ppermute | solution.py:32
  64.9 59.0 %copy-start.13 = (bf16[2048,128]{1,0:T(8,128)(2,1)}, bf16[2048,128]{1,0:T(8,128)(2,1)S(1)}, u32[]{:S(2)}) copy-start(bf16[2048,128]{1,0:T(8,128)(2,1)S(1)} %collective-permute-done.10.refs_3_) | copy-start | bytes 1572868
  64.9 23.8 %collective-permute-start.22 = (bf16[2048,128]{1,0:T(8,128)(2,1)}, bf16[2048,128]{1,0:T(8,128)(2,1)S(1)}, u32[]{:S(2)}, u32[]{:S(2)}) collective-permute-start(bf16[2048,128]{1,0:T(8,128)(2,1)} %copy-done.28), channel_id=1, source_target_pairs={{0,14},{1,15},{2,0},{3,1},{4,2},{5,3},{6,4},{7,5},{8,6},{9,7},{10,... | collective-permute-start | bytes 1572872 | tf_op jit(solution)/shard_map/ppermute | solution.py:27
  66.1 57.8 %copy-start.15 = (bf16[2048,128]{1,0:T(8,128)(2,1)}, bf16[2048,128]{1,0:T(8,128)(2,1)S(1)}, u32[]{:S(2)}) copy-start(bf16[2048,128]{1,0:T(8,128)(2,1)S(1)} %collective-permute-done.14.refs_6_) | copy-start | bytes 1572868
  66.1 22.9 %collective-permute-start.6 = (bf16[2048,128]{1,0:T(8,128)(2,1)}, bf16[2048,128]{1,0:T(8,128)(2,1)S(1)}, u32[]{:S(2)}, u32[]{:S(2)}) collective-permute-start(bf16[2048,128]{1,0:T(8,128)(2,1)} %collective-permute-done.5.refs_5_), channel_id=1, source_target_pairs={{0,14},{1,15},{2,0},{3,1},{4,2},{5,3},{6,4},{7,5},{8,6},{9,7},{10,... | collective-permute-start | bytes 1572872 | tf_op jit(solution)/shard_map/ppermute | solution.py:27
  76.1 47.8 %copy-start.17 = (bf16[2048,128]{1,0:T(8,128)(2,1)}, bf16[2048,128]{1,0:T(8,128)(2,1)S(1)}, u32[]{:S(2)}) copy-start(bf16[2048,128]{1,0:T(8,128)(2,1)S(1)} %collective-permute-done.18.refs_4_) | copy-start | bytes 1572868
  76.1 22.5 %collective-permute-start.11 = (bf16[2048,128]{1,0:T(8,128)(2,1)S(1)}, bf16[2048,128]{1,0:T(8,128)(2,1)S(1)}, u32[]{:S(2)}, u32[]{:S(2)}) collective-permute-start(bf16[2048,128]{1,0:T(8,128)(2,1)S(1)} %collective-permute-done.10.refs_3_), channel_id=1, source_target_pairs={{0,2},{1,3},{2,4},{3,5},{4,6},{5,7},{6,8},{7,9},{8,10},{9,11},{10,... | collective-permute-start | bytes 1572872 | tf_op jit(solution)/shard_map/ppermute | solution.py:27
  87.4 11.1 %collective-permute-start.15 = (bf16[2048,128]{1,0:T(8,128)(2,1)S(1)}, bf16[2048,128]{1,0:T(8,128)(2,1)S(1)}, u32[]{:S(2)}, u32[]{:S(2)}) collective-permute-start(bf16[2048,128]{1,0:T(8,128)(2,1)S(1)} %collective-permute-done.14.refs_6_), channel_id=1, source_target_pairs={{0,14},{1,15},{2,0},{3,1},{4,2},{5,3},{6,4},{7,5},{8,6},{9,7},{10,... | collective-permute-start | bytes 1572872 | tf_op jit(solution)/shard_map/ppermute | solution.py:27
  88.6 21.2 %collective-permute-start.19 = (bf16[2048,128]{1,0:T(8,128)(2,1)S(1)}, bf16[2048,128]{1,0:T(8,128)(2,1)S(1)}, u32[]{:S(2)}, u32[]{:S(2)}) collective-permute-start(bf16[2048,128]{1,0:T(8,128)(2,1)S(1)} %collective-permute-done.18.refs_4_), channel_id=1, source_target_pairs={{0,2},{1,3},{2,4},{3,5},{4,6},{5,7},{6,8},{7,9},{8,10},{9,11},{10,... | collective-permute-start | bytes 1572872 | tf_op jit(solution)/shard_map/ppermute | solution.py:27
  88.9 20.9 %collective-permute-start.23 = (bf16[2048,128]{1,0:T(8,128)(2,1)S(1)}, bf16[2048,128]{1,0:T(8,128)(2,1)S(1)}, u32[]{:S(2)}, u32[]{:S(2)}) collective-permute-start(bf16[2048,128]{1,0:T(8,128)(2,1)S(1)} %collective-permute-done.22.refs_7_), channel_id=1, source_target_pairs={{0,14},{1,15},{2,0},{3,1},{4,2},{5,3},{6,4},{7,5},{8,6},{9,7},{10,... | collective-permute-start | bytes 1572872 | tf_op jit(solution)/shard_map/ppermute | solution.py:27
  98.6 22.5 %collective-permute-start.3 = (bf16[2048,128]{1,0:T(8,128)(2,1)}, bf16[2048,128]{1,0:T(8,128)(2,1)S(1)}, u32[]{:S(2)}, u32[]{:S(2)}) collective-permute-start(bf16[2048,128]{1,0:T(8,128)(2,1)} %collective-permute-done.2.refs_2_), channel_id=1, source_target_pairs={{0,2},{1,3},{2,4},{3,5},{4,6},{5,7},{6,8},{7,9},{8,10},{9,11},{10,... | collective-permute-start | bytes 1572872 | tf_op jit(solution)/shard_map/ppermute | solution.py:27
  98.6 22.5 %collective-permute-start.7 = (bf16[2048,128]{1,0:T(8,128)(2,1)S(1)}, bf16[2048,128]{1,0:T(8,128)(2,1)S(1)}, u32[]{:S(2)}, u32[]{:S(2)}) collective-permute-start(bf16[2048,128]{1,0:T(8,128)(2,1)S(1)} %collective-permute-done.6.refs_5_), channel_id=1, source_target_pairs={{0,14},{1,15},{2,0},{3,1},{4,2},{5,3},{6,4},{7,5},{8,6},{9,7},{10,... | collective-permute-start | bytes 1572872 | tf_op jit(solution)/shard_map/ppermute | solution.py:27
  109.8 22.9 %collective-permute-start.12 = (bf16[1024,128]{1,0:T(8,128)(2,1)S(1)}, bf16[1024,128]{1,0:T(8,128)(2,1)S(1)}, u32[]{:S(2)}, u32[]{:S(2)}) collective-permute-start(bf16[1024,128]{1,0:T(8,128)(2,1)S(1)} %slice.30), channel_id=1, source_target_pairs={{0,2},{1,3},{2,4},{3,5},{4,6},{5,7},{6,8},{7,9},{8,10},{9,11},{10,... | collective-permute-start | bytes 786440 | tf_op jit(solution)/shard_map/ppermute | solution.py:27
  109.8 33.1 %collective-permute-start.16 = (bf16[1024,128]{1,0:T(8,128)(2,1)S(1)}, bf16[1024,128]{1,0:T(8,128)(2,1)S(1)}, u32[]{:S(2)}, u32[]{:S(2)}) collective-permute-start(bf16[1024,128]{1,0:T(8,128)(2,1)S(1)} %slice.31), channel_id=1, source_target_pairs={{0,14},{1,15},{2,0},{3,1},{4,2},{5,3},{6,4},{7,5},{8,6},{9,7},{10,... | collective-permute-start | bytes 786440 | tf_op jit(solution)/shard_map/ppermute | solution.py:27
  121.0 21.9 %collective-permute-start.20 = (bf16[1024,128]{1,0:T(8,128)(2,1)S(1)}, bf16[1024,128]{1,0:T(8,128)(2,1)S(1)}, u32[]{:S(2)}, u32[]{:S(2)}) collective-permute-start(bf16[1024,128]{1,0:T(8,128)(2,1)S(1)} %slice.32), channel_id=1, source_target_pairs={{0,2},{1,3},{2,4},{3,5},{4,6},{5,7},{6,8},{7,9},{8,10},{9,11},{10,... | collective-permute-start | bytes 786440 | tf_op jit(solution)/shard_map/ppermute | solution.py:27
  121.1 21.9 %collective-permute-start.24 = (bf16[1024,128]{1,0:T(8,128)(2,1)S(1)}, bf16[1024,128]{1,0:T(8,128)(2,1)S(1)}, u32[]{:S(2)}, u32[]{:S(2)}) collective-permute-start(bf16[1024,128]{1,0:T(8,128)(2,1)S(1)} %slice.33), channel_id=1, source_target_pairs={{0,14},{1,15},{2,0},{3,1},{4,2},{5,3},{6,4},{7,5},{8,6},{9,7},{10,... | collective-permute-start | bytes 786440 | tf_op jit(solution)/shard_map/ppermute | solution.py:27
  123.9 19.1 %collective-permute-start.4 = (bf16[1024,128]{1,0:T(8,128)(2,1)S(1)}, bf16[1024,128]{1,0:T(8,128)(2,1)S(1)}, u32[]{:S(2)}, u32[]{:S(2)}) collective-permute-start(bf16[1024,128]{1,0:T(8,128)(2,1)S(1)} %slice.28), channel_id=1, source_target_pairs={{0,2},{1,3},{2,4},{3,5},{4,6},{5,7},{6,8},{7,9},{8,10},{9,11},{10,... | collective-permute-start | bytes 786440 | tf_op jit(solution)/shard_map/ppermute | solution.py:27
  124.0 1.4 copy-start.1
  125.4 10.3 %copy-start.14 = (bf16[2048,128]{1,0:T(8,128)(2,1)S(1)}, bf16[2048,128]{1,0:T(8,128)(2,1)}, u32[]{:S(2)}) copy-start(bf16[2048,128]{1,0:T(8,128)(2,1)} %copy-done.13) | copy-start | bytes 1572868
  125.4 10.3 %copy-start.16 = (bf16[2048,128]{1,0:T(8,128)(2,1)S(1)}, bf16[2048,128]{1,0:T(8,128)(2,1)}, u32[]{:S(2)}) copy-start(bf16[2048,128]{1,0:T(8,128)(2,1)} %copy-done.15) | copy-start | bytes 1572868
  125.4 10.3 %copy-start.18 = (bf16[2048,128]{1,0:T(8,128)(2,1)S(1)}, bf16[2048,128]{1,0:T(8,128)(2,1)}, u32[]{:S(2)}) copy-start(bf16[2048,128]{1,0:T(8,128)(2,1)} %copy-done.17) | copy-start | bytes 1572868
  132.8 10.3 %collective-permute-start.8 = (bf16[1024,128]{1,0:T(8,128)(2,1)S(1)}, bf16[1024,128]{1,0:T(8,128)(2,1)S(1)}, u32[]{:S(2)}, u32[]{:S(2)}) collective-permute-start(bf16[1024,128]{1,0:T(8,128)(2,1)S(1)} %slice.29), channel_id=1, source_target_pairs={{0,14},{1,15},{2,0},{3,1},{4,2},{5,3},{6,4},{7,5},{8,6},{9,7},{10,... | collective-permute-start | bytes 786440 | tf_op jit(solution)/shard_map/ppermute | solution.py:27
  143.0 3.1 %copy-start.3 = (bf16[1024,128]{1,0:T(8,128)(2,1)}, bf16[1024,128]{1,0:T(8,128)(2,1)S(1)}, u32[]{:S(2)}) copy-start(bf16[1024,128]{1,0:T(8,128)(2,1)S(1)} %collective-permute-done.16.refs_4_) | copy-start | bytes 786436
  143.0 3.1 %copy-start.5 = (bf16[1024,128]{1,0:T(8,128)(2,1)}, bf16[1024,128]{1,0:T(8,128)(2,1)S(1)}, u32[]{:S(2)}) copy-start(bf16[1024,128]{1,0:T(8,128)(2,1)S(1)} %collective-permute-done.20.refs_5_) | copy-start | bytes 786436
  143.0 3.1 %copy-start.7 = (bf16[1024,128]{1,0:T(8,128)(2,1)}, bf16[1024,128]{1,0:T(8,128)(2,1)S(1)}, u32[]{:S(2)}) copy-start(bf16[1024,128]{1,0:T(8,128)(2,1)S(1)} %collective-permute-done.24.refs_6_) | copy-start | bytes 786436
  143.0 3.1 %copy-start.9 = (bf16[1024,128]{1,0:T(8,128)(2,1)}, bf16[1024,128]{1,0:T(8,128)(2,1)S(1)}, u32[]{:S(2)}) copy-start(bf16[1024,128]{1,0:T(8,128)(2,1)S(1)} %collective-permute-done.4.refs_1_) | copy-start | bytes 786436
  143.1 3.1 %copy-start.11 = (bf16[1024,128]{1,0:T(8,128)(2,1)}, bf16[1024,128]{1,0:T(8,128)(2,1)S(1)}, u32[]{:S(2)}) copy-start(bf16[1024,128]{1,0:T(8,128)(2,1)S(1)} %collective-permute-done.8.refs_2_) | copy-start | bytes 786436
  143.1 14.7 %copy-start.41 = (f32[1024]{0:T(1024)S(1)}, f32[1024]{0:T(1024)}, u32[]{:S(2)}) copy-start(f32[1024]{0:T(1024)} %param.20) | copy-start | bytes 12292
  143.1 15.7 %copy-start.40 = (bf16[1024,4]{0,1:T(4,128)(2,1)S(1)}, bf16[1024,4]{0,1:T(4,128)(2,1)}, u32[]{:S(2)}) copy-start(bf16[1024,4]{0,1:T(4,128)(2,1)} %param.17) | copy-start | bytes 24580
  143.1 16.6 %copy-start.33 = (f32[2048]{0:T(1024)S(1)}, f32[2048]{0:T(1024)}, u32[]{:S(2)}) copy-start(f32[2048]{0:T(1024)} %param.21) | copy-start | bytes 24580
  146.1 58.3 %collective-permute-start.26 = (bf16[384,2048]{1,0:T(8,128)(2,1)}, bf16[384,2048]{1,0:T(8,128)(2,1)}, u32[]{:S(2)}, u32[]{:S(2)}) collective-permute-start(bf16[384,2048]{1,0:T(8,128)(2,1)} %shard_map.162), channel_id=1, source_target_pairs={{0,1},{1,0},{2,3},{3,2},{4,5},{5,4},{6,7},{7,6},{8,9},{9,8},{10,11... | collective-permute-start | bytes 4718600 | tf_op jit(solution)/shard_map/ppermute | solution.py:32
  154.3 5.4 %collective-permute-start = (bf16[64,128]{1,0:T(8,128)(2,1)S(1)}, bf16[64,128]{1,0:T(8,128)(2,1)S(1)}, u32[]{:S(2)}, u32[]{:S(2)}) collective-permute-start(bf16[64,128]{1,0:T(8,128)(2,1)S(1)} %slice.21), channel_id=1, source_target_pairs={{0,16},{16,32},{32,48},{48,64},{64,80},{80,96},{96,112},{112,128},... | collective-permute-start | bytes 49160 | tf_op jit(solution)/shard_map/ppermute | solution.py:22
  159.7 1.0 copy-start.19
  160.7 0.9 copy-start.23
  161.7 0.9 copy-start.24
  162.6 0.9 copy-start.30
  163.6 0.9 copy-start.31
  172.1 12.6 %all-to-all-start = ((f32[16,1,512]{2,1,0:T(1,128)}), f32[16,1,512]{2,1,0:T(1,128)S(1)}, u32[]{:S(2)}, u32[]{:S(2)}) async-start(f32[16,1,512]{2,1,0:T(1,128)} %reshape.24), calls=%async_computation | async-start | bytes 65536 | tf_op jit(solution)/shard_map/all_to_all | solution.py:16
  186.0 1.0 copy-start.32
  187.0 1.0 copy-start.37
  188.0 1.0 copy-start.39
  190.1 18.1 %all-to-all-start.1 = ((bf16[16,64,128]{2,1,0:T(8,128)(2,1)}), bf16[16,64,128]{2,1,0:T(8,128)(2,1)}, u32[]{:S(2)}, u32[]{:S(2)}) async-start(bf16[16,64,128]{2,1,0:T(8,128)(2,1)} %copy-done.22), calls=%async_computation.1 | async-start | bytes 524288 | tf_op jit(solution)/shard_map/all_to_all | solution.py:202
  196.3 1.4 copy-start.2
  197.7 0.9 copy-start.4
  198.7 0.9 copy-start.6
  199.6 0.9 copy-start.8
  208.2 30.7 %all-to-all-start.3 = ((bf16[16,24,2048]{2,1,0:T(8,128)(2,1)}), bf16[16,24,2048]{2,1,0:T(8,128)(2,1)S(1)}, u32[]{:S(2)}, u32[]{:S(2)}) async-start(bf16[16,24,2048]{2,1,0:T(8,128)(2,1)} %bitcast.28), calls=%async_computation.3 | async-start | bytes 3145728 | tf_op jit(solution)/shard_map/all_to_all | solution.py:380
  211.9 27.0 %copy-start.21 = (bf16[3,128,384]{2,1,0:T(8,128)(2,1)S(1)}, bf16[3,128,384]{2,1,0:T(8,128)(2,1)}, u32[]{:S(2)}) copy-start(bf16[3,128,384]{2,1,0:T(8,128)(2,1)} %copy-done.20) | copy-start | bytes 884740
  (9 other events, 7.1 us)

commit v2 on v1

--- a/solution.py
+++ b/solution.py
@@ -9,11 +9,11 @@
 LANES = 128
 TILES_AT_ONCE = 4
 CUT = 512
-
-
-def from_everyone(x, axis):
-    copies = jnp.broadcast_to(x, (lax.axis_size(axis), *x.shape))
-    return lax.all_to_all(copies, axis, split_axis=0, concat_axis=0, tiled=True)
+STEP_MIB = 12
+
+
+def swapped(x, axis):
+    return lax.all_to_all(x, axis, split_axis=0, concat_axis=0, tiled=True)
 
 
 def from_behind(x, axis, by):
@@ -24,7 +24,7 @@
 
 def along_z(x, by):
     tp = lax.axis_size("tp")
-    return lax.ppermute(x, "tp", [(i, (i + 2 * by) % tp) for i in range(tp)])
+    return lax.ppermute(x, "tp", [(i, (i + (2 * by if i % 2 == 0 else -2 * by)) % tp) for i in range(tp)])
 
 
 def other_core(x):
@@ -38,6 +38,10 @@
 
 def times_t(a, b):
     return lax.dot_general(a, b, (((1,), (1,)), ((), ())), preferred_element_type=jnp.float32)
+
+
+def far(x):
+    return pltpu.with_memory_space_constraint(x, pltpu.HBM)
 
 
 def cost(flops, moved):
@@ -51,16 +55,25 @@
     return jnp.where(v > -0.5, -v * series, 1.0 - exp_v)
 
 
-def local_scan(x, halo, taps, rate_map, entry_map, fade, spike, group):
+def local_scan(x, halo, taps, rate_map, entry_map, fade, spike, group, blocks):
     channels, positions = x.shape
     block = rate_map.shape[1]
 
-    def body(_, x_ref, halo_ref, taps_ref, rate_ref, entry_ref, fade_ref, spike_ref, decay_ref, state_ref, total_ref, map_ref):
+    def body(group_ref, x_ref, halo_ref, taps_ref, rate_ref, entry_ref, fade_ref, spike_ref, decay_ref, state_ref, total_ref, map_ref):
         map_ref[:block] = rate_ref[0].astype(jnp.float32).T.astype(jnp.bfloat16)
         map_ref[block:] = entry_ref[0].astype(jnp.float32).T.astype(jnp.bfloat16)
         lane = lax.broadcasted_iota(jnp.int32, (channels, LANES), 1)
-        tap = [taps_ref[:, k : k + 1].astype(jnp.float32) for k in range(4)]
-        speed = -8.0 * fade_ref[...]
+        group = group_ref[0]
+        per_row = LANES // channels
+
+        def column(row):
+            row = jnp.where(group % per_row == 0, row, pltpu.roll(row, LANES - channels, 1))
+            return jnp.broadcast_to(row, (LANES, LANES)).T[:channels]
+
+        at = pl.ds(pl.multiple_of(group // per_row * LANES, LANES), LANES)
+        here = taps_ref[:, at].astype(jnp.float32)
+        tap = [column(here[k : k + 1]) for k in range(4)]
+        speed = -8.0 * column(fade_ref[pl.ds(group // per_row, 1), :])
 
         def rolled(a):
             return [pltpu.roll(a, s, 1) for s in (1, 2, 3)]
@@ -105,7 +118,8 @@
         first = (one, jnp.zeros_like(one), *rolled(halo_ref[...].astype(jnp.float32)))
         last = lax.fori_loop(0, positions // (LANES * TILES_AT_ONCE), steps, first)
         ends = jnp.where(lane == 0, last[0], jnp.where(lane == 1, last[1], 0.0))
-        total_ref[...] = ends.T[:8]
+        ends = jnp.concatenate([ends, jnp.zeros_like(ends)], axis=0).T[:8]
+        total_ref[...] = jnp.broadcast_to(ends, total_ref.shape)
 
     whole = lambda *shape: pl.BlockSpec(shape, lambda i, g: (0,) * len(shape))
     return pl.pallas_call(
@@ -116,28 +130,28 @@
             in_specs=[
                 whole(channels, positions),
                 whole(channels, LANES),
-                pl.BlockSpec((channels, 4), lambda i, g: (g[0], 0)),
+                whole(*taps.shape),
                 pl.BlockSpec((1, block, block), lambda i, g: (g[0], 0, 0)),
                 pl.BlockSpec((1, block, block), lambda i, g: (g[0], 0, 0)),
-                pl.BlockSpec((channels, 1), lambda i, g: (g[0], 0)),
+                whole(*fade.shape),
                 whole(1, positions),
             ],
             out_specs=[
                 whole(channels, positions),
                 whole(channels, positions),
-                whole(8, channels),
+                whole(blocks, 8, LANES),
             ],
             scratch_shapes=[pltpu.VMEM((2 * block, block), jnp.bfloat16)],
         ),
         out_shape=[
             jax.ShapeDtypeStruct((channels, positions), jnp.float32),
             jax.ShapeDtypeStruct((channels, positions), jnp.float32),
-            jax.ShapeDtypeStruct((8, channels), jnp.float32),
+            jax.ShapeDtypeStruct((blocks, 8, LANES), jnp.float32),
         ],
         cost_estimate=cost(4 * 10**9, 2 * 10**6),
         compiler_params=pltpu.CompilerParams(vmem_limit_bytes=12 * 2**20),
         name="local_scan",
-    )(group, x, halo, taps, rate_map, entry_map, fade, spike)
+    )(group, far(x), halo, far(taps), far(rate_map), far(entry_map), far(fade), far(spike))
 
 
 def gated_states(decay, state, switch, totals, place, pieces):
@@ -145,13 +159,13 @@
     width = positions // pieces
 
     def body(place_ref, decay_ref, state_ref, switch_ref, totals_ref, out_ref):
-        entering = jnp.zeros((1, channels), jnp.float32)
+        entering = jnp.zeros((1, LANES), jnp.float32)
         for b in range(totals.shape[0]):
             passed = b < place_ref[0]
             entering = jnp.where(
                 passed, totals_ref[b, 0:1] * entering + totals_ref[b, 1:2], entering
             )
-        entering = jnp.broadcast_to(entering, (LANES, channels)).T
+        entering = jnp.broadcast_to(entering, (LANES, LANES)).T[:channels]
         for p in range(pieces):
             at = slice(p * width, (p + 1) * width)
             whole = state_ref[:, at] + decay_ref[:, at] * entering
@@ -167,7 +181,7 @@
         cost_estimate=cost(10**9, 2 * 10**6),
         compiler_params=pltpu.CompilerParams(vmem_limit_bytes=12 * 2**20),
         name="gated_states",
-    )(place, decay, state, switch, totals)
+    )(place, decay, state, far(switch), totals)
 
 
 def mixer_half(
@@ -184,18 +198,19 @@
     decay, state, total = local_scan(
         scan_source_values,
         halo,
-        causal_filter_coefficients,
+        causal_filter_coefficients.T,
         scan_switch_blockmap,
         entry_switch_blockmap,
-        feature_fading_speeds[:, None],
+        feature_fading_speeds.reshape(-1, LANES),
         spike_amount[None, :],
         lax.axis_index("tp").astype(jnp.int32)[None],
+        lax.axis_size("ep"),
     )
     pieces = gated_states(
         decay,
         state,
         switch_path_values,
-        from_everyone(total, "ep"),
+        swapped(total, "ep"),
         lax.axis_index("ep").astype(jnp.int32)[None],
         lax.axis_size("tp"),
     )
@@ -247,7 +262,7 @@
         cost_estimate=cost(10**9, 2 * 10**6),
         compiler_params=pltpu.CompilerParams(vmem_limit_bytes=12 * 2**20),
         name="token_rows",
-    )(activity, gain, ids, share)
+    )(far(activity), gain, far(ids), far(share))
 
 
 def weighted_sum(back, results):
@@ -279,27 +294,19 @@
     return ((up_cut + 1.0) * gate_cut * jax.nn.sigmoid(1.702 * gate_cut)).astype(jnp.bfloat16)
 
 
-def expert_step(rows, shards, so_far, dtype):
+def expert_step(rows, shards, so_far):
     sets, count, width = len(rows), *rows[0].shape
-    placed = pltpu.VMEM if dtype == jnp.float32 else jax.ShapeDtypeStruct
-    hidden = shards[0][0][0].shape[1]
-    operands, layout = [], []
-    for shard in shards:
-        layout.append([])
-        for pieces in shard:
-            layout[-1].append((len(operands), len(pieces)))
-            operands += pieces
+    hidden = shards[0][0].shape[1]
+    operands = [a for shard in shards for a in shard]
+    layout = [(3 * k, 3 * k + 1, 3 * k + 2) for k in range(len(shards))]
 
     def body(*refs):
         row_refs, weights = refs[:sets], refs[sets : sets + len(operands)]
         refs = refs[sets + len(operands) :]
         old, new = (refs[:sets], refs[sets:]) if so_far else ((), refs)
 
-        def load(at):
-            return jnp.concatenate([weights[at[0] + k][...] for k in range(at[1])], axis=0)
-
         def side_by_side(ats):
-            return jnp.concatenate([load(at) for at in ats], axis=1)
+            return jnp.concatenate([weights[at][...] for at in ats], axis=1)
 
         for k in range(sets):
             first = 0
@@ -318,37 +325,90 @@
                     added = times_t(units, down[at : at + CUT])
                     if base:
                         added = base[k][:, at : at + CUT] + added
-                    new[k][:, at : at + CUT] = added.astype(dtype)
+                    new[k][:, at : at + CUT] = added
                 first += 2
 
-    alias = {sets + len(operands) + k: k for k in range(sets)} if so_far and dtype == jnp.float32 else {}
+    alias = {sets + len(operands) + k: k for k in range(sets)} if so_far else {}
     return pl.pallas_call(
         body,
         in_specs=[pl.BlockSpec(memory_space=pltpu.VMEM)] * (sets + len(operands) + len(so_far)),
         out_specs=[pl.BlockSpec(memory_space=pltpu.VMEM)] * sets,
-        out_shape=[placed((count, width), dtype)] * sets,
+        out_shape=[pltpu.VMEM((count, width), jnp.float32)] * sets,
         input_output_aliases=alias,
         cost_estimate=cost(
             2 * sets * count * 3 * width * hidden * len(shards), 6 * width * hidden * len(shards)
         ),
-        compiler_params=pltpu.CompilerParams(vmem_limit_bytes=24 * 2**20),
-    )(*map(near, rows), *operands, *map(near, so_far))
+        compiler_params=pltpu.CompilerParams(vmem_limit_bytes=STEP_MIB * 2**20),
+    )(*map(far, rows), *operands, *map(near, so_far))
+
+
+def last_units(rows, gate, up):
+    count, width = rows[0].shape
+    hidden = gate.shape[1]
+
+    def body(*refs):
+        both = jnp.concatenate([refs[2][...], refs[3][...]], axis=1)
+        for k in range(2):
+            pre = times(refs[k][...], both)
+            refs[4 + k][...] = gated(pre[:, :hidden], pre[:, hidden:])
+
+    return pl.pallas_call(
+        body,
+        in_specs=[pl.BlockSpec(memory_space=pltpu.VMEM)] * 4,
+        out_specs=[pl.BlockSpec(memory_space=pltpu.VMEM)] * 2,
+        out_shape=[pltpu.VMEM((count, hidden), jnp.bfloat16)] * 2,
+        cost_estimate=cost(8 * count * width * hidden, 4 * width * hidden),
+        compiler_params=pltpu.CompilerParams(vmem_limit_bytes=STEP_MIB * 2**20),
+        name="last_units",
+    )(*map(far, rows), gate, up)
+
+
+def last_down(units, down, so_far, dtype):
+    count, width = so_far.shape
+
+    def body(units_ref, down_ref, old_ref, new_ref):
+        for at in range(0, width, CUT):
+            added = times_t(units_ref[...], down_ref[at : at + CUT])
+            new_ref[:, at : at + CUT] = (old_ref[:, at : at + CUT] + added).astype(dtype)
+
+    return pl.pallas_call(
+        body,
+        in_specs=[pl.BlockSpec(memory_space=pltpu.VMEM)] * 3,
+        out_specs=pl.BlockSpec(memory_space=pltpu.VMEM),
+        out_shape=pltpu.VMEM((count, width), dtype),
+        input_output_aliases={2: 0} if dtype == so_far.dtype else {},
+        cost_estimate=cost(2 * count * width * units.shape[1], 8 * count * width),
+        compiler_params=pltpu.CompilerParams(vmem_limit_bytes=STEP_MIB * 2**20),
+        name="last_down",
+    )(near(units), near(down), near(so_far))
+
+
+def both_cores(mine, theirs):
+    def body(mine_ref, theirs_ref, out_ref):
+        out_ref[...] = (mine_ref[...] + theirs_ref[...].astype(jnp.float32)).astype(jnp.bfloat16)
+
+    return pl.pallas_call(
+        body,
+        in_specs=[pl.BlockSpec(memory_space=pltpu.VMEM)] * 2,
+        out_specs=pl.BlockSpec(memory_space=pltpu.VMEM),
+        out_shape=pltpu.VMEM(mine.shape, jnp.bfloat16),
+        cost_estimate=cost(mine.size, 8 * mine.size),
+        compiler_params=pltpu.CompilerParams(vmem_limit_bytes=STEP_MIB * 2**20),
+        name="both_cores",
+    )(near(mine), near(theirs))
 
 
 def z_ring(own):
     chips = lax.axis_size("tp") // 2
-    up, down, found = own, own, []
+    fore, aft, found = own, own, []
 
     def moved(arrays, by):
         return [along_z(a, by) for a in arrays]
 
     for _ in range(1, chips // 2):
-        up, down = moved(up, 1), moved(down, -1)
-        found.append([[(a,) for a in up], [(a,) for a in down]])
-    half = own[0].shape[0] // 2
-    up = moved([a[:half] for a in up], 1)
-    down = moved([a[half:] for a in down], -1)
-    return found, list(zip(up, down))
+        fore, aft = moved(fore, 1), moved(aft, -1)
+        found.append([fore, aft])
+    return found, moved(fore, 1)
 
 
 def expert_half(
@@ -383,14 +443,15 @@
 
     kept = exchange(outgoing)
     lent = other_core(kept)
-    found[0].append([(a,) for a in own])
+    found[0].append(own)
     partial = ()
     for shards in found:
-        partial = expert_step((lent, kept), shards, tuple(partial), jnp.float32)
-    (sent,) = expert_step((lent,), [opposite], partial[:1], jnp.bfloat16)
-    back_home = other_core(sent)
-    (mine,) = expert_step((kept,), [opposite], partial[1:], jnp.float32)
-    result = (mine + back_home.astype(jnp.float32)).astype(jnp.bfloat16)
+        partial = expert_step((lent, kept), shards, tuple(partial))
+    lent_units, kept_units = last_units((lent, kept), *opposite[:2])
+    sent = last_down(lent_units, opposite[2], partial[0], jnp.bfloat16)
+    given = other_core(sent)
+    mine = last_down(kept_units, opposite[2], partial[1], jnp.float32)
+    result = both_cores(mine, given)
     return weighted_sum(back, exchange(result))
 
 

time: 242 us -> 229 us (0.946)
  local copies, waits for them, and re-layouts: 26.4 us -> 17.9 us
  Pallas kernels: 28.7 us -> 37 us
  waiting for transfers between devices: 110 us -> 105 us
  other arithmetic: 3.78 us -> 0 us
  starting transfers between devices: 67.3 us -> 63.8 us
    ppermute x24 -> x21, waiting for transfers between devices: 79.4 us -> 66.7 us  [along_z(): lax.ppermute(x, 'tp', [(i, (i + (2 * by if i % 2 == 0 else -2 * by)) % tp...]
    ppermute x2, starting transfers between devices: 10.2 us -> 0.01 us  [other_core(): return lax.ppermute(x, 'tp', [(i, i ^ 1) for i in range(tp)])]
    unnamed x87 -> x44, local copies, waits for them, and re-layouts: 23.3 us -> 15.9 us
    pallas_call x0 -> x4, Pallas kernels: none -> 6.92 us  [the longest x1 2.87 us: last_units(): pl.pallas_call(body, in_specs=[pl.BlockSpec(memory_space=pltpu.VMEM)] * 4...]
    all_to_all x1, waiting for transfers between devices: 0.64 us -> 7.15 us  [mixer_half(): lax.all_to_all(pieces, 'tp', split_axis=0, concat_axis=0, tiled=True)]
    ppermute x24 -> x21, starting transfers between devices: 29.9 us -> 34 us  [along_z(): lax.ppermute(x, 'tp', [(i, (i + (2 * by if i % 2 == 0 else -2 * by)) % tp...]
    convert_element_type x1 -> x0, other arithmetic: 3.08 us -> none  [expert_half(): result = (mine + back_home.astype(jnp.float32)).astype(jnp.bfloat16)]
    pallas_call x5 -> x3, Pallas kernels: 19.5 us -> 17.6 us  [expert_step(): pl.pallas_call(body, in_specs=[pl.BlockSpec(memory_space=pltpu.VMEM)] * (...]
  transfers between devices with their start and end apart: 31 -> 28, of which waited for: 12 -> 16; matrix products, arithmetic and copies ran while one was open for 5% -> 2% of each run, Pallas kernels for 9% -> 13%
where the time goes in v2:
time: 229 us; the launch traced here: 228 us
  waiting for transfers between devices  105 us (46%)
  starting transfers between devices  63.8 us (28%)
  Pallas kernels  37 us (16%)
  local copies, waits for them, and re-layouts  17.9 us (8%)
  matrix products  3.82 us (2%)
    ppermute x21, waiting for transfers between devices, along_z(): lax.ppermute(x, 'tp', [(i, (i + (2 * by if i % 2 == 0 else -2 * by)) % tp...  66.7 us
    ppermute x21, starting transfers between devices, along_z(): lax.ppermute(x, 'tp', [(i, (i + (2 * by if i % 2 == 0 else -2 * by)) % tp...  34 us
    all_to_all x2, waiting for transfers between devices, exchange(): lax.all_to_all(blocks, 'ep', split_axis=0, concat_axis=0, tiled=True)  23.2 us
    pallas_call x3, Pallas kernels, expert_step(): pl.pallas_call(body, in_specs=[pl.BlockSpec(memory_space=pltpu.VMEM)] * (...  17.6 us
    unnamed x44, local copies, waits for them, and re-layouts  15.9 us
    all_to_all x2, starting transfers between devices, exchange(): lax.all_to_all(blocks, 'ep', split_axis=0, concat_axis=0, tiled=True)  11.3 us
    all_to_all x1, starting transfers between devices, mixer_half(): lax.all_to_all(pieces, 'tp', split_axis=0, concat_axis=0, tiled=True)  8.33 us
    all_to_all x1, waiting for transfers between devices, mixer_half(): lax.all_to_all(pieces, 'tp', split_axis=0, concat_axis=0, tiled=True)  7.15 us
  transfers between devices with their start and end apart: 28, of which 16 were waited for; matrix products, arithmetic and copies ran while one was open for 2% of the time, Pallas kernels for 13%

profile of v2, /device:TPU:1, one launch (start us, length us, event | category | flops | bytes accessed | tf_op | source)
XLA Modules:
  0.0 228.0 jit_solution(1575815802447239121)
XLA Ops:
  0.6 0.7 broadcast_in_dim.15.gain_ref
  1.3 3.1 %token_rows.1 = (bf16[384,2048]{1,0:T(8,128)(2,1)}, bf16[3,128,384]{2,1,0:T(8,128)(2,1)S(1)}) custom-call(bf16[128,2048]{1,0:T(8,128)(2,1)} %act_ref.1, bf16[1,2048]{1,0:T(2,128)(2,1)S(1)} %broadcast_in_dim.15.gain_ref, s32[2,128]{1,0:T(2,128)} %bitcast.31, f32[2,128]{1,0:T(2,128)} %bitcast.32), custom_call_target="tpu_custom_call" | custom-call | flops 1000000000 | bytes 2000000 | tf_op jit(solution)/shard_map/token_rows/pallas_call | solution.py:256
  4.4 7.6 %all-to-all-start.2 = ((bf16[16,24,2048]{2,1,0:T(8,128)(2,1)}), bf16[16,24,2048]{2,1,0:T(8,128)(2,1)}, u32[]{:S(2)}, u32[]{:S(2)}) async-start(bf16[16,24,2048]{2,1,0:T(8,128)(2,1)} %bitcast.8), calls=%async_computation.2 | async-start | bytes 3145728 | tf_op jit(solution)/shard_map/all_to_all | solution.py:440
  12.0 5.7 %collective-permute-start.10 = (bf16[2048,128]{1,0:T(8,128)(2,1)S(1)}, bf16[2048,128]{1,0:T(8,128)(2,1)S(1)}, u32[]{:S(2)}, u32[]{:S(2)}) collective-permute-start(bf16[2048,128]{1,0:T(8,128)(2,1)S(1)} %bitcast.25), channel_id=1, source_target_pairs={{0,2},{1,15},{2,4},{3,1},{4,6},{5,3},{6,8},{7,5},{8,10},{9,7},{10,... | collective-permute-start | bytes 1572872 | tf_op jit(solution)/shard_map/ppermute | solution.py:27
  17.7 0.1 collective-permute-start.17
  17.8 2.7 %collective-permute-start.2 = (bf16[2048,128]{1,0:T(8,128)(2,1)S(1)}, bf16[2048,128]{1,0:T(8,128)(2,1)}, u32[]{:S(2)}, u32[]{:S(2)}) collective-permute-start(bf16[2048,128]{1,0:T(8,128)(2,1)S(1)} %bitcast.20), channel_id=1, source_target_pairs={{0,2},{1,15},{2,4},{3,1},{4,6},{5,3},{6,8},{7,5},{8,10},{9,7},{10,... | collective-permute-start | bytes 1572872 | tf_op jit(solution)/shard_map/ppermute | solution.py:27
  20.5 1.4 collective-permute-start.6
  21.8 6.1 %collective-permute-done.10.refs_4_ = bf16[2048,128]{1,0:T(8,128)(2,1)S(1)} collective-permute-done((bf16[2048,128]{1,0:T(8,128)(2,1)S(1)}, bf16[2048,128]{1,0:T(8,128)(2,1)S(1)}, u32[]{:S(2)}, u32[]{:S(2)}) %collective-permute-start.10) | collective-permute-done | bytes 524320 | tf_op jit(solution)/shard_map/ppermute | solution.py:27
  27.9 5.0 %collective-permute-done.14.refs_5_ = bf16[2048,128]{1,0:T(8,128)(2,1)S(1)} collective-permute-done((bf16[2048,128]{1,0:T(8,128)(2,1)S(1)}, bf16[2048,128]{1,0:T(8,128)(2,1)S(1)}, u32[]{:S(2)}, u32[]{:S(2)}) %collective-permute-start.14) | collective-permute-done | bytes 524320 | tf_op jit(solution)/shard_map/ppermute | solution.py:27
  33.0 0.8 copy-done.13
  33.8 10.4 %collective-permute-done.17.refs_6_ = bf16[2048,128]{1,0:T(8,128)(2,1)} collective-permute-done((bf16[2048,128]{1,0:T(8,128)(2,1)S(1)}, bf16[2048,128]{1,0:T(8,128)(2,1)}, u32[]{:S(2)}, u32[]{:S(2)}) %collective-permute-start.17) | collective-permute-done | bytes 524320 | tf_op jit(solution)/shard_map/ppermute | solution.py:27
  44.2 1.9 collective-permute-start.3
  46.1 4.3 %collective-permute-done.6.refs_3_ = bf16[2048,128]{1,0:T(8,128)(2,1)} collective-permute-done((bf16[2048,128]{1,0:T(8,128)(2,1)S(1)}, bf16[2048,128]{1,0:T(8,128)(2,1)}, u32[]{:S(2)}, u32[]{:S(2)}) %collective-permute-start.6) | collective-permute-done | bytes 524320 | tf_op jit(solution)/shard_map/ppermute | solution.py:27
  50.4 3.5 %collective-permute-start.7 = (bf16[2048,128]{1,0:T(8,128)(2,1)}, bf16[2048,128]{1,0:T(8,128)(2,1)S(1)}, u32[]{:S(2)}, u32[]{:S(2)}) collective-permute-start(bf16[2048,128]{1,0:T(8,128)(2,1)} %collective-permute-done.6.refs_3_), channel_id=1, source_target_pairs={{0,2},{1,15},{2,4},{3,1},{4,6},{5,3},{6,8},{7,5},{8,10},{9,7},{10,... | collective-permute-start | bytes 1572872 | tf_op jit(solution)/shard_map/ppermute | solution.py:27
  53.9 1.4 collective-permute-done.20.refs_7_
  55.3 0.8 copy-done.15
  56.1 1.4 collective-permute-done.11.refs_4_
  57.5 10.6 %collective-permute-done.3.refs_2_ = bf16[2048,128]{1,0:T(8,128)(2,1)S(1)} collective-permute-done((bf16[2048,128]{1,0:T(8,128)(2,1)}, bf16[2048,128]{1,0:T(8,128)(2,1)S(1)}, u32[]{:S(2)}, u32[]{:S(2)}) %collective-permute-start.3) | collective-permute-done | bytes 524320 | tf_op jit(solution)/shard_map/ppermute | solution.py:27
  68.1 3.3 %collective-permute-start.4 = (bf16[2048,128]{1,0:T(8,128)(2,1)S(1)}, bf16[2048,128]{1,0:T(8,128)(2,1)S(1)}, u32[]{:S(2)}, u32[]{:S(2)}) collective-permute-start(bf16[2048,128]{1,0:T(8,128)(2,1)S(1)} %collective-permute-done.3.refs_2_), channel_id=1, source_target_pairs={{0,2},{1,15},{2,4},{3,1},{4,6},{5,3},{6,8},{7,5},{8,10},{9,7},{10,... | collective-permute-start | bytes 1572872 | tf_op jit(solution)/shard_map/ppermute | solution.py:27
  71.4 7.9 %collective-permute-done.7.refs_3_ = bf16[2048,128]{1,0:T(8,128)(2,1)S(1)} collective-permute-done((bf16[2048,128]{1,0:T(8,128)(2,1)}, bf16[2048,128]{1,0:T(8,128)(2,1)S(1)}, u32[]{:S(2)}, u32[]{:S(2)}) %collective-permute-start.7) | collective-permute-done | bytes 524320 | tf_op jit(solution)/shard_map/ppermute | solution.py:27
  79.3 3.3 %collective-permute-start.8 = (bf16[2048,128]{1,0:T(8,128)(2,1)S(1)}, bf16[2048,128]{1,0:T(8,128)(2,1)S(1)}, u32[]{:S(2)}, u32[]{:S(2)}) collective-permute-start(bf16[2048,128]{1,0:T(8,128)(2,1)S(1)} %collective-permute-done.7.refs_3_), channel_id=1, source_target_pairs={{0,2},{1,15},{2,4},{3,1},{4,6},{5,3},{6,8},{7,5},{8,10},{9,7},{10,... | collective-permute-start | bytes 1572872 | tf_op jit(solution)/shard_map/ppermute | solution.py:27
  82.6 2.7 %collective-permute-start.12 = (bf16[2048,128]{1,0:T(8,128)(2,1)S(1)}, bf16[2048,128]{1,0:T(8,128)(2,1)S(1)}, u32[]{:S(2)}, u32[]{:S(2)}) collective-permute-start(bf16[2048,128]{1,0:T(8,128)(2,1)S(1)} %collective-permute-done.11.refs_4_), channel_id=1, source_target_pairs={{0,2},{1,15},{2,4},{3,1},{4,6},{5,3},{6,8},{7,5},{8,10},{9,7},{10,... | collective-permute-start | bytes 1572872 | tf_op jit(solution)/shard_map/ppermute | solution.py:27
  85.3 0.8 copy-done.3
  86.1 2.6 %collective-permute-start.5 = (bf16[2048,128]{1,0:T(8,128)(2,1)S(1)}, bf16[2048,128]{1,0:T(8,128)(2,1)S(1)}, u32[]{:S(2)}, u32[]{:S(2)}) collective-permute-start(bf16[2048,128]{1,0:T(8,128)(2,1)S(1)} %collective-permute-done.4.refs_2_), channel_id=1, source_target_pairs={{0,2},{1,15},{2,4},{3,1},{4,6},{5,3},{6,8},{7,5},{8,10},{9,7},{10,... | collective-permute-start | bytes 1572872 | tf_op jit(solution)/shard_map/ppermute | solution.py:27
  88.7 7.3 %collective-permute-done.8.refs_3_ = bf16[2048,128]{1,0:T(8,128)(2,1)S(1)} collective-permute-done((bf16[2048,128]{1,0:T(8,128)(2,1)S(1)}, bf16[2048,128]{1,0:T(8,128)(2,1)S(1)}, u32[]{:S(2)}, u32[]{:S(2)}) %collective-permute-start.8) | collective-permute-done | bytes 524320 | tf_op jit(solution)/shard_map/ppermute | solution.py:27
  96.1 3.4 %collective-permute-start.9 = (bf16[2048,128]{1,0:T(8,128)(2,1)S(1)}, bf16[2048,128]{1,0:T(8,128)(2,1)S(1)}, u32[]{:S(2)}, u32[]{:S(2)}) collective-permute-start(bf16[2048,128]{1,0:T(8,128)(2,1)S(1)} %collective-permute-done.8.refs_3_), channel_id=1, source_target_pairs={{0,2},{1,15},{2,4},{3,1},{4,6},{5,3},{6,8},{7,5},{8,10},{9,7},{10,... | collective-permute-start | bytes 1572872 | tf_op jit(solution)/shard_map/ppermute | solution.py:27
  99.5 3.0 %collective-permute-done.12.refs_4_ = bf16[2048,128]{1,0:T(8,128)(2,1)S(1)} collective-permute-done((bf16[2048,128]{1,0:T(8,128)(2,1)S(1)}, bf16[2048,128]{1,0:T(8,128)(2,1)S(1)}, u32[]{:S(2)}, u32[]{:S(2)}) %collective-permute-start.12) | collective-permute-done | bytes 524320 | tf_op jit(solution)/shard_map/ppermute | solution.py:27
  102.6 1.0 copy-done.21
  103.6 1.0 copy-done.8
  104.7 1.0 copy-done.10
  105.7 1.0 copy-done.12
  106.7 1.0 copy-done.14
  107.8 1.0 copy-done.16
  108.8 7.7 %shard_map.158 = (f32[384,2048]{1,0:T(8,128)S(1)}, f32[384,2048]{1,0:T(8,128)S(1)}) custom-call(bf16[384,2048]{1,0:T(8,128)(2,1)} %copy-done.21, bf16[384,2048]{1,0:T(8,128)(2,1)} %bitcast.9.refs_1_, bf16[2048,128]{1,0:T(8,128)(2,1)} %collective-permute-done.2.refs_2_, bf16[2048,128]{1,0:T(8,128)(2,1)} %collective-permute-done.6.refs_3_, ...), custom_call_target="tpu_custom_call" | custom-call | flops 3623878656 | bytes 4718592 | tf_op jit(solution)/shard_map/pallas_call | solution.py:332
  116.5 3.4 %collective-permute-start.13 = (bf16[2048,128]{1,0:T(8,128)(2,1)S(1)}, bf16[2048,128]{1,0:T(8,128)(2,1)S(1)}, u32[]{:S(2)}, u32[]{:S(2)}) collective-permute-start(bf16[2048,128]{1,0:T(8,128)(2,1)S(1)} %collective-permute-done.12.refs_4_), channel_id=1, source_target_pairs={{0,2},{1,15},{2,4},{3,1},{4,6},{5,3},{6,8},{7,5},{8,10},{9,7},{10,... | collective-permute-start | bytes 1572872 | tf_op jit(solution)/shard_map/ppermute | solution.py:27
  119.9 4.4 %collective-permute-done.9.refs_3_ = bf16[2048,128]{1,0:T(8,128)(2,1)S(1)} collective-permute-done((bf16[2048,128]{1,0:T(8,128)(2,1)S(1)}, bf16[2048,128]{1,0:T(8,128)(2,1)S(1)}, u32[]{:S(2)}, u32[]{:S(2)}) %collective-permute-start.9) | collective-permute-done | bytes 524320 | tf_op jit(solution)/shard_map/ppermute | solution.py:27
  124.4 2.9 %last_units.1 = (bf16[384,128]{1,0:T(8,128)(2,1)S(1)}, bf16[384,128]{1,0:T(8,128)(2,1)S(1)}) custom-call(bf16[384,2048]{1,0:T(8,128)(2,1)} %copy-done.21, bf16[384,2048]{1,0:T(8,128)(2,1)} %bitcast.9.refs_1_, bf16[2048,128]{1,0:T(8,128)(2,1)S(1)} %collective-permute-done.5.refs_2_, bf16[2048,128]{1,0:T(8,128)(2,1)S(1)} %collective-permute-done.9.refs_3_), custom_call_target="tpu_custom_call" | custom-call | flops 805306368 | bytes 1048576 | tf_op jit(solution)/shard_map/last_units/pallas_call | solution.py:355
  127.2 5.0 %shard_map.159 = (f32[384,2048]{1,0:T(8,128)S(1)}, f32[384,2048]{1,0:T(8,128)S(1)}) custom-call(bf16[384,2048]{1,0:T(8,128)(2,1)} %copy-done.21, bf16[384,2048]{1,0:T(8,128)(2,1)} %bitcast.9.refs_1_, bf16[2048,128]{1,0:T(8,128)(2,1)S(1)} %collective-permute-done.3.refs_2_, ...), custom_call_target="tpu_custom_call", output_to_operand_aliasing={{0}: (8, {}), {1}: (9, {})} | custom-call | flops 2415919104 | bytes 3145728 | tf_op jit(solution)/shard_map/pallas_call | solution.py:332
  132.2 4.9 %collective-permute-done.22.refs_7_ = bf16[2048,128]{1,0:T(8,128)(2,1)S(1)} collective-permute-done((bf16[2048,128]{1,0:T(8,128)(2,1)S(1)}, bf16[2048,128]{1,0:T(8,128)(2,1)S(1)}, u32[]{:S(2)}, u32[]{:S(2)}) %collective-permute-start.22) | collective-permute-done | bytes 524320 | tf_op jit(solution)/shard_map/ppermute | solution.py:27
  137.1 5.0 %shard_map.160 = (f32[384,2048]{1,0:T(8,128)S(1)}, f32[384,2048]{1,0:T(8,128)S(1)}) custom-call(bf16[384,2048]{1,0:T(8,128)(2,1)} %copy-done.21, bf16[384,2048]{1,0:T(8,128)(2,1)} %bitcast.9.refs_1_, bf16[2048,128]{1,0:T(8,128)(2,1)S(1)} %collective-permute-done.4.refs_2_, ...), custom_call_target="tpu_custom_call", output_to_operand_aliasing={{0}: (8, {}), {1}: (9, {})} | custom-call | flops 2415919104 | bytes 3145728 | tf_op jit(solution)/shard_map/pallas_call | solution.py:332
  142.1 1.7 last_down.3
  143.8 1.3 slice.3
  145.2 3.0 %collective-permute-start = (bf16[64,128]{1,0:T(8,128)(2,1)}, bf16[64,128]{1,0:T(8,128)(2,1)S(1)}, u32[]{:S(2)}, u32[]{:S(2)}) collective-permute-start(bf16[64,128]{1,0:T(8,128)(2,1)} %slice.3), channel_id=1, source_target_pairs={{0,16},{16,32},{32,48},{48,64},{64,80},{80,96},{96,112},{112,128},... | collective-permute-start | bytes 49160 | tf_op jit(solution)/shard_map/ppermute | solution.py:22
  148.2 1.1 collective-permute-done.halo_ref
  149.3 6.4 %local_scan.1 = (f32[64,2048]{1,0:T(8,128)S(1)}, f32[64,2048]{1,0:T(8,128)S(1)}, f32[16,8,128]{2,1,0:T(8,128)S(1)}) custom-call(s32[1]{0:T(128)} %bitcast.1.group_ref, bf16[64,2048]{1,0:T(8,128)(2,1)} %x_ref.1, bf16[64,128]{1,0:T(8,128)(2,1)S(1)} %collective-permute-done.halo_ref, bf16[4,1024]{1,0:T(4,128)(2,1)} %bitcast.28, bf16[16,64,64]{2,1,0:T(8,128)(2,1)} %rate_ref.1, ...), custom_call_target="tpu_custom_call" | custom-call | flops 4000000000 | bytes 2000000 | tf_op jit(solution)/shard_map/local_scan/pallas_call | solution.py:125
  155.6 0.6 copy-done.6
  156.3 0.8 copy-done.17
  157.0 0.8 copy-done.19
  157.8 7.1 %all-to-all-start = ((f32[16,8,128]{2,1,0:T(8,128)}), f32[16,8,128]{2,1,0:T(8,128)}, u32[]{:S(2)}, u32[]{:S(2)}) async-start(f32[16,8,128]{2,1,0:T(8,128)} %copy-done.6), calls=%async_computation | async-start | bytes 131072 | tf_op jit(solution)/shard_map/all_to_all | solution.py:16
  164.9 6.6 %all-to-all-done.totals_ref = f32[16,8,128]{2,1,0:T(8,128)} async-done(((f32[16,8,128]{2,1,0:T(8,128)}), f32[16,8,128]{2,1,0:T(8,128)}, u32[]{:S(2)}, u32[]{:S(2)}) %all-to-all-start) | async-done | bytes 65568 | tf_op jit(solution)/shard_map/all_to_all | solution.py:16
  171.5 1.0 copy-done.18
  172.5 1.0 copy-done.20
  173.6 1.2 gated_states.1
  174.8 0.7 copy-done.5
  175.5 8.3 %all-to-all-start.1 = ((bf16[16,64,128]{2,1,0:T(8,128)(2,1)}), bf16[16,64,128]{2,1,0:T(8,128)(2,1)}, u32[]{:S(2)}, u32[]{:S(2)}) async-start(bf16[16,64,128]{2,1,0:T(8,128)(2,1)} %copy-done.5), calls=%async_computation.1 | async-start | bytes 524288 | tf_op jit(solution)/shard_map/all_to_all | solution.py:217
  183.8 1.0 copy-done.2
  184.9 0.6 last_down.2.mine_ref
  185.5 1.7 both_cores.1
  187.2 1.2 copy-done
  188.4 7.2 %all-to-all-done.1 = bf16[16,64,128]{2,1,0:T(8,128)(2,1)} async-done(((bf16[16,64,128]{2,1,0:T(8,128)(2,1)}), bf16[16,64,128]{2,1,0:T(8,128)(2,1)}, u32[]{:S(2)}, u32[]{:S(2)}) %all-to-all-start.1) | async-done | bytes 262176 | tf_op jit(solution)/shard_map/all_to_all | solution.py:217
  195.5 3.7 %all-to-all-start.3 = ((bf16[16,24,2048]{2,1,0:T(8,128)(2,1)}), bf16[16,24,2048]{2,1,0:T(8,128)(2,1)S(1)}, u32[]{:S(2)}, u32[]{:S(2)}) async-start(bf16[16,24,2048]{2,1,0:T(8,128)(2,1)} %bitcast.18), calls=%async_computation.3 | async-start | bytes 3145728 | tf_op jit(solution)/shard_map/all_to_all | solution.py:440
  199.2 3.8 %convolution_convert_fusion = bf16[128,2048]{1,0:T(8,128)(2,1)} fusion(bf16[1024,128]{1,0:T(8,128)(2,1)} %bitcast.5, bf16[1024,2048]{1,0:T(8,128)(2,1)} %param.22), kind=kOutput, calls=%fused_computation | convolution fusion | flops 537133056 | bytes 4980736 | tf_op jit(solution)/shard_map/dot_general | solution.py:218
  203.1 23.2 %all-to-all-done.3 = bf16[16,24,2048]{2,1,0:T(8,128)(2,1)S(1)} async-done(((bf16[16,24,2048]{2,1,0:T(8,128)(2,1)}), bf16[16,24,2048]{2,1,0:T(8,128)(2,1)S(1)}, u32[]{:S(2)}, u32[]{:S(2)}) %all-to-all-start.3) | async-done | bytes 1572896 | tf_op jit(solution)/shard_map/all_to_all | solution.py:440
  226.2 1.8 weighted_sum.1
  (50 shorter events, 0.2 us)
Async XLA Ops:
  1.3 10.7 %copy-start.11 = (bf16[1,2048,128]{2,1,0:T(8,128)(2,1)S(1)}, bf16[1,2048,128]{2,1,0:T(8,128)(2,1)}, u32[]{:S(2)}) copy-start(bf16[1,2048,128]{2,1,0:T(8,128)(2,1)} %param.29) | copy-start | bytes 1572868
  1.3 16.4 %copy-start.7 = (bf16[1,2048,128]{2,1,0:T(8,128)(2,1)S(1)}, bf16[1,2048,128]{2,1,0:T(8,128)(2,1)}, u32[]{:S(2)}) copy-start(bf16[1,2048,128]{2,1,0:T(8,128)(2,1)} %param.27) | copy-start | bytes 1572868
  1.3 16.4 %copy-start.9 = (bf16[1,2048,128]{2,1,0:T(8,128)(2,1)S(1)}, bf16[1,2048,128]{2,1,0:T(8,128)(2,1)}, u32[]{:S(2)}) copy-start(bf16[1,2048,128]{2,1,0:T(8,128)(2,1)} %param.28) | copy-start | bytes 1572868
  4.4 39.8 %all-to-all-start.2 = ((bf16[16,24,2048]{2,1,0:T(8,128)(2,1)}), bf16[16,24,2048]{2,1,0:T(8,128)(2,1)}, u32[]{:S(2)}, u32[]{:S(2)}) async-start(bf16[16,24,2048]{2,1,0:T(8,128)(2,1)} %bitcast.8), calls=%async_computation.2 | async-start | bytes 3145728 | tf_op jit(solution)/shard_map/all_to_all | solution.py:440
  12.0 15.9 %collective-permute-start.10 = (bf16[2048,128]{1,0:T(8,128)(2,1)S(1)}, bf16[2048,128]{1,0:T(8,128)(2,1)S(1)}, u32[]{:S(2)}, u32[]{:S(2)}) collective-permute-start(bf16[2048,128]{1,0:T(8,128)(2,1)S(1)} %bitcast.25), channel_id=1, source_target_pairs={{0,2},{1,15},{2,4},{3,1},{4,6},{5,3},{6,8},{7,5},{8,10},{9,7},{10,... | collective-permute-start | bytes 1572872 | tf_op jit(solution)/shard_map/ppermute | solution.py:27
  17.7 15.3 %collective-permute-start.14 = (bf16[2048,128]{1,0:T(8,128)(2,1)S(1)}, bf16[2048,128]{1,0:T(8,128)(2,1)S(1)}, u32[]{:S(2)}, u32[]{:S(2)}) collective-permute-start(bf16[2048,128]{1,0:T(8,128)(2,1)S(1)} %bitcast.19), channel_id=1, source_target_pairs={{0,14},{1,3},{2,0},{3,5},{4,2},{5,7},{6,4},{7,9},{8,6},{9,11},{10,... | collective-permute-start | bytes 1572872 | tf_op jit(solution)/shard_map/ppermute | solution.py:27
  17.7 26.5 %collective-permute-start.17 = (bf16[2048,128]{1,0:T(8,128)(2,1)S(1)}, bf16[2048,128]{1,0:T(8,128)(2,1)}, u32[]{:S(2)}, u32[]{:S(2)}) collective-permute-start(bf16[2048,128]{1,0:T(8,128)(2,1)S(1)} %bitcast.22), channel_id=1, source_target_pairs={{0,14},{1,3},{2,0},{3,5},{4,2},{5,7},{6,4},{7,9},{8,6},{9,11},{10,... | collective-permute-start | bytes 1572872 | tf_op jit(solution)/shard_map/ppermute | solution.py:27
  17.8 26.4 %collective-permute-start.2 = (bf16[2048,128]{1,0:T(8,128)(2,1)S(1)}, bf16[2048,128]{1,0:T(8,128)(2,1)}, u32[]{:S(2)}, u32[]{:S(2)}) collective-permute-start(bf16[2048,128]{1,0:T(8,128)(2,1)S(1)} %bitcast.20), channel_id=1, source_target_pairs={{0,2},{1,15},{2,4},{3,1},{4,6},{5,3},{6,8},{7,5},{8,10},{9,7},{10,... | collective-permute-start | bytes 1572872 | tf_op jit(solution)/shard_map/ppermute | solution.py:27
  20.5 29.9 %collective-permute-start.6 = (bf16[2048,128]{1,0:T(8,128)(2,1)S(1)}, bf16[2048,128]{1,0:T(8,128)(2,1)}, u32[]{:S(2)}, u32[]{:S(2)}) collective-permute-start(bf16[2048,128]{1,0:T(8,128)(2,1)S(1)} %bitcast.23), channel_id=1, source_target_pairs={{0,2},{1,15},{2,4},{3,1},{4,6},{5,3},{6,8},{7,5},{8,10},{9,7},{10,... | collective-permute-start | bytes 1572872 | tf_op jit(solution)/shard_map/ppermute | solution.py:27
  27.9 27.4 %collective-permute-start.20 = (bf16[2048,128]{1,0:T(8,128)(2,1)S(1)}, bf16[2048,128]{1,0:T(8,128)(2,1)}, u32[]{:S(2)}, u32[]{:S(2)}) collective-permute-start(bf16[2048,128]{1,0:T(8,128)(2,1)S(1)} %bitcast.26), channel_id=1, source_target_pairs={{0,14},{1,3},{2,0},{3,5},{4,2},{5,7},{6,4},{7,9},{8,6},{9,11},{10,... | collective-permute-start | bytes 1572872 | tf_op jit(solution)/shard_map/ppermute | solution.py:27
  33.0 24.6 %collective-permute-start.11 = (bf16[2048,128]{1,0:T(8,128)(2,1)S(1)}, bf16[2048,128]{1,0:T(8,128)(2,1)S(1)}, u32[]{:S(2)}, u32[]{:S(2)}) collective-permute-start(bf16[2048,128]{1,0:T(8,128)(2,1)S(1)} %collective-permute-done.10.refs_4_), channel_id=1, source_target_pairs={{0,2},{1,15},{2,4},{3,1},{4,6},{5,3},{6,8},{7,5},{8,10},{9,7},{10,... | collective-permute-start | bytes 1572872 | tf_op jit(solution)/shard_map/ppermute | solution.py:27
  33.0 0.8 copy-start.13
  44.2 58.3 %collective-permute-start.1 = (bf16[384,2048]{1,0:T(8,128)(2,1)}, bf16[384,2048]{1,0:T(8,128)(2,1)S(1)}, u32[]{:S(2)}, u32[]{:S(2)}) collective-permute-start(bf16[384,2048]{1,0:T(8,128)(2,1)} %bitcast.9.refs_1_), channel_id=1, source_target_pairs={{0,1},{1,0},{2,3},{3,2},{4,5},{5,4},{6,7},{7,6},{8,9},{9,8},{10,11... | collective-permute-start | bytes 4718600 | tf_op jit(solution)/shard_map/ppermute | solution.py:32
  44.2 23.9 %collective-permute-start.3 = (bf16[2048,128]{1,0:T(8,128)(2,1)}, bf16[2048,128]{1,0:T(8,128)(2,1)S(1)}, u32[]{:S(2)}, u32[]{:S(2)}) collective-permute-start(bf16[2048,128]{1,0:T(8,128)(2,1)} %collective-permute-done.2.refs_2_), channel_id=1, source_target_pairs={{0,2},{1,15},{2,4},{3,1},{4,6},{5,3},{6,8},{7,5},{8,10},{9,7},{10,... | collective-permute-start | bytes 1572872 | tf_op jit(solution)/shard_map/ppermute | solution.py:27
  50.4 28.9 %collective-permute-start.7 = (bf16[2048,128]{1,0:T(8,128)(2,1)}, bf16[2048,128]{1,0:T(8,128)(2,1)S(1)}, u32[]{:S(2)}, u32[]{:S(2)}) collective-permute-start(bf16[2048,128]{1,0:T(8,128)(2,1)} %collective-permute-done.6.refs_3_), channel_id=1, source_target_pairs={{0,2},{1,15},{2,4},{3,1},{4,6},{5,3},{6,8},{7,5},{8,10},{9,7},{10,... | collective-permute-start | bytes 1572872 | tf_op jit(solution)/shard_map/ppermute | solution.py:27
  55.3 27.3 %collective-permute-start.15 = (bf16[2048,128]{1,0:T(8,128)(2,1)S(1)}, bf16[2048,128]{1,0:T(8,128)(2,1)S(1)}, u32[]{:S(2)}, u32[]{:S(2)}) collective-permute-start(bf16[2048,128]{1,0:T(8,128)(2,1)S(1)} %collective-permute-done.14.refs_5_), channel_id=1, source_target_pairs={{0,14},{1,3},{2,0},{3,5},{4,2},{5,7},{6,4},{7,9},{8,6},{9,11},{10,... | collective-permute-start | bytes 1572872 | tf_op jit(solution)/shard_map/ppermute | solution.py:27
  55.3 0.8 copy-start.15
  57.5 25.1 %collective-permute-start.18 = (bf16[2048,128]{1,0:T(8,128)(2,1)}, bf16[2048,128]{1,0:T(8,128)(2,1)S(1)}, u32[]{:S(2)}, u32[]{:S(2)}) collective-permute-start(bf16[2048,128]{1,0:T(8,128)(2,1)} %collective-permute-done.17.refs_6_), channel_id=1, source_target_pairs={{0,14},{1,3},{2,0},{3,5},{4,2},{5,7},{6,4},{7,9},{8,6},{9,11},{10,... | collective-permute-start | bytes 1572872 | tf_op jit(solution)/shard_map/ppermute | solution.py:27
  68.1 18.0 %collective-permute-start.4 = (bf16[2048,128]{1,0:T(8,128)(2,1)S(1)}, bf16[2048,128]{1,0:T(8,128)(2,1)S(1)}, u32[]{:S(2)}, u32[]{:S(2)}) collective-permute-start(bf16[2048,128]{1,0:T(8,128)(2,1)S(1)} %collective-permute-done.3.refs_2_), channel_id=1, source_target_pairs={{0,2},{1,15},{2,4},{3,1},{4,6},{5,3},{6,8},{7,5},{8,10},{9,7},{10,... | collective-permute-start | bytes 1572872 | tf_op jit(solution)/shard_map/ppermute | solution.py:27
  79.3 16.7 %collective-permute-start.8 = (bf16[2048,128]{1,0:T(8,128)(2,1)S(1)}, bf16[2048,128]{1,0:T(8,128)(2,1)S(1)}, u32[]{:S(2)}, u32[]{:S(2)}) collective-permute-start(bf16[2048,128]{1,0:T(8,128)(2,1)S(1)} %collective-permute-done.7.refs_3_), channel_id=1, source_target_pairs={{0,2},{1,15},{2,4},{3,1},{4,6},{5,3},{6,8},{7,5},{8,10},{9,7},{10,... | collective-permute-start | bytes 1572872 | tf_op jit(solution)/shard_map/ppermute | solution.py:27
  82.6 16.8 %collective-permute-start.21 = (bf16[2048,128]{1,0:T(8,128)(2,1)}, bf16[2048,128]{1,0:T(8,128)(2,1)S(1)}, u32[]{:S(2)}, u32[]{:S(2)}) collective-permute-start(bf16[2048,128]{1,0:T(8,128)(2,1)} %collective-permute-done.20.refs_7_), channel_id=1, source_target_pairs={{0,14},{1,3},{2,0},{3,5},{4,2},{5,7},{6,4},{7,9},{8,6},{9,11},{10,... | collective-permute-start | bytes 1572872 | tf_op jit(solution)/shard_map/ppermute | solution.py:27
  82.6 19.8 %collective-permute-start.12 = (bf16[2048,128]{1,0:T(8,128)(2,1)S(1)}, bf16[2048,128]{1,0:T(8,128)(2,1)S(1)}, u32[]{:S(2)}, u32[]{:S(2)}) collective-permute-start(bf16[2048,128]{1,0:T(8,128)(2,1)S(1)} %collective-permute-done.11.refs_4_), channel_id=1, source_target_pairs={{0,2},{1,15},{2,4},{3,1},{4,6},{5,3},{6,8},{7,5},{8,10},{9,7},{10,... | collective-permute-start | bytes 1572872 | tf_op jit(solution)/shard_map/ppermute | solution.py:27
  85.3 0.8 copy-start.3
  86.1 30.4 %collective-permute-start.5 = (bf16[2048,128]{1,0:T(8,128)(2,1)S(1)}, bf16[2048,128]{1,0:T(8,128)(2,1)S(1)}, u32[]{:S(2)}, u32[]{:S(2)}) collective-permute-start(bf16[2048,128]{1,0:T(8,128)(2,1)S(1)} %collective-permute-done.4.refs_2_), channel_id=1, source_target_pairs={{0,2},{1,15},{2,4},{3,1},{4,6},{5,3},{6,8},{7,5},{8,10},{9,7},{10,... | collective-permute-start | bytes 1572872 | tf_op jit(solution)/shard_map/ppermute | solution.py:27
  96.1 28.3 %collective-permute-start.9 = (bf16[2048,128]{1,0:T(8,128)(2,1)S(1)}, bf16[2048,128]{1,0:T(8,128)(2,1)S(1)}, u32[]{:S(2)}, u32[]{:S(2)}) collective-permute-start(bf16[2048,128]{1,0:T(8,128)(2,1)S(1)} %collective-permute-done.8.refs_3_), channel_id=1, source_target_pairs={{0,2},{1,15},{2,4},{3,1},{4,6},{5,3},{6,8},{7,5},{8,10},{9,7},{10,... | collective-permute-start | bytes 1572872 | tf_op jit(solution)/shard_map/ppermute | solution.py:27
  99.5 32.8 %collective-permute-start.16 = (bf16[2048,128]{1,0:T(8,128)(2,1)S(1)}, bf16[2048,128]{1,0:T(8,128)(2,1)S(1)}, u32[]{:S(2)}, u32[]{:S(2)}) collective-permute-start(bf16[2048,128]{1,0:T(8,128)(2,1)S(1)} %collective-permute-done.15.refs_5_), channel_id=1, source_target_pairs={{0,14},{1,3},{2,0},{3,5},{4,2},{5,7},{6,4},{7,9},{8,6},{9,11},{10,... | collective-permute-start | bytes 1572872 | tf_op jit(solution)/shard_map/ppermute | solution.py:27
  102.5 29.8 %collective-permute-start.19 = (bf16[2048,128]{1,0:T(8,128)(2,1)S(1)}, bf16[2048,128]{1,0:T(8,128)(2,1)S(1)}, u32[]{:S(2)}, u32[]{:S(2)}) collective-permute-start(bf16[2048,128]{1,0:T(8,128)(2,1)S(1)} %collective-permute-done.18.refs_6_), channel_id=1, source_target_pairs={{0,14},{1,3},{2,0},{3,5},{4,2},{5,7},{6,4},{7,9},{8,6},{9,11},{10,... | collective-permute-start | bytes 1572872 | tf_op jit(solution)/shard_map/ppermute | solution.py:27
  102.5 1.1 copy-start.21
  102.5 34.6 %collective-permute-start.22 = (bf16[2048,128]{1,0:T(8,128)(2,1)S(1)}, bf16[2048,128]{1,0:T(8,128)(2,1)S(1)}, u32[]{:S(2)}, u32[]{:S(2)}) collective-permute-start(bf16[2048,128]{1,0:T(8,128)(2,1)S(1)} %collective-permute-done.21.refs_7_), channel_id=1, source_target_pairs={{0,14},{1,3},{2,0},{3,5},{4,2},{5,7},{6,4},{7,9},{8,6},{9,11},{10,... | collective-permute-start | bytes 1572872 | tf_op jit(solution)/shard_map/ppermute | solution.py:27
  103.6 1.0 copy-start.8
  104.7 1.0 copy-start.10
  105.7 1.0 copy-start.12
  106.7 1.0 copy-start.14
  107.8 1.0 copy-start.16
  116.5 10.7 %copy-start.4 = (bf16[2048,128]{1,0:T(8,128)(2,1)S(1)}, bf16[2048,128]{1,0:T(8,128)(2,1)}, u32[]{:S(2)}) copy-start(bf16[2048,128]{1,0:T(8,128)(2,1)} %copy-done.3) | copy-start | bytes 1572868
  116.5 25.5 %collective-permute-start.13 = (bf16[2048,128]{1,0:T(8,128)(2,1)S(1)}, bf16[2048,128]{1,0:T(8,128)(2,1)S(1)}, u32[]{:S(2)}, u32[]{:S(2)}) collective-permute-start(bf16[2048,128]{1,0:T(8,128)(2,1)S(1)} %collective-permute-done.12.refs_4_), channel_id=1, source_target_pairs={{0,2},{1,15},{2,4},{3,1},{4,6},{5,3},{6,8},{7,5},{8,10},{9,7},{10,... | collective-permute-start | bytes 1572872 | tf_op jit(solution)/shard_map/ppermute | solution.py:27
  142.1 1.8 copy-start.1
  143.8 41.7 %collective-permute-start.23 = (bf16[384,2048]{1,0:T(8,128)(2,1)}, bf16[384,2048]{1,0:T(8,128)(2,1)}, u32[]{:S(2)}, u32[]{:S(2)}) collective-permute-start(bf16[384,2048]{1,0:T(8,128)(2,1)} %last_down.3), channel_id=1, source_target_pairs={{0,1},{1,0},{2,3},{3,2},{4,5},{5,4},{6,7},{7,6},{8,9},{9,8},{10,11... | collective-permute-start | bytes 4718600 | tf_op jit(solution)/shard_map/ppermute | solution.py:32
  145.2 4.1 %collective-permute-start = (bf16[64,128]{1,0:T(8,128)(2,1)}, bf16[64,128]{1,0:T(8,128)(2,1)S(1)}, u32[]{:S(2)}, u32[]{:S(2)}) collective-permute-start(bf16[64,128]{1,0:T(8,128)(2,1)} %slice.3), channel_id=1, source_target_pairs={{0,16},{16,32},{32,48},{48,64},{64,80},{80,96},{96,112},{112,128},... | collective-permute-start | bytes 49160 | tf_op jit(solution)/shard_map/ppermute | solution.py:22
  155.6 0.6 copy-start.6
  156.2 0.8 copy-start.17
  157.0 0.8 copy-start.19
  157.8 13.6 %all-to-all-start = ((f32[16,8,128]{2,1,0:T(8,128)}), f32[16,8,128]{2,1,0:T(8,128)}, u32[]{:S(2)}, u32[]{:S(2)}) async-start(f32[16,8,128]{2,1,0:T(8,128)} %copy-done.6), calls=%async_computation | async-start | bytes 131072 | tf_op jit(solution)/shard_map/all_to_all | solution.py:16
  171.5 1.0 copy-start.18
  172.5 1.0 copy-start.20
  174.8 0.7 copy-start.5
  175.5 20.0 %all-to-all-start.1 = ((bf16[16,64,128]{2,1,0:T(8,128)(2,1)}), bf16[16,64,128]{2,1,0:T(8,128)(2,1)}, u32[]{:S(2)}, u32[]{:S(2)}) async-start(bf16[16,64,128]{2,1,0:T(8,128)(2,1)} %copy-done.5), calls=%async_computation.1 | async-start | bytes 524288 | tf_op jit(solution)/shard_map/all_to_all | solution.py:217
  183.8 1.0 copy-start.2
  187.2 1.2 copy-start
  195.5 30.7 %all-to-all-start.3 = ((bf16[16,24,2048]{2,1,0:T(8,128)(2,1)}), bf16[16,24,2048]{2,1,0:T(8,128)(2,1)S(1)}, u32[]{:S(2)}, u32[]{:S(2)}) async-start(bf16[16,24,2048]{2,1,0:T(8,128)(2,1)} %bitcast.18), calls=%async_computation.3 | async-start | bytes 3145728 | tf_op jit(solution)/shard_map/all_to_all | solution.py:440

commit v3 on v2

--- a/solution.py
+++ b/solution.py
@@ -1,3 +1,5 @@
+import math
+
 import jax
 import jax.numpy as jnp
 from jax import lax
@@ -223,8 +225,9 @@
     ).astype(jnp.bfloat16)
 
 
-def token_rows(activity, gain, ids, share, experts, slots):
+def token_rows(activity, gain, ids, share, slots, order):
     tokens, width = activity.shape
+    experts = len(order)
 
     def body(act_ref, gain_ref, ids_ref, share_ref, rows_ref, back_ref):
         values = act_ref[...].astype(jnp.float32)
@@ -243,9 +246,12 @@
             rank = times(mine.astype(jnp.bfloat16), ahead) + count
             rank = jnp.sum(mine * rank, axis=0, keepdims=True)
             count = count + jnp.sum(mine, axis=1, keepdims=True)
-            here = slot == ids_ref[j : j + 1] * slots + rank.astype(jnp.int32)
-            taken = taken + jnp.where(here, 1.0, 0.0)
-            back = back + jnp.where(here, share_ref[j : j + 1], 0.0)
+            chosen, rank = ids_ref[j : j + 1], rank.astype(jnp.int32)
+            comes = jnp.zeros_like(chosen)
+            for k, e in enumerate(order):
+                comes = jnp.where(chosen == e, k, comes)
+            taken = taken + jnp.where(slot == chosen * slots + rank, 1.0, 0.0)
+            back = back + jnp.where(slot == comes * slots + rank, share_ref[j : j + 1], 0.0)
         rows_ref[...] = times(taken.astype(jnp.bfloat16), normed).astype(jnp.bfloat16)
         rest = back.T
         for k in range(3):
@@ -270,18 +276,22 @@
     width = results.shape[1]
 
     def body(back_ref, results_ref, out_ref):
-        total = times(back_ref[0], results_ref[...])
-        for k in range(1, parts):
-            total = total + times(back_ref[k], results_ref[...])
-        out_ref[...] = total.astype(jnp.bfloat16)
-
-    return pl.pallas_call(
-        body,
+        for at in range(0, width, CUT):
+            cut = slice(at, at + CUT)
+            each = times(back_ref[...], results_ref[:, cut])
+            total = each[:tokens]
+            for k in range(1, parts):
+                total = total + each[k * tokens : (k + 1) * tokens]
+            out_ref[:, cut] = total.astype(jnp.bfloat16)
+
+    return pl.pallas_call(
+        body,
+        in_specs=[pl.BlockSpec(memory_space=pltpu.VMEM)] * 2,
         out_shape=jax.ShapeDtypeStruct((tokens, width), jnp.bfloat16),
         cost_estimate=cost(2 * parts * tokens * slots * width, 2 * slots * width),
         compiler_params=pltpu.CompilerParams(vmem_limit_bytes=12 * 2**20),
         name="weighted_sum",
-    )(back, results)
+    )(near(back.reshape(parts * tokens, slots)), near(results))
 
 
 def near(x):
@@ -294,7 +304,7 @@
     return ((up_cut + 1.0) * gate_cut * jax.nn.sigmoid(1.702 * gate_cut)).astype(jnp.bfloat16)
 
 
-def expert_step(rows, shards, so_far):
+def expert_step(rows, shards, so_far, leaving=()):
     sets, count, width = len(rows), *rows[0].shape
     hidden = shards[0][0].shape[1]
     operands = [a for shard in shards for a in shard]
@@ -328,12 +338,15 @@
                     new[k][:, at : at + CUT] = added
                 first += 2
 
-    alias = {sets + len(operands) + k: k for k in range(sets)} if so_far else {}
+    alias = {sets + len(operands) + k: k for k in range(len(so_far)) if k not in leaving}
     return pl.pallas_call(
         body,
         in_specs=[pl.BlockSpec(memory_space=pltpu.VMEM)] * (sets + len(operands) + len(so_far)),
         out_specs=[pl.BlockSpec(memory_space=pltpu.VMEM)] * sets,
-        out_shape=[pltpu.VMEM((count, width), jnp.float32)] * sets,
+        out_shape=[
+            (jax.ShapeDtypeStruct if k in leaving else pltpu.VMEM)((count, width), jnp.float32)
+            for k in range(sets)
+        ],
         input_output_aliases=alias,
         cost_estimate=cost(
             2 * sets * count * 3 * width * hidden * len(shards), 6 * width * hidden * len(shards)
@@ -342,60 +355,67 @@
     )(*map(far, rows), *operands, *map(near, so_far))
 
 
-def last_units(rows, gate, up):
-    count, width = rows[0].shape
-    hidden = gate.shape[1]
-
-    def body(*refs):
-        both = jnp.concatenate([refs[2][...], refs[3][...]], axis=1)
-        for k in range(2):
-            pre = times(refs[k][...], both)
-            refs[4 + k][...] = gated(pre[:, :hidden], pre[:, hidden:])
-
-    return pl.pallas_call(
-        body,
-        in_specs=[pl.BlockSpec(memory_space=pltpu.VMEM)] * 4,
-        out_specs=[pl.BlockSpec(memory_space=pltpu.VMEM)] * 2,
-        out_shape=[pltpu.VMEM((count, hidden), jnp.bfloat16)] * 2,
-        cost_estimate=cost(8 * count * width * hidden, 4 * width * hidden),
+def last_units(row, shards):
+    count, width = row.shape
+    hidden = shards[0][0].shape[1]
+
+    def body(row_ref, *refs):
+        weights, out_ref = refs[:-1], refs[-1]
+        gate = jnp.concatenate([weights[0][...], weights[2][...]], axis=1)
+        up = jnp.concatenate([weights[1][...], weights[3][...]], axis=1)
+        out_ref[...] = gated(times(row_ref[...], gate), times(row_ref[...], up))
+
+    return pl.pallas_call(
+        body,
+        in_specs=[pl.BlockSpec(memory_space=pltpu.VMEM)] * 5,
+        out_specs=pl.BlockSpec(memory_space=pltpu.VMEM),
+        out_shape=pltpu.VMEM((count, 2 * hidden), jnp.bfloat16),
+        cost_estimate=cost(8 * count * width * hidden, 8 * width * hidden),
         compiler_params=pltpu.CompilerParams(vmem_limit_bytes=STEP_MIB * 2**20),
         name="last_units",
-    )(*map(far, rows), gate, up)
-
-
-def last_down(units, down, so_far, dtype):
+    )(row, *(a for shard in shards for a in shard))
+
+
+def joined(mine, given):
+    def body(mine_ref, given_ref, out_ref):
+        out_ref[...] = mine_ref[...] + given_ref[...]
+
+    return pl.pallas_call(
+        body,
+        in_specs=[pl.BlockSpec(memory_space=pltpu.VMEM)] * 2,
+        out_specs=pl.BlockSpec(memory_space=pltpu.VMEM),
+        out_shape=pltpu.VMEM(mine.shape, mine.dtype),
+        input_output_aliases={0: 0},
+        cost_estimate=cost(mine.size, 12 * mine.size),
+        compiler_params=pltpu.CompilerParams(vmem_limit_bytes=STEP_MIB * 2**20),
+        name="joined",
+    )(near(mine), given)
+
+
+def last_down(units, part, down, so_far, order, dtype):
     count, width = so_far.shape
+    hidden = down.shape[1]
+    rows = count // len(order)
 
     def body(units_ref, down_ref, old_ref, new_ref):
+        mine = units_ref[:, part * hidden : (part + 1) * hidden]
         for at in range(0, width, CUT):
-            added = times_t(units_ref[...], down_ref[at : at + CUT])
-            new_ref[:, at : at + CUT] = (old_ref[:, at : at + CUT] + added).astype(dtype)
-
-    return pl.pallas_call(
-        body,
-        in_specs=[pl.BlockSpec(memory_space=pltpu.VMEM)] * 3,
+            cut = slice(at, at + CUT)
+            total = (old_ref[:, cut] + times_t(mine, down_ref[cut])).astype(dtype)
+            for k, place in enumerate(order):
+                new_ref[k * rows : (k + 1) * rows, cut] = total[place * rows : (place + 1) * rows]
+
+    operands = (units, down, so_far)
+    return pl.pallas_call(
+        body,
+        in_specs=[pl.BlockSpec(memory_space=pltpu.VMEM)] * len(operands),
         out_specs=pl.BlockSpec(memory_space=pltpu.VMEM),
         out_shape=pltpu.VMEM((count, width), dtype),
         input_output_aliases={2: 0} if dtype == so_far.dtype else {},
-        cost_estimate=cost(2 * count * width * units.shape[1], 8 * count * width),
+        cost_estimate=cost(2 * count * width * hidden, 8 * count * width),
         compiler_params=pltpu.CompilerParams(vmem_limit_bytes=STEP_MIB * 2**20),
         name="last_down",
-    )(near(units), near(down), near(so_far))
-
-
-def both_cores(mine, theirs):
-    def body(mine_ref, theirs_ref, out_ref):
-        out_ref[...] = (mine_ref[...] + theirs_ref[...].astype(jnp.float32)).astype(jnp.bfloat16)
-
-    return pl.pallas_call(
-        body,
-        in_specs=[pl.BlockSpec(memory_space=pltpu.VMEM)] * 2,
-        out_specs=pl.BlockSpec(memory_space=pltpu.VMEM),
-        out_shape=pltpu.VMEM(mine.shape, jnp.bfloat16),
-        cost_estimate=cost(mine.size, 8 * mine.size),
-        compiler_params=pltpu.CompilerParams(vmem_limit_bytes=STEP_MIB * 2**20),
-        name="both_cores",
-    )(near(mine), near(theirs))
+    )(*map(near, operands))
 
 
 def z_ring(own):
@@ -409,6 +429,14 @@
         fore, aft = moved(fore, 1), moved(aft, -1)
         found.append([fore, aft])
     return found, moved(fore, 1)
+
+
+def interleaved(count):
+    side = math.isqrt(count)
+    key = lambda i: sum(
+        ((i % side >> b & 1) << 2 * b) | ((i // side >> b & 1) << 2 * b + 1) for b in range(side)
+    )
+    return sorted(range(count), key=key)
 
 
 def expert_half(
@@ -426,13 +454,14 @@
     slot_count = 3 * route_count * token_count // (2 * expert_count)
     own = [specialist_switch_maps[0], specialist_widen_maps[0], specialist_shrink_maps[0]]
     found, opposite = z_ring(own)
+    order = interleaved(expert_count)
     outgoing, back = token_rows(
         dispatched_group_activity,
         specialist_rmsgain[None, :],
         selected_specialist_ids.T,
         selected_specialist_share.T,
-        expert_count,
         slot_count,
+        order,
     )
 
     def exchange(rows):
@@ -445,14 +474,24 @@
     lent = other_core(kept)
     found[0].append(own)
     partial = ()
-    for shards in found:
-        partial = expert_step((lent, kept), shards, tuple(partial))
-    lent_units, kept_units = last_units((lent, kept), *opposite[:2])
-    sent = last_down(lent_units, opposite[2], partial[0], jnp.bfloat16)
-    given = other_core(sent)
-    mine = last_down(kept_units, opposite[2], partial[1], jnp.float32)
-    result = both_cores(mine, given)
-    return weighted_sum(back, exchange(result))
+    for r, shards in enumerate(found):
+        leaving = (0,) if r + 1 == len(found) else ()
+        partial = expert_step((lent, kept), shards, tuple(partial), leaving)
+    given = other_core(partial[0])
+    theirs = [other_core(a) for a in opposite]
+    units = last_units(kept, [opposite[:2], theirs[:2]])
+    mine = joined(partial[1], given)
+    mine = last_down(units, 0, opposite[2], mine, (0,), jnp.float32)
+    result = last_down(units, 1, theirs[2], mine, order, jnp.bfloat16)
+    returned = lax.all_to_all(
+        result.reshape(expert_count, slot_count, model_width),
+        "ep",
+        split_axis=0,
+        concat_axis=0,
+        tiled=True,
+        axis_index_groups=[order],
+    ).reshape(expert_count * slot_count, model_width)
+    return weighted_sum(back, returned)
 
 
 def on_device(

time: 229 us -> 211 us (0.921)
  waiting for transfers between devices: 105 us -> 92.8 us
  local copies, waits for them, and re-layouts: 17.9 us -> 13 us
  starting transfers between devices: 63.8 us -> 61 us
    all_to_all x0 -> x1, waiting for transfers between devices: none -> 21.2 us  [expert_half(): lax.all_to_all(result.reshape(expert_count, slot_count, model_width), 'ep...]
    all_to_all x2 -> x1, waiting for transfers between devices: 23.2 us -> 7.3 us  [exchange(): lax.all_to_all(blocks, 'ep', split_axis=0, concat_axis=0, tiled=True)]
    ppermute x21, waiting for transfers between devices: 66.7 us -> 57.8 us  [along_z(): lax.ppermute(x, 'tp', [(i, (i + (2 * by if i % 2 == 0 else -2 * by)) % tp...]
    ppermute x21, starting transfers between devices: 34 us -> 27.3 us  [along_z(): lax.ppermute(x, 'tp', [(i, (i + (2 * by if i % 2 == 0 else -2 * by)) % tp...]
    all_to_all x1, waiting for transfers between devices: 7.15 us -> 0.78 us  [mixer_half(): lax.all_to_all(pieces, 'tp', split_axis=0, concat_axis=0, tiled=True)]
    unnamed x44 -> x32, local copies, waits for them, and re-layouts: 15.9 us -> 11.6 us
    ppermute x2 -> x5, starting transfers between devices: 0.01 us -> 3.99 us  [other_core(): return lax.ppermute(x, 'tp', [(i, i ^ 1) for i in range(tp)])]
    all_to_all x2 -> x1, starting transfers between devices: 11.3 us -> 7.56 us  [exchange(): lax.all_to_all(blocks, 'ep', split_axis=0, concat_axis=0, tiled=True)]
  transfers between devices with their start and end apart: 28 -> 31, of which waited for: 16 -> 16; matrix products, arithmetic and copies ran while one was open for 2% -> 2% of each run, Pallas kernels for 13% -> 14%
where the time goes in v3:
time: 211 us; the launch traced here: 210 us
  waiting for transfers between devices  92.8 us (44%)
  starting transfers between devices  61 us (29%)
  Pallas kernels  38.9 us (18%)
  local copies, waits for them, and re-layouts  13 us (6%)
  matrix products  3.82 us (2%)
    ppermute x21, waiting for transfers between devices, along_z(): lax.ppermute(x, 'tp', [(i, (i + (2 * by if i % 2 == 0 else -2 * by)) % tp...  57.8 us
    ppermute x21, starting transfers between devices, along_z(): lax.ppermute(x, 'tp', [(i, (i + (2 * by if i % 2 == 0 else -2 * by)) % tp...  27.3 us
    all_to_all x1, waiting for transfers between devices, expert_half(): lax.all_to_all(result.reshape(expert_count, slot_count, model_width), 'ep...  21.2 us
    pallas_call x3, Pallas kernels, expert_step(): pl.pallas_call(body, in_specs=[pl.BlockSpec(memory_space=pltpu.VMEM)] * (...  18.2 us
    unnamed x32, local copies, waits for them, and re-layouts  11.6 us
    all_to_all x1, starting transfers between devices, mixer_half(): lax.all_to_all(pieces, 'tp', split_axis=0, concat_axis=0, tiled=True)  7.75 us
    all_to_all x1, starting transfers between devices, exchange(): lax.all_to_all(blocks, 'ep', split_axis=0, concat_axis=0, tiled=True)  7.56 us
    all_to_all x1, starting transfers between devices, swapped(): return lax.all_to_all(x, axis, split_axis=0, concat_axis=0, tiled=True)  7.41 us
  transfers between devices with their start and end apart: 31, of which 16 were waited for; matrix products, arithmetic and copies ran while one was open for 2% of the time, Pallas kernels for 14%

profile of v3, /device:TPU:1, one launch (start us, length us, event | category | flops | bytes accessed | tf_op | source)
XLA Modules:
  0.0 210.4 jit_solution(9720774269969026025)
XLA Ops:
  0.6 0.7 broadcast_in_dim.15.gain_ref
  1.3 3.1 %token_rows.1 = (bf16[384,2048]{1,0:T(8,128)(2,1)}, bf16[3,128,384]{2,1,0:T(8,128)(2,1)S(1)}) custom-call(bf16[128,2048]{1,0:T(8,128)(2,1)} %act_ref.1, bf16[1,2048]{1,0:T(2,128)(2,1)S(1)} %broadcast_in_dim.15.gain_ref, s32[2,128]{1,0:T(2,128)} %bitcast.38, f32[2,128]{1,0:T(2,128)} %bitcast.39), custom_call_target="tpu_custom_call" | custom-call | flops 1000000000 | bytes 2000000 | tf_op jit(solution)/shard_map/token_rows/pallas_call | solution.py:262
  4.5 7.6 %all-to-all-start.2 = ((bf16[16,24,2048]{2,1,0:T(8,128)(2,1)}), bf16[16,24,2048]{2,1,0:T(8,128)(2,1)S(1)}, u32[]{:S(2)}, u32[]{:S(2)}) async-start(bf16[16,24,2048]{2,1,0:T(8,128)(2,1)} %bitcast.9), calls=%async_computation.2 | async-start | bytes 3145728 | tf_op jit(solution)/shard_map/all_to_all | solution.py:469
  12.0 5.7 %collective-permute-start.1 = (bf16[2048,128]{1,0:T(8,128)(2,1)S(1)}, bf16[2048,128]{1,0:T(8,128)(2,1)}, u32[]{:S(2)}, u32[]{:S(2)}) collective-permute-start(bf16[2048,128]{1,0:T(8,128)(2,1)S(1)} %bitcast.26), channel_id=1, source_target_pairs={{0,2},{1,15},{2,4},{3,1},{4,6},{5,3},{6,8},{7,5},{8,10},{9,7},{10,... | collective-permute-start | bytes 1572872 | tf_op jit(solution)/shard_map/ppermute | solution.py:29
  17.7 0.7 collective-permute-start.11
  18.4 0.7 collective-permute-start.17
  19.3 8.6 %collective-permute-done.1.refs_2_ = bf16[2048,128]{1,0:T(8,128)(2,1)} collective-permute-done((bf16[2048,128]{1,0:T(8,128)(2,1)S(1)}, bf16[2048,128]{1,0:T(8,128)(2,1)}, u32[]{:S(2)}, u32[]{:S(2)}) %collective-permute-start.1) | collective-permute-done | bytes 524320 | tf_op jit(solution)/shard_map/ppermute | solution.py:29
  27.8 7.3 %all-to-all-done.2 = bf16[16,24,2048]{2,1,0:T(8,128)(2,1)S(1)} async-done(((bf16[16,24,2048]{2,1,0:T(8,128)(2,1)}), bf16[16,24,2048]{2,1,0:T(8,128)(2,1)S(1)}, u32[]{:S(2)}, u32[]{:S(2)}) %all-to-all-start.2) | async-done | bytes 1572896 | tf_op jit(solution)/shard_map/all_to_all | solution.py:469
  35.1 2.4 %collective-permute-start.16 = (bf16[384,2048]{1,0:T(8,128)(2,1)S(1)}, bf16[384,2048]{1,0:T(8,128)(2,1)S(1)}, u32[]{:S(2)}, u32[]{:S(2)}) collective-permute-start(bf16[384,2048]{1,0:T(8,128)(2,1)S(1)} %bitcast.18), channel_id=1, source_target_pairs={{0,1},{1,0},{2,3},{3,2},{4,5},{5,4},{6,7},{7,6},{8,9},{9,8},{10,11... | collective-permute-start | bytes 4718600 | tf_op jit(solution)/shard_map/ppermute | solution.py:34
  37.5 1.5 collective-permute-done.11.refs_4_
  39.0 4.0 %collective-permute-start.5 = (bf16[2048,128]{1,0:T(8,128)(2,1)S(1)}, bf16[2048,128]{1,0:T(8,128)(2,1)S(1)}, u32[]{:S(2)}, u32[]{:S(2)}) collective-permute-start(bf16[2048,128]{1,0:T(8,128)(2,1)S(1)} %bitcast.30), channel_id=1, source_target_pairs={{0,2},{1,15},{2,4},{3,1},{4,6},{5,3},{6,8},{7,5},{8,10},{9,7},{10,... | collective-permute-start | bytes 1572872 | tf_op jit(solution)/shard_map/ppermute | solution.py:29
  43.1 0.7 collective-permute-start.12
  43.8 0.7 collective-permute-start.18
  44.6 5.6 %collective-permute-done.23.refs_7_ = bf16[2048,128]{1,0:T(8,128)(2,1)} collective-permute-done((bf16[2048,128]{1,0:T(8,128)(2,1)S(1)}, bf16[2048,128]{1,0:T(8,128)(2,1)}, u32[]{:S(2)}, u32[]{:S(2)}) %collective-permute-start.23) | collective-permute-done | bytes 524320 | tf_op jit(solution)/shard_map/ppermute | solution.py:29
  50.2 1.8 collective-permute-start.2
  52.0 2.8 %collective-permute-done.5.refs_3_ = bf16[2048,128]{1,0:T(8,128)(2,1)S(1)} collective-permute-done((bf16[2048,128]{1,0:T(8,128)(2,1)S(1)}, bf16[2048,128]{1,0:T(8,128)(2,1)S(1)}, u32[]{:S(2)}, u32[]{:S(2)}) %collective-permute-start.5) | collective-permute-done | bytes 524320 | tf_op jit(solution)/shard_map/ppermute | solution.py:29
  54.8 10.8 %collective-permute-done.12.refs_4_ = bf16[2048,128]{1,0:T(8,128)(2,1)S(1)} collective-permute-done((bf16[2048,128]{1,0:T(8,128)(2,1)}, bf16[2048,128]{1,0:T(8,128)(2,1)S(1)}, u32[]{:S(2)}, u32[]{:S(2)}) %collective-permute-start.12) | collective-permute-done | bytes 524320 | tf_op jit(solution)/shard_map/ppermute | solution.py:29
  65.6 3.3 %collective-permute-start.6 = (bf16[2048,128]{1,0:T(8,128)(2,1)S(1)}, bf16[2048,128]{1,0:T(8,128)(2,1)S(1)}, u32[]{:S(2)}, u32[]{:S(2)}) collective-permute-start(bf16[2048,128]{1,0:T(8,128)(2,1)S(1)} %collective-permute-done.5.refs_3_), channel_id=1, source_target_pairs={{0,2},{1,15},{2,4},{3,1},{4,6},{5,3},{6,8},{7,5},{8,10},{9,7},{10,... | collective-permute-start | bytes 1572872 | tf_op jit(solution)/shard_map/ppermute | solution.py:29
  69.0 6.7 %collective-permute-done.2.refs_2_ = bf16[2048,128]{1,0:T(8,128)(2,1)S(1)} collective-permute-done((bf16[2048,128]{1,0:T(8,128)(2,1)}, bf16[2048,128]{1,0:T(8,128)(2,1)S(1)}, u32[]{:S(2)}, u32[]{:S(2)}) %collective-permute-start.2) | collective-permute-done | bytes 524320 | tf_op jit(solution)/shard_map/ppermute | solution.py:29
  75.7 3.3 %collective-permute-start.13 = (bf16[2048,128]{1,0:T(8,128)(2,1)S(1)}, bf16[2048,128]{1,0:T(8,128)(2,1)}, u32[]{:S(2)}, u32[]{:S(2)}) collective-permute-start(bf16[2048,128]{1,0:T(8,128)(2,1)S(1)} %collective-permute-done.12.refs_4_), channel_id=1, source_target_pairs={{0,2},{1,15},{2,4},{3,1},{4,6},{5,3},{6,8},{7,5},{8,10},{9,7},{10,... | collective-permute-start | bytes 1572872 | tf_op jit(solution)/shard_map/ppermute | solution.py:29
  79.0 6.6 %collective-permute-done.6.refs_3_ = bf16[2048,128]{1,0:T(8,128)(2,1)S(1)} collective-permute-done((bf16[2048,128]{1,0:T(8,128)(2,1)S(1)}, bf16[2048,128]{1,0:T(8,128)(2,1)S(1)}, u32[]{:S(2)}, u32[]{:S(2)}) %collective-permute-start.6) | collective-permute-done | bytes 524320 | tf_op jit(solution)/shard_map/ppermute | solution.py:29
  85.6 3.1 %collective-permute-start.7 = (bf16[2048,128]{1,0:T(8,128)(2,1)S(1)}, bf16[2048,128]{1,0:T(8,128)(2,1)}, u32[]{:S(2)}, u32[]{:S(2)}) collective-permute-start(bf16[2048,128]{1,0:T(8,128)(2,1)S(1)} %collective-permute-done.6.refs_3_), channel_id=1, source_target_pairs={{0,2},{1,15},{2,4},{3,1},{4,6},{5,3},{6,8},{7,5},{8,10},{9,7},{10,... | collective-permute-start | bytes 1572872 | tf_op jit(solution)/shard_map/ppermute | solution.py:29
  88.7 2.5 %collective-permute-done.13.refs_4_ = bf16[2048,128]{1,0:T(8,128)(2,1)} collective-permute-done((bf16[2048,128]{1,0:T(8,128)(2,1)S(1)}, bf16[2048,128]{1,0:T(8,128)(2,1)}, u32[]{:S(2)}, u32[]{:S(2)}) %collective-permute-start.13) | collective-permute-done | bytes 524320 | tf_op jit(solution)/shard_map/ppermute | solution.py:29
  91.3 0.2 collective-permute-start.25
  91.5 0.9 copy-done.15
  92.4 1.0 copy-done.6
  93.4 1.0 copy-done.8
  94.5 1.0 copy-done.10
  95.5 7.8 %shard_map.158 = (f32[384,2048]{1,0:T(8,128)S(1)}, f32[384,2048]{1,0:T(8,128)S(1)}) custom-call(bf16[384,2048]{1,0:T(8,128)(2,1)} %copy-done.15, bf16[384,2048]{1,0:T(8,128)(2,1)} %bitcast.19, bf16[2048,128]{1,0:T(8,128)(2,1)} %collective-permute-done.1.refs_2_, bf16[2048,128]{1,0:T(8,128)(2,1)S(1)} %collective-permute-done.5.refs_3_, ...), custom_call_target="tpu_custom_call" | custom-call | flops 3623878656 | bytes 4718592 | tf_op jit(solution)/shard_map/pallas_call | solution.py:342
  103.4 5.0 %shard_map.159 = (f32[384,2048]{1,0:T(8,128)S(1)}, f32[384,2048]{1,0:T(8,128)S(1)}) custom-call(bf16[384,2048]{1,0:T(8,128)(2,1)} %copy-done.15, bf16[384,2048]{1,0:T(8,128)(2,1)} %bitcast.20, bf16[2048,128]{1,0:T(8,128)(2,1)S(1)} %collective-permute-done.2.refs_2_, ...), custom_call_target="tpu_custom_call", output_to_operand_aliasing={{0}: (8, {}), {1}: (9, {})} | custom-call | flops 2415919104 | bytes 3145728 | tf_op jit(solution)/shard_map/pallas_call | solution.py:342
  108.3 4.8 %collective-permute-done.7.refs_3_ = bf16[2048,128]{1,0:T(8,128)(2,1)} collective-permute-done((bf16[2048,128]{1,0:T(8,128)(2,1)S(1)}, bf16[2048,128]{1,0:T(8,128)(2,1)}, u32[]{:S(2)}, u32[]{:S(2)}) %collective-permute-start.7) | collective-permute-done | bytes 524320 | tf_op jit(solution)/shard_map/ppermute | solution.py:29
  113.1 2.1 %collective-permute-done.22.refs_6_ = bf16[2048,128]{1,0:T(8,128)(2,1)S(1)} collective-permute-done((bf16[2048,128]{1,0:T(8,128)(2,1)S(1)}, bf16[2048,128]{1,0:T(8,128)(2,1)S(1)}, u32[]{:S(2)}, u32[]{:S(2)}) %collective-permute-start.22) | collective-permute-done | bytes 524320 | tf_op jit(solution)/shard_map/ppermute | solution.py:29
  115.2 5.7 %collective-permute-done.25.refs_7_ = bf16[2048,128]{1,0:T(8,128)(2,1)S(1)} collective-permute-done((bf16[2048,128]{1,0:T(8,128)(2,1)S(1)}, bf16[2048,128]{1,0:T(8,128)(2,1)S(1)}, u32[]{:S(2)}, u32[]{:S(2)}) %collective-permute-start.25) | collective-permute-done | bytes 524320 | tf_op jit(solution)/shard_map/ppermute | solution.py:29
  120.9 5.4 %shard_map.160 = (f32[384,2048]{1,0:T(8,128)}, f32[384,2048]{1,0:T(8,128)S(1)}) custom-call(bf16[384,2048]{1,0:T(8,128)(2,1)} %copy-done.15, bf16[384,2048]{1,0:T(8,128)(2,1)} %bitcast.21, bf16[2048,128]{1,0:T(8,128)(2,1)} %collective-permute-done.3.refs_2_, bf16[2048,128]{1,0:T(8,128)(2,1)} %collective-permute-done.7.refs_3_, ...), custom_call_target="tpu_custom_call", output_to_operand_aliasing={{1}: (9, {})} | custom-call | flops 2415919104 | bytes 3145728 | tf_op jit(solution)/shard_map/pallas_call | solution.py:342
  126.3 2.2 %collective-permute-start.8 = (bf16[2048,128]{1,0:T(8,128)(2,1)}, bf16[2048,128]{1,0:T(8,128)(2,1)}, u32[]{:S(2)}, u32[]{:S(2)}) collective-permute-start(bf16[2048,128]{1,0:T(8,128)(2,1)} %collective-permute-done.7.refs_3_), channel_id=1, source_target_pairs={{0,2},{1,15},{2,4},{3,1},{4,6},{5,3},{6,8},{7,5},{8,10},{9,7},{10,... | collective-permute-start | bytes 1572872 | tf_op jit(solution)/shard_map/ppermute | solution.py:29
  128.5 0.4 collective-permute-start.4
  128.9 0.2 collective-permute-start.14
  129.1 0.7 slice.3
  129.8 3.3 %collective-permute-start = (bf16[64,128]{1,0:T(8,128)(2,1)S(1)}, bf16[64,128]{1,0:T(8,128)(2,1)S(1)}, u32[]{:S(2)}, u32[]{:S(2)}) collective-permute-start(bf16[64,128]{1,0:T(8,128)(2,1)S(1)} %slice.3), channel_id=1, source_target_pairs={{0,16},{16,32},{32,48},{48,64},{64,80},{80,96},{96,112},{112,128},... | collective-permute-start | bytes 49160 | tf_op jit(solution)/shard_map/ppermute | solution.py:24
  133.1 0.8 collective-permute-done.halo_ref
  133.9 6.4 %local_scan.1 = (f32[64,2048]{1,0:T(8,128)S(1)}, f32[64,2048]{1,0:T(8,128)S(1)}, f32[16,8,128]{2,1,0:T(8,128)S(1)}) custom-call(s32[1]{0:T(128)} %bitcast.1.group_ref, bf16[64,2048]{1,0:T(8,128)(2,1)} %x_ref.1, bf16[64,128]{1,0:T(8,128)(2,1)S(1)} %collective-permute-done.halo_ref, bf16[4,1024]{1,0:T(4,128)(2,1)} %bitcast.35, bf16[16,64,64]{2,1,0:T(8,128)(2,1)} %rate_ref.1, ...), custom_call_target="tpu_custom_call" | custom-call | flops 4000000000 | bytes 2000000 | tf_op jit(solution)/shard_map/local_scan/pallas_call | solution.py:127
  140.3 0.6 copy-done.4
  140.9 0.8 copy-done.11
  141.7 0.8 copy-done.13
  142.5 7.4 %all-to-all-start = ((f32[16,8,128]{2,1,0:T(8,128)}), f32[16,8,128]{2,1,0:T(8,128)S(1)}, u32[]{:S(2)}, u32[]{:S(2)}) async-start(f32[16,8,128]{2,1,0:T(8,128)} %copy-done.4), calls=%async_computation | async-start | bytes 131072 | tf_op jit(solution)/shard_map/all_to_all | solution.py:18
  149.9 1.1 collective-permute-start.10
  151.1 0.4 collective-permute-start.15
  151.5 4.9 %all-to-all-done.totals_ref = f32[16,8,128]{2,1,0:T(8,128)S(1)} async-done(((f32[16,8,128]{2,1,0:T(8,128)}), f32[16,8,128]{2,1,0:T(8,128)S(1)}, u32[]{:S(2)}, u32[]{:S(2)}) %all-to-all-start) | async-done | bytes 65568 | tf_op jit(solution)/shard_map/all_to_all | solution.py:18
  156.4 1.0 copy-done.12
  157.5 1.0 copy-done.14
  158.5 1.2 gated_states.1
  159.8 0.7 copy-done.3
  160.5 7.7 %all-to-all-start.1 = ((bf16[16,64,128]{2,1,0:T(8,128)(2,1)}), bf16[16,64,128]{2,1,0:T(8,128)(2,1)}, u32[]{:S(2)}, u32[]{:S(2)}) async-start(bf16[16,64,128]{2,1,0:T(8,128)(2,1)} %copy-done.3), calls=%async_computation.1 | async-start | bytes 524288 | tf_op jit(solution)/shard_map/all_to_all | solution.py:219
  168.2 1.4 copy-done.1
  169.6 2.5 %last_units.1.units_ref = bf16[384,256]{1,0:T(8,128)(2,1)S(1)} custom-call(bf16[384,2048]{1,0:T(8,128)(2,1)S(1)} %bitcast.22, bf16[2048,128]{1,0:T(8,128)(2,1)} %collective-permute-done.4.refs_0_, bf16[2048,128]{1,0:T(8,128)(2,1)} %collective-permute-done.8.refs_1_, bf16[2048,128]{1,0:T(8,128)(2,1)} %collective-permute-done.9.refs_2_, ...), custom_call_target="tpu_custom_call" | custom-call | flops 805306368 | bytes 2097152 | tf_op jit(solution)/shard_map/last_units/pallas_call | solution.py:368
  172.2 2.4 %joined.1.old_ref = f32[384,2048]{1,0:T(8,128)S(1)} custom-call(f32[384,2048]{1,0:T(8,128)S(1)} %get-tuple-element.22.mine_ref, f32[384,2048]{1,0:T(8,128)} %collective-permute-done.26.given_ref), custom_call_target="tpu_custom_call", output_to_operand_aliasing={{}: (0, {})} | custom-call | flops 786432 | bytes 9437184 | tf_op jit(solution)/shard_map/joined/pallas_call | solution.py:383
  174.6 1.7 last_down.2.old_ref
  176.3 1.6 last_down.3
  178.0 1.2 copy-done.2
  179.1 0.8 all-to-all-done.1
  179.9 3.7 %all-to-all-start.3 = ((bf16[16,24,2048]{2,1,0:T(8,128)(2,1)}), bf16[16,24,2048]{2,1,0:T(8,128)(2,1)S(1)}, u32[]{:S(2)}, u32[]{:S(2)}) async-start(bf16[16,24,2048]{2,1,0:T(8,128)(2,1)} %bitcast.24), calls=%async_computation.3 | async-start | bytes 3145728 | tf_op jit(solution)/shard_map/all_to_all | solution.py:486
  183.6 3.8 %convolution_convert_fusion = bf16[128,2048]{1,0:T(8,128)(2,1)} fusion(bf16[1024,128]{1,0:T(8,128)(2,1)} %bitcast.5, bf16[1024,2048]{1,0:T(8,128)(2,1)} %param.22), kind=kOutput, calls=%fused_computation | convolution fusion | flops 537133056 | bytes 4980736 | tf_op jit(solution)/shard_map/dot_general | solution.py:220
  187.4 21.2 %all-to-all-done.3 = bf16[16,24,2048]{2,1,0:T(8,128)(2,1)S(1)} async-done(((bf16[16,24,2048]{2,1,0:T(8,128)(2,1)}), bf16[16,24,2048]{2,1,0:T(8,128)(2,1)S(1)}, u32[]{:S(2)}, u32[]{:S(2)}) %all-to-all-start.3) | async-done | bytes 1572896 | tf_op jit(solution)/shard_map/all_to_all | solution.py:486
  208.6 1.8 weighted_sum.1
  (44 shorter events, 0.3 us)
Async XLA Ops:
  1.3 10.7 %copy-start.5 = (bf16[1,2048,128]{2,1,0:T(8,128)(2,1)S(1)}, bf16[1,2048,128]{2,1,0:T(8,128)(2,1)}, u32[]{:S(2)}) copy-start(bf16[1,2048,128]{2,1,0:T(8,128)(2,1)} %param.27) | copy-start | bytes 1572868
  1.3 16.4 %copy-start.9 = (bf16[1,2048,128]{2,1,0:T(8,128)(2,1)S(1)}, bf16[1,2048,128]{2,1,0:T(8,128)(2,1)}, u32[]{:S(2)}) copy-start(bf16[1,2048,128]{2,1,0:T(8,128)(2,1)} %param.29) | copy-start | bytes 1572868
  1.3 17.8 %copy-start.7 = (bf16[1,2048,128]{2,1,0:T(8,128)(2,1)S(1)}, bf16[1,2048,128]{2,1,0:T(8,128)(2,1)}, u32[]{:S(2)}) copy-start(bf16[1,2048,128]{2,1,0:T(8,128)(2,1)} %param.28) | copy-start | bytes 1572868
  4.5 30.7 %all-to-all-start.2 = ((bf16[16,24,2048]{2,1,0:T(8,128)(2,1)}), bf16[16,24,2048]{2,1,0:T(8,128)(2,1)S(1)}, u32[]{:S(2)}, u32[]{:S(2)}) async-start(bf16[16,24,2048]{2,1,0:T(8,128)(2,1)} %bitcast.9), calls=%async_computation.2 | async-start | bytes 3145728 | tf_op jit(solution)/shard_map/all_to_all | solution.py:469
  12.0 15.8 %collective-permute-start.1 = (bf16[2048,128]{1,0:T(8,128)(2,1)S(1)}, bf16[2048,128]{1,0:T(8,128)(2,1)}, u32[]{:S(2)}, u32[]{:S(2)}) collective-permute-start(bf16[2048,128]{1,0:T(8,128)(2,1)S(1)} %bitcast.26), channel_id=1, source_target_pairs={{0,2},{1,15},{2,4},{3,1},{4,6},{5,3},{6,8},{7,5},{8,10},{9,7},{10,... | collective-permute-start | bytes 1572872 | tf_op jit(solution)/shard_map/ppermute | solution.py:29
  17.7 21.4 %collective-permute-start.11 = (bf16[2048,128]{1,0:T(8,128)(2,1)S(1)}, bf16[2048,128]{1,0:T(8,128)(2,1)}, u32[]{:S(2)}, u32[]{:S(2)}) collective-permute-start(bf16[2048,128]{1,0:T(8,128)(2,1)S(1)} %bitcast.32), channel_id=1, source_target_pairs={{0,2},{1,15},{2,4},{3,1},{4,6},{5,3},{6,8},{7,5},{8,10},{9,7},{10,... | collective-permute-start | bytes 1572872 | tf_op jit(solution)/shard_map/ppermute | solution.py:29
  18.4 24.7 %collective-permute-start.17 = (bf16[2048,128]{1,0:T(8,128)(2,1)S(1)}, bf16[2048,128]{1,0:T(8,128)(2,1)}, u32[]{:S(2)}, u32[]{:S(2)}) collective-permute-start(bf16[2048,128]{1,0:T(8,128)(2,1)S(1)} %bitcast.27), channel_id=1, source_target_pairs={{0,14},{1,3},{2,0},{3,5},{4,2},{5,7},{6,4},{7,9},{8,6},{9,11},{10,... | collective-permute-start | bytes 1572872 | tf_op jit(solution)/shard_map/ppermute | solution.py:29
  19.2 24.7 %collective-permute-start.20 = (bf16[2048,128]{1,0:T(8,128)(2,1)S(1)}, bf16[2048,128]{1,0:T(8,128)(2,1)}, u32[]{:S(2)}, u32[]{:S(2)}) collective-permute-start(bf16[2048,128]{1,0:T(8,128)(2,1)S(1)} %bitcast.29), channel_id=1, source_target_pairs={{0,14},{1,3},{2,0},{3,5},{4,2},{5,7},{6,4},{7,9},{8,6},{9,11},{10,... | collective-permute-start | bytes 1572872 | tf_op jit(solution)/shard_map/ppermute | solution.py:29
  19.2 31.0 %collective-permute-start.23 = (bf16[2048,128]{1,0:T(8,128)(2,1)S(1)}, bf16[2048,128]{1,0:T(8,128)(2,1)}, u32[]{:S(2)}, u32[]{:S(2)}) collective-permute-start(bf16[2048,128]{1,0:T(8,128)(2,1)S(1)} %bitcast.33), channel_id=1, source_target_pairs={{0,14},{1,3},{2,0},{3,5},{4,2},{5,7},{6,4},{7,9},{8,6},{9,11},{10,... | collective-permute-start | bytes 1572872 | tf_op jit(solution)/shard_map/ppermute | solution.py:29
  35.1 56.1 %copy-start = (bf16[16,24,2048]{2,1,0:T(8,128)(2,1)}, bf16[16,24,2048]{2,1,0:T(8,128)(2,1)S(1)}, u32[]{:S(2)}) copy-start(bf16[16,24,2048]{2,1,0:T(8,128)(2,1)S(1)} %all-to-all-done.2) | copy-start | bytes 4718596
  35.1 56.1 %collective-permute-start.16 = (bf16[384,2048]{1,0:T(8,128)(2,1)S(1)}, bf16[384,2048]{1,0:T(8,128)(2,1)S(1)}, u32[]{:S(2)}, u32[]{:S(2)}) collective-permute-start(bf16[384,2048]{1,0:T(8,128)(2,1)S(1)} %bitcast.18), channel_id=1, source_target_pairs={{0,1},{1,0},{2,3},{3,2},{4,5},{5,4},{6,7},{7,6},{8,9},{9,8},{10,11... | collective-permute-start | bytes 4718600 | tf_op jit(solution)/shard_map/ppermute | solution.py:34
  39.0 15.8 %collective-permute-start.5 = (bf16[2048,128]{1,0:T(8,128)(2,1)S(1)}, bf16[2048,128]{1,0:T(8,128)(2,1)S(1)}, u32[]{:S(2)}, u32[]{:S(2)}) collective-permute-start(bf16[2048,128]{1,0:T(8,128)(2,1)S(1)} %bitcast.30), channel_id=1, source_target_pairs={{0,2},{1,15},{2,4},{3,1},{4,6},{5,3},{6,8},{7,5},{8,10},{9,7},{10,... | collective-permute-start | bytes 1572872 | tf_op jit(solution)/shard_map/ppermute | solution.py:29
  43.1 22.6 %collective-permute-start.12 = (bf16[2048,128]{1,0:T(8,128)(2,1)}, bf16[2048,128]{1,0:T(8,128)(2,1)S(1)}, u32[]{:S(2)}, u32[]{:S(2)}) collective-permute-start(bf16[2048,128]{1,0:T(8,128)(2,1)} %collective-permute-done.11.refs_4_), channel_id=1, source_target_pairs={{0,2},{1,15},{2,4},{3,1},{4,6},{5,3},{6,8},{7,5},{8,10},{9,7},{10,... | collective-permute-start | bytes 1572872 | tf_op jit(solution)/shard_map/ppermute | solution.py:29
  43.8 25.1 %collective-permute-start.18 = (bf16[2048,128]{1,0:T(8,128)(2,1)}, bf16[2048,128]{1,0:T(8,128)(2,1)S(1)}, u32[]{:S(2)}, u32[]{:S(2)}) collective-permute-start(bf16[2048,128]{1,0:T(8,128)(2,1)} %collective-permute-done.17.refs_5_), channel_id=1, source_target_pairs={{0,14},{1,3},{2,0},{3,5},{4,2},{5,7},{6,4},{7,9},{8,6},{9,11},{10,... | collective-permute-start | bytes 1572872 | tf_op jit(solution)/shard_map/ppermute | solution.py:29
  50.2 25.5 %collective-permute-start.2 = (bf16[2048,128]{1,0:T(8,128)(2,1)}, bf16[2048,128]{1,0:T(8,128)(2,1)S(1)}, u32[]{:S(2)}, u32[]{:S(2)}) collective-permute-start(bf16[2048,128]{1,0:T(8,128)(2,1)} %collective-permute-done.1.refs_2_), channel_id=1, source_target_pairs={{0,2},{1,15},{2,4},{3,1},{4,6},{5,3},{6,8},{7,5},{8,10},{9,7},{10,... | collective-permute-start | bytes 1572872 | tf_op jit(solution)/shard_map/ppermute | solution.py:29
  54.8 24.1 %collective-permute-start.21 = (bf16[2048,128]{1,0:T(8,128)(2,1)}, bf16[2048,128]{1,0:T(8,128)(2,1)S(1)}, u32[]{:S(2)}, u32[]{:S(2)}) collective-permute-start(bf16[2048,128]{1,0:T(8,128)(2,1)} %collective-permute-done.20.refs_6_), channel_id=1, source_target_pairs={{0,14},{1,3},{2,0},{3,5},{4,2},{5,7},{6,4},{7,9},{8,6},{9,11},{10,... | collective-permute-start | bytes 1572872 | tf_op jit(solution)/shard_map/ppermute | solution.py:29
  65.6 20.0 %collective-permute-start.6 = (bf16[2048,128]{1,0:T(8,128)(2,1)S(1)}, bf16[2048,128]{1,0:T(8,128)(2,1)S(1)}, u32[]{:S(2)}, u32[]{:S(2)}) collective-permute-start(bf16[2048,128]{1,0:T(8,128)(2,1)S(1)} %collective-permute-done.5.refs_3_), channel_id=1, source_target_pairs={{0,2},{1,15},{2,4},{3,1},{4,6},{5,3},{6,8},{7,5},{8,10},{9,7},{10,... | collective-permute-start | bytes 1572872 | tf_op jit(solution)/shard_map/ppermute | solution.py:29
  68.9 19.8 %collective-permute-start.24 = (bf16[2048,128]{1,0:T(8,128)(2,1)}, bf16[2048,128]{1,0:T(8,128)(2,1)S(1)}, u32[]{:S(2)}, u32[]{:S(2)}) collective-permute-start(bf16[2048,128]{1,0:T(8,128)(2,1)} %collective-permute-done.23.refs_7_), channel_id=1, source_target_pairs={{0,14},{1,3},{2,0},{3,5},{4,2},{5,7},{6,4},{7,9},{8,6},{9,11},{10,... | collective-permute-start | bytes 1572872 | tf_op jit(solution)/shard_map/ppermute | solution.py:29
  75.7 15.6 %collective-permute-start.13 = (bf16[2048,128]{1,0:T(8,128)(2,1)S(1)}, bf16[2048,128]{1,0:T(8,128)(2,1)}, u32[]{:S(2)}, u32[]{:S(2)}) collective-permute-start(bf16[2048,128]{1,0:T(8,128)(2,1)S(1)} %collective-permute-done.12.refs_4_), channel_id=1, source_target_pairs={{0,2},{1,15},{2,4},{3,1},{4,6},{5,3},{6,8},{7,5},{8,10},{9,7},{10,... | collective-permute-start | bytes 1572872 | tf_op jit(solution)/shard_map/ppermute | solution.py:29
  79.0 29.4 %collective-permute-start.3 = (bf16[2048,128]{1,0:T(8,128)(2,1)S(1)}, bf16[2048,128]{1,0:T(8,128)(2,1)}, u32[]{:S(2)}, u32[]{:S(2)}) collective-permute-start(bf16[2048,128]{1,0:T(8,128)(2,1)S(1)} %collective-permute-done.2.refs_2_), channel_id=1, source_target_pairs={{0,2},{1,15},{2,4},{3,1},{4,6},{5,3},{6,8},{7,5},{8,10},{9,7},{10,... | collective-permute-start | bytes 1572872 | tf_op jit(solution)/shard_map/ppermute | solution.py:29
  85.6 27.5 %collective-permute-start.7 = (bf16[2048,128]{1,0:T(8,128)(2,1)S(1)}, bf16[2048,128]{1,0:T(8,128)(2,1)}, u32[]{:S(2)}, u32[]{:S(2)}) collective-permute-start(bf16[2048,128]{1,0:T(8,128)(2,1)S(1)} %collective-permute-done.6.refs_3_), channel_id=1, source_target_pairs={{0,2},{1,15},{2,4},{3,1},{4,6},{5,3},{6,8},{7,5},{8,10},{9,7},{10,... | collective-permute-start | bytes 1572872 | tf_op jit(solution)/shard_map/ppermute | solution.py:29
  88.7 24.4 %collective-permute-start.19 = (bf16[2048,128]{1,0:T(8,128)(2,1)S(1)}, bf16[2048,128]{1,0:T(8,128)(2,1)S(1)}, u32[]{:S(2)}, u32[]{:S(2)}) collective-permute-start(bf16[2048,128]{1,0:T(8,128)(2,1)S(1)} %collective-permute-done.18.refs_5_), channel_id=1, source_target_pairs={{0,14},{1,3},{2,0},{3,5},{4,2},{5,7},{6,4},{7,9},{8,6},{9,11},{10,... | collective-permute-start | bytes 1572872 | tf_op jit(solution)/shard_map/ppermute | solution.py:29
  91.2 24.0 %collective-permute-start.22 = (bf16[2048,128]{1,0:T(8,128)(2,1)S(1)}, bf16[2048,128]{1,0:T(8,128)(2,1)S(1)}, u32[]{:S(2)}, u32[]{:S(2)}) collective-permute-start(bf16[2048,128]{1,0:T(8,128)(2,1)S(1)} %collective-permute-done.21.refs_6_), channel_id=1, source_target_pairs={{0,14},{1,3},{2,0},{3,5},{4,2},{5,7},{6,4},{7,9},{8,6},{9,11},{10,... | collective-permute-start | bytes 1572872 | tf_op jit(solution)/shard_map/ppermute | solution.py:29
  91.2 1.2 copy-start.15
  91.3 29.7 %collective-permute-start.25 = (bf16[2048,128]{1,0:T(8,128)(2,1)S(1)}, bf16[2048,128]{1,0:T(8,128)(2,1)S(1)}, u32[]{:S(2)}, u32[]{:S(2)}) collective-permute-start(bf16[2048,128]{1,0:T(8,128)(2,1)S(1)} %collective-permute-done.24.refs_7_), channel_id=1, source_target_pairs={{0,14},{1,3},{2,0},{3,5},{4,2},{5,7},{6,4},{7,9},{8,6},{9,11},{10,... | collective-permute-start | bytes 1572872 | tf_op jit(solution)/shard_map/ppermute | solution.py:29
  92.4 1.0 copy-start.6
  93.4 1.0 copy-start.8
  94.5 1.0 copy-start.10
  126.3 45.8 %collective-permute-start.26 = (f32[384,2048]{1,0:T(8,128)}, f32[384,2048]{1,0:T(8,128)}, u32[]{:S(2)}, u32[]{:S(2)}) collective-permute-start(f32[384,2048]{1,0:T(8,128)} %get-tuple-element.23), channel_id=1, source_target_pairs={{0,1},{1,0},{2,3},{3,2},{4,5},{5,4},{6,7},{7,6},{8,9},{9,8},{10,11... | collective-permute-start | bytes 9437192 | tf_op jit(solution)/shard_map/ppermute | solution.py:34
  126.3 23.6 %collective-permute-start.8 = (bf16[2048,128]{1,0:T(8,128)(2,1)}, bf16[2048,128]{1,0:T(8,128)(2,1)}, u32[]{:S(2)}, u32[]{:S(2)}) collective-permute-start(bf16[2048,128]{1,0:T(8,128)(2,1)} %collective-permute-done.7.refs_3_), channel_id=1, source_target_pairs={{0,2},{1,15},{2,4},{3,1},{4,6},{5,3},{6,8},{7,5},{8,10},{9,7},{10,... | collective-permute-start | bytes 1572872 | tf_op jit(solution)/shard_map/ppermute | solution.py:29
  128.5 22.5 %collective-permute-start.4 = (bf16[2048,128]{1,0:T(8,128)(2,1)}, bf16[2048,128]{1,0:T(8,128)(2,1)}, u32[]{:S(2)}, u32[]{:S(2)}) collective-permute-start(bf16[2048,128]{1,0:T(8,128)(2,1)} %collective-permute-done.3.refs_2_), channel_id=1, source_target_pairs={{0,2},{1,15},{2,4},{3,1},{4,6},{5,3},{6,8},{7,5},{8,10},{9,7},{10,... | collective-permute-start | bytes 1572872 | tf_op jit(solution)/shard_map/ppermute | solution.py:29
  128.9 22.2 %collective-permute-start.14 = (bf16[2048,128]{1,0:T(8,128)(2,1)}, bf16[2048,128]{1,0:T(8,128)(2,1)}, u32[]{:S(2)}, u32[]{:S(2)}) collective-permute-start(bf16[2048,128]{1,0:T(8,128)(2,1)} %collective-permute-done.13.refs_4_), channel_id=1, source_target_pairs={{0,2},{1,15},{2,4},{3,1},{4,6},{5,3},{6,8},{7,5},{8,10},{9,7},{10,... | collective-permute-start | bytes 1572872 | tf_op jit(solution)/shard_map/ppermute | solution.py:29
  129.8 4.1 %collective-permute-start = (bf16[64,128]{1,0:T(8,128)(2,1)S(1)}, bf16[64,128]{1,0:T(8,128)(2,1)S(1)}, u32[]{:S(2)}, u32[]{:S(2)}) collective-permute-start(bf16[64,128]{1,0:T(8,128)(2,1)S(1)} %slice.3), channel_id=1, source_target_pairs={{0,16},{16,32},{32,48},{48,64},{64,80},{80,96},{96,112},{112,128},... | collective-permute-start | bytes 49160 | tf_op jit(solution)/shard_map/ppermute | solution.py:24
  140.3 0.6 copy-start.4
  140.9 0.8 copy-start.11
  141.7 0.8 copy-start.13
  142.5 13.9 %all-to-all-start = ((f32[16,8,128]{2,1,0:T(8,128)}), f32[16,8,128]{2,1,0:T(8,128)S(1)}, u32[]{:S(2)}, u32[]{:S(2)}) async-start(f32[16,8,128]{2,1,0:T(8,128)} %copy-done.4), calls=%async_computation | async-start | bytes 131072 | tf_op jit(solution)/shard_map/all_to_all | solution.py:18
  149.9 18.3 %collective-permute-start.10 = (bf16[2048,128]{1,0:T(8,128)(2,1)}, bf16[2048,128]{1,0:T(8,128)(2,1)}, u32[]{:S(2)}, u32[]{:S(2)}) collective-permute-start(bf16[2048,128]{1,0:T(8,128)(2,1)} %collective-permute-done.8.refs_1_), channel_id=1, source_target_pairs={{0,1},{1,0},{2,3},{3,2},{4,5},{5,4},{6,7},{7,6},{8,9},{9,8},{10,11... | collective-permute-start | bytes 1572872 | tf_op jit(solution)/shard_map/ppermute | solution.py:34
  151.0 17.2 %collective-permute-start.9 = (bf16[2048,128]{1,0:T(8,128)(2,1)}, bf16[2048,128]{1,0:T(8,128)(2,1)}, u32[]{:S(2)}, u32[]{:S(2)}) collective-permute-start(bf16[2048,128]{1,0:T(8,128)(2,1)} %collective-permute-done.4.refs_0_), channel_id=1, source_target_pairs={{0,1},{1,0},{2,3},{3,2},{4,5},{5,4},{6,7},{7,6},{8,9},{9,8},{10,11... | collective-permute-start | bytes 1572872 | tf_op jit(solution)/shard_map/ppermute | solution.py:34
  151.1 25.2 %collective-permute-start.15 = (bf16[2048,128]{1,0:T(8,128)(2,1)}, bf16[2048,128]{1,0:T(8,128)(2,1)}, u32[]{:S(2)}, u32[]{:S(2)}) collective-permute-start(bf16[2048,128]{1,0:T(8,128)(2,1)} %collective-permute-done.14.down_ref), channel_id=1, source_target_pairs={{0,1},{1,0},{2,3},{3,2},{4,5},{5,4},{6,7},{7,6},{8,9},{9,8},{10,11... | collective-permute-start | bytes 1572872 | tf_op jit(solution)/shard_map/ppermute | solution.py:34
  156.4 1.0 copy-start.12
  157.5 1.0 copy-start.14
  159.8 0.7 copy-start.3
  160.5 19.4 %all-to-all-start.1 = ((bf16[16,64,128]{2,1,0:T(8,128)(2,1)}), bf16[16,64,128]{2,1,0:T(8,128)(2,1)}, u32[]{:S(2)}, u32[]{:S(2)}) async-start(bf16[16,64,128]{2,1,0:T(8,128)(2,1)} %copy-done.3), calls=%async_computation.1 | async-start | bytes 524288 | tf_op jit(solution)/shard_map/all_to_all | solution.py:219
  168.2 1.4 copy-start.1
  177.9 1.2 copy-start.2
  179.9 28.7 %all-to-all-start.3 = ((bf16[16,24,2048]{2,1,0:T(8,128)(2,1)}), bf16[16,24,2048]{2,1,0:T(8,128)(2,1)S(1)}, u32[]{:S(2)}, u32[]{:S(2)}) async-start(bf16[16,24,2048]{2,1,0:T(8,128)(2,1)} %bitcast.24), calls=%async_computation.3 | async-start | bytes 3145728 | tf_op jit(solution)/shard_map/all_to_all | solution.py:486

commit v4 on v3

--- a/solution.py
+++ b/solution.py
@@ -12,6 +12,7 @@
 TILES_AT_ONCE = 4
 CUT = 512
 STEP_MIB = 12
+SHARE_TERMS = 2
 
 
 def swapped(x, axis):
@@ -254,7 +255,7 @@
             back = back + jnp.where(slot == comes * slots + rank, share_ref[j : j + 1], 0.0)
         rows_ref[...] = times(taken.astype(jnp.bfloat16), normed).astype(jnp.bfloat16)
         rest = back.T
-        for k in range(3):
+        for k in range(SHARE_TERMS):
             part = rest.astype(jnp.bfloat16)
             back_ref[k] = part
             rest = rest - part.astype(jnp.float32)
@@ -263,7 +264,7 @@
         body,
         out_shape=[
             jax.ShapeDtypeStruct((experts * slots, width), jnp.bfloat16),
-            jax.ShapeDtypeStruct((3, tokens, experts * slots), jnp.bfloat16),
+            jax.ShapeDtypeStruct((SHARE_TERMS, tokens, experts * slots), jnp.bfloat16),
         ],
         cost_estimate=cost(10**9, 2 * 10**6),
         compiler_params=pltpu.CompilerParams(vmem_limit_bytes=12 * 2**20),
@@ -275,19 +276,31 @@
     parts, tokens, slots = back.shape
     width = results.shape[1]
 
-    def body(back_ref, results_ref, out_ref):
-        for at in range(0, width, CUT):
+    def body(back_ref, results_ref, out_ref, done_ref, sems):
+        copies = []
+        for k, at in enumerate(range(0, width, CUT)):
             cut = slice(at, at + CUT)
             each = times(back_ref[...], results_ref[:, cut])
             total = each[:tokens]
-            for k in range(1, parts):
-                total = total + each[k * tokens : (k + 1) * tokens]
-            out_ref[:, cut] = total.astype(jnp.bfloat16)
+            for p in range(1, parts):
+                total = total + each[p * tokens : (p + 1) * tokens]
+            done_ref[:, cut] = total.astype(jnp.bfloat16)
+            copies.append(
+                pltpu.make_async_copy(done_ref.at[:, cut], out_ref.at[:, cut], sems.at[k])
+            )
+            copies[-1].start()
+        for copy in copies:
+            copy.wait()
 
     return pl.pallas_call(
         body,
         in_specs=[pl.BlockSpec(memory_space=pltpu.VMEM)] * 2,
+        out_specs=pl.BlockSpec(memory_space=pl.ANY),
         out_shape=jax.ShapeDtypeStruct((tokens, width), jnp.bfloat16),
+        scratch_shapes=[
+            pltpu.VMEM((tokens, width), jnp.bfloat16),
+            pltpu.SemaphoreType.DMA((width // CUT,)),
+        ],
         cost_estimate=cost(2 * parts * tokens * slots * width, 2 * slots * width),
         compiler_params=pltpu.CompilerParams(vmem_limit_bytes=12 * 2**20),
         name="weighted_sum",

time: 211 us -> 211 us (level)
    unnamed x32 -> x28, local copies, waits for them, and re-layouts: 11.6 us -> 10.3 us
where the time goes in v4:
time: 211 us; the launch traced here: 210 us
  waiting for transfers between devices  92.8 us (44%)
  starting transfers between devices  61 us (29%)
  Pallas kernels  39.9 us (19%)
  local copies, waits for them, and re-layouts  11.7 us (6%)
  matrix products  3.82 us (2%)
    ppermute x21, waiting for transfers between devices, along_z(): lax.ppermute(x, 'tp', [(i, (i + (2 * by if i % 2 == 0 else -2 * by)) % tp...  57.8 us
    ppermute x21, starting transfers between devices, along_z(): lax.ppermute(x, 'tp', [(i, (i + (2 * by if i % 2 == 0 else -2 * by)) % tp...  27.3 us
    all_to_all x1, waiting for transfers between devices, expert_half(): lax.all_to_all(result.reshape(expert_count, slot_count, model_width), 'ep...  21.2 us
    pallas_call x3, Pallas kernels, expert_step(): pl.pallas_call(body, in_specs=[pl.BlockSpec(memory_space=pltpu.VMEM)] * (...  18.2 us
    unnamed x28, local copies, waits for them, and re-layouts  10.3 us
    all_to_all x1, starting transfers between devices, mixer_half(): lax.all_to_all(pieces, 'tp', split_axis=0, concat_axis=0, tiled=True)  7.75 us
    all_to_all x1, starting transfers between devices, exchange(): lax.all_to_all(blocks, 'ep', split_axis=0, concat_axis=0, tiled=True)  7.56 us
    all_to_all x1, starting transfers between devices, swapped(): return lax.all_to_all(x, axis, split_axis=0, concat_axis=0, tiled=True)  7.41 us
  transfers between devices with their start and end apart: 31, of which 16 were waited for; matrix products, arithmetic and copies ran while one was open for 2% of the time, Pallas kernels for 14%

profile of v4, /device:TPU:1, one launch (start us, length us, event | category | flops | bytes accessed | tf_op | source)
XLA Modules:
  0.0 210.2 jit_solution(9903144393172988529)
XLA Ops:
  0.6 0.7 broadcast_in_dim.15.gain_ref
  1.3 3.1 %token_rows.1 = (bf16[384,2048]{1,0:T(8,128)(2,1)}, bf16[2,128,384]{2,1,0:T(8,128)(2,1)S(1)}) custom-call(bf16[128,2048]{1,0:T(8,128)(2,1)} %act_ref.1, bf16[1,2048]{1,0:T(2,128)(2,1)S(1)} %broadcast_in_dim.15.gain_ref, s32[2,128]{1,0:T(2,128)} %bitcast.38, f32[2,128]{1,0:T(2,128)} %bitcast.39), custom_call_target="tpu_custom_call" | custom-call | flops 1000000000 | bytes 2000000 | tf_op jit(solution)/shard_map/token_rows/pallas_call | solution.py:263
  4.5 7.6 %all-to-all-start.2 = ((bf16[16,24,2048]{2,1,0:T(8,128)(2,1)}), bf16[16,24,2048]{2,1,0:T(8,128)(2,1)S(1)}, u32[]{:S(2)}, u32[]{:S(2)}) async-start(bf16[16,24,2048]{2,1,0:T(8,128)(2,1)} %bitcast.9), calls=%async_computation.2 | async-start | bytes 3145728 | tf_op jit(solution)/shard_map/all_to_all | solution.py:482
  12.0 5.7 %collective-permute-start.1 = (bf16[2048,128]{1,0:T(8,128)(2,1)S(1)}, bf16[2048,128]{1,0:T(8,128)(2,1)}, u32[]{:S(2)}, u32[]{:S(2)}) collective-permute-start(bf16[2048,128]{1,0:T(8,128)(2,1)S(1)} %bitcast.26), channel_id=1, source_target_pairs={{0,2},{1,15},{2,4},{3,1},{4,6},{5,3},{6,8},{7,5},{8,10},{9,7},{10,... | collective-permute-start | bytes 1572872 | tf_op jit(solution)/shard_map/ppermute | solution.py:30
  17.7 0.7 collective-permute-start.11
  18.4 0.7 collective-permute-start.17
  19.2 0.1 collective-permute-start.23
  19.2 8.6 %collective-permute-done.1.refs_2_ = bf16[2048,128]{1,0:T(8,128)(2,1)} collective-permute-done((bf16[2048,128]{1,0:T(8,128)(2,1)S(1)}, bf16[2048,128]{1,0:T(8,128)(2,1)}, u32[]{:S(2)}, u32[]{:S(2)}) %collective-permute-start.1) | collective-permute-done | bytes 524320 | tf_op jit(solution)/shard_map/ppermute | solution.py:30
  27.8 7.3 %all-to-all-done.2 = bf16[16,24,2048]{2,1,0:T(8,128)(2,1)S(1)} async-done(((bf16[16,24,2048]{2,1,0:T(8,128)(2,1)}), bf16[16,24,2048]{2,1,0:T(8,128)(2,1)S(1)}, u32[]{:S(2)}, u32[]{:S(2)}) %all-to-all-start.2) | async-done | bytes 1572896 | tf_op jit(solution)/shard_map/all_to_all | solution.py:482
  35.1 2.4 %collective-permute-start.16 = (bf16[384,2048]{1,0:T(8,128)(2,1)S(1)}, bf16[384,2048]{1,0:T(8,128)(2,1)S(1)}, u32[]{:S(2)}, u32[]{:S(2)}) collective-permute-start(bf16[384,2048]{1,0:T(8,128)(2,1)S(1)} %bitcast.18), channel_id=1, source_target_pairs={{0,1},{1,0},{2,3},{3,2},{4,5},{5,4},{6,7},{7,6},{8,9},{9,8},{10,11... | collective-permute-start | bytes 4718600 | tf_op jit(solution)/shard_map/ppermute | solution.py:35
  37.5 1.5 collective-permute-done.11.refs_4_
  39.0 4.0 %collective-permute-start.5 = (bf16[2048,128]{1,0:T(8,128)(2,1)S(1)}, bf16[2048,128]{1,0:T(8,128)(2,1)S(1)}, u32[]{:S(2)}, u32[]{:S(2)}) collective-permute-start(bf16[2048,128]{1,0:T(8,128)(2,1)S(1)} %bitcast.30), channel_id=1, source_target_pairs={{0,2},{1,15},{2,4},{3,1},{4,6},{5,3},{6,8},{7,5},{8,10},{9,7},{10,... | collective-permute-start | bytes 1572872 | tf_op jit(solution)/shard_map/ppermute | solution.py:30
  43.1 0.7 collective-permute-start.12
  43.8 0.7 collective-permute-start.18
  44.6 5.6 %collective-permute-done.23.refs_7_ = bf16[2048,128]{1,0:T(8,128)(2,1)} collective-permute-done((bf16[2048,128]{1,0:T(8,128)(2,1)S(1)}, bf16[2048,128]{1,0:T(8,128)(2,1)}, u32[]{:S(2)}, u32[]{:S(2)}) %collective-permute-start.23) | collective-permute-done | bytes 524320 | tf_op jit(solution)/shard_map/ppermute | solution.py:30
  50.2 1.8 collective-permute-start.2
  52.0 2.8 %collective-permute-done.5.refs_3_ = bf16[2048,128]{1,0:T(8,128)(2,1)S(1)} collective-permute-done((bf16[2048,128]{1,0:T(8,128)(2,1)S(1)}, bf16[2048,128]{1,0:T(8,128)(2,1)S(1)}, u32[]{:S(2)}, u32[]{:S(2)}) %collective-permute-start.5) | collective-permute-done | bytes 524320 | tf_op jit(solution)/shard_map/ppermute | solution.py:30
  54.8 10.8 %collective-permute-done.12.refs_4_ = bf16[2048,128]{1,0:T(8,128)(2,1)S(1)} collective-permute-done((bf16[2048,128]{1,0:T(8,128)(2,1)}, bf16[2048,128]{1,0:T(8,128)(2,1)S(1)}, u32[]{:S(2)}, u32[]{:S(2)}) %collective-permute-start.12) | collective-permute-done | bytes 524320 | tf_op jit(solution)/shard_map/ppermute | solution.py:30
  65.6 3.3 %collective-permute-start.6 = (bf16[2048,128]{1,0:T(8,128)(2,1)S(1)}, bf16[2048,128]{1,0:T(8,128)(2,1)S(1)}, u32[]{:S(2)}, u32[]{:S(2)}) collective-permute-start(bf16[2048,128]{1,0:T(8,128)(2,1)S(1)} %collective-permute-done.5.refs_3_), channel_id=1, source_target_pairs={{0,2},{1,15},{2,4},{3,1},{4,6},{5,3},{6,8},{7,5},{8,10},{9,7},{10,... | collective-permute-start | bytes 1572872 | tf_op jit(solution)/shard_map/ppermute | solution.py:30
  69.0 6.7 %collective-permute-done.2.refs_2_ = bf16[2048,128]{1,0:T(8,128)(2,1)S(1)} collective-permute-done((bf16[2048,128]{1,0:T(8,128)(2,1)}, bf16[2048,128]{1,0:T(8,128)(2,1)S(1)}, u32[]{:S(2)}, u32[]{:S(2)}) %collective-permute-start.2) | collective-permute-done | bytes 524320 | tf_op jit(solution)/shard_map/ppermute | solution.py:30
  75.7 3.3 %collective-permute-start.13 = (bf16[2048,128]{1,0:T(8,128)(2,1)S(1)}, bf16[2048,128]{1,0:T(8,128)(2,1)}, u32[]{:S(2)}, u32[]{:S(2)}) collective-permute-start(bf16[2048,128]{1,0:T(8,128)(2,1)S(1)} %collective-permute-done.12.refs_4_), channel_id=1, source_target_pairs={{0,2},{1,15},{2,4},{3,1},{4,6},{5,3},{6,8},{7,5},{8,10},{9,7},{10,... | collective-permute-start | bytes 1572872 | tf_op jit(solution)/shard_map/ppermute | solution.py:30
  79.0 6.6 %collective-permute-done.6.refs_3_ = bf16[2048,128]{1,0:T(8,128)(2,1)S(1)} collective-permute-done((bf16[2048,128]{1,0:T(8,128)(2,1)S(1)}, bf16[2048,128]{1,0:T(8,128)(2,1)S(1)}, u32[]{:S(2)}, u32[]{:S(2)}) %collective-permute-start.6) | collective-permute-done | bytes 524320 | tf_op jit(solution)/shard_map/ppermute | solution.py:30
  85.6 3.1 %collective-permute-start.7 = (bf16[2048,128]{1,0:T(8,128)(2,1)S(1)}, bf16[2048,128]{1,0:T(8,128)(2,1)}, u32[]{:S(2)}, u32[]{:S(2)}) collective-permute-start(bf16[2048,128]{1,0:T(8,128)(2,1)S(1)} %collective-permute-done.6.refs_3_), channel_id=1, source_target_pairs={{0,2},{1,15},{2,4},{3,1},{4,6},{5,3},{6,8},{7,5},{8,10},{9,7},{10,... | collective-permute-start | bytes 1572872 | tf_op jit(solution)/shard_map/ppermute | solution.py:30
  88.7 2.5 %collective-permute-done.13.refs_4_ = bf16[2048,128]{1,0:T(8,128)(2,1)} collective-permute-done((bf16[2048,128]{1,0:T(8,128)(2,1)S(1)}, bf16[2048,128]{1,0:T(8,128)(2,1)}, u32[]{:S(2)}, u32[]{:S(2)}) %collective-permute-start.13) | collective-permute-done | bytes 524320 | tf_op jit(solution)/shard_map/ppermute | solution.py:30
  91.3 0.2 collective-permute-start.25
  91.5 0.9 copy-done.13
  92.4 1.0 copy-done.4
  93.4 1.0 copy-done.6
  94.5 1.0 copy-done.8
  95.5 7.8 %shard_map.158 = (f32[384,2048]{1,0:T(8,128)S(1)}, f32[384,2048]{1,0:T(8,128)S(1)}) custom-call(bf16[384,2048]{1,0:T(8,128)(2,1)} %copy-done.13, bf16[384,2048]{1,0:T(8,128)(2,1)} %bitcast.19, bf16[2048,128]{1,0:T(8,128)(2,1)} %collective-permute-done.1.refs_2_, bf16[2048,128]{1,0:T(8,128)(2,1)S(1)} %collective-permute-done.5.refs_3_, ...), custom_call_target="tpu_custom_call" | custom-call | flops 3623878656 | bytes 4718592 | tf_op jit(solution)/shard_map/pallas_call | solution.py:355
  103.4 5.0 %shard_map.159 = (f32[384,2048]{1,0:T(8,128)S(1)}, f32[384,2048]{1,0:T(8,128)S(1)}) custom-call(bf16[384,2048]{1,0:T(8,128)(2,1)} %copy-done.13, bf16[384,2048]{1,0:T(8,128)(2,1)} %bitcast.20, bf16[2048,128]{1,0:T(8,128)(2,1)S(1)} %collective-permute-done.2.refs_2_, ...), custom_call_target="tpu_custom_call", output_to_operand_aliasing={{0}: (8, {}), {1}: (9, {})} | custom-call | flops 2415919104 | bytes 3145728 | tf_op jit(solution)/shard_map/pallas_call | solution.py:355
  108.3 4.8 %collective-permute-done.7.refs_3_ = bf16[2048,128]{1,0:T(8,128)(2,1)} collective-permute-done((bf16[2048,128]{1,0:T(8,128)(2,1)S(1)}, bf16[2048,128]{1,0:T(8,128)(2,1)}, u32[]{:S(2)}, u32[]{:S(2)}) %collective-permute-start.7) | collective-permute-done | bytes 524320 | tf_op jit(solution)/shard_map/ppermute | solution.py:30
  113.1 2.1 %collective-permute-done.22.refs_6_ = bf16[2048,128]{1,0:T(8,128)(2,1)S(1)} collective-permute-done((bf16[2048,128]{1,0:T(8,128)(2,1)S(1)}, bf16[2048,128]{1,0:T(8,128)(2,1)S(1)}, u32[]{:S(2)}, u32[]{:S(2)}) %collective-permute-start.22) | collective-permute-done | bytes 524320 | tf_op jit(solution)/shard_map/ppermute | solution.py:30
  115.2 5.7 %collective-permute-done.25.refs_7_ = bf16[2048,128]{1,0:T(8,128)(2,1)S(1)} collective-permute-done((bf16[2048,128]{1,0:T(8,128)(2,1)S(1)}, bf16[2048,128]{1,0:T(8,128)(2,1)S(1)}, u32[]{:S(2)}, u32[]{:S(2)}) %collective-permute-start.25) | collective-permute-done | bytes 524320 | tf_op jit(solution)/shard_map/ppermute | solution.py:30
  120.9 5.4 %shard_map.160 = (f32[384,2048]{1,0:T(8,128)}, f32[384,2048]{1,0:T(8,128)S(1)}) custom-call(bf16[384,2048]{1,0:T(8,128)(2,1)} %copy-done.13, bf16[384,2048]{1,0:T(8,128)(2,1)} %bitcast.21, bf16[2048,128]{1,0:T(8,128)(2,1)} %collective-permute-done.3.refs_2_, bf16[2048,128]{1,0:T(8,128)(2,1)} %collective-permute-done.7.refs_3_, ...), custom_call_target="tpu_custom_call", output_to_operand_aliasing={{1}: (9, {})} | custom-call | flops 2415919104 | bytes 3145728 | tf_op jit(solution)/shard_map/pallas_call | solution.py:355
  126.3 2.2 %collective-permute-start.8 = (bf16[2048,128]{1,0:T(8,128)(2,1)}, bf16[2048,128]{1,0:T(8,128)(2,1)}, u32[]{:S(2)}, u32[]{:S(2)}) collective-permute-start(bf16[2048,128]{1,0:T(8,128)(2,1)} %collective-permute-done.7.refs_3_), channel_id=1, source_target_pairs={{0,2},{1,15},{2,4},{3,1},{4,6},{5,3},{6,8},{7,5},{8,10},{9,7},{10,... | collective-permute-start | bytes 1572872 | tf_op jit(solution)/shard_map/ppermute | solution.py:30
  128.5 0.4 collective-permute-start.4
  128.9 0.2 collective-permute-start.14
  129.1 0.7 slice.3
  129.8 3.3 %collective-permute-start = (bf16[64,128]{1,0:T(8,128)(2,1)S(1)}, bf16[64,128]{1,0:T(8,128)(2,1)S(1)}, u32[]{:S(2)}, u32[]{:S(2)}) collective-permute-start(bf16[64,128]{1,0:T(8,128)(2,1)S(1)} %slice.3), channel_id=1, source_target_pairs={{0,16},{16,32},{32,48},{48,64},{64,80},{80,96},{96,112},{112,128},... | collective-permute-start | bytes 49160 | tf_op jit(solution)/shard_map/ppermute | solution.py:25
  133.1 0.8 collective-permute-done.halo_ref
  133.9 7.0 %local_scan.1 = (f32[64,2048]{1,0:T(8,128)S(1)}, f32[64,2048]{1,0:T(8,128)S(1)}, f32[16,8,128]{2,1,0:T(8,128)}) custom-call(s32[1]{0:T(128)} %bitcast.1.group_ref, bf16[64,2048]{1,0:T(8,128)(2,1)} %x_ref.1, bf16[64,128]{1,0:T(8,128)(2,1)S(1)} %collective-permute-done.halo_ref, bf16[4,1024]{1,0:T(4,128)(2,1)} %bitcast.35, bf16[16,64,64]{2,1,0:T(8,128)(2,1)} %rate_ref.1, ...), custom_call_target="tpu_custom_call" | custom-call | flops 4000000000 | bytes 2000000 | tf_op jit(solution)/shard_map/local_scan/pallas_call | solution.py:128
  140.9 0.8 copy-done.9
  141.7 0.8 copy-done.11
  142.5 7.4 %all-to-all-start = ((f32[16,8,128]{2,1,0:T(8,128)}), f32[16,8,128]{2,1,0:T(8,128)S(1)}, u32[]{:S(2)}, u32[]{:S(2)}) async-start(f32[16,8,128]{2,1,0:T(8,128)} %get-tuple-element.15), calls=%async_computation | async-start | bytes 131072 | tf_op jit(solution)/shard_map/all_to_all | solution.py:19
  149.9 1.1 collective-permute-start.10
  151.0 0.1 collective-permute-start.9
  151.1 0.4 collective-permute-start.15
  151.5 4.9 %all-to-all-done.totals_ref = f32[16,8,128]{2,1,0:T(8,128)S(1)} async-done(((f32[16,8,128]{2,1,0:T(8,128)}), f32[16,8,128]{2,1,0:T(8,128)S(1)}, u32[]{:S(2)}, u32[]{:S(2)}) %all-to-all-start) | async-done | bytes 65568 | tf_op jit(solution)/shard_map/all_to_all | solution.py:19
  156.4 1.0 copy-done.10
  157.5 1.0 copy-done.12
  158.5 1.9 gated_states.1
  160.5 7.7 %all-to-all-start.1 = ((bf16[16,64,128]{2,1,0:T(8,128)(2,1)}), bf16[16,64,128]{2,1,0:T(8,128)(2,1)}, u32[]{:S(2)}, u32[]{:S(2)}) async-start(bf16[16,64,128]{2,1,0:T(8,128)(2,1)} %gated_states.1), calls=%async_computation.1 | async-start | bytes 524288 | tf_op jit(solution)/shard_map/all_to_all | solution.py:220
  168.2 1.4 copy-done.1
  169.6 2.5 %last_units.1.units_ref = bf16[384,256]{1,0:T(8,128)(2,1)S(1)} custom-call(bf16[384,2048]{1,0:T(8,128)(2,1)S(1)} %bitcast.22, bf16[2048,128]{1,0:T(8,128)(2,1)} %collective-permute-done.4.refs_0_, bf16[2048,128]{1,0:T(8,128)(2,1)} %collective-permute-done.8.refs_1_, bf16[2048,128]{1,0:T(8,128)(2,1)} %collective-permute-done.9.refs_2_, ...), custom_call_target="tpu_custom_call" | custom-call | flops 805306368 | bytes 2097152 | tf_op jit(solution)/shard_map/last_units/pallas_call | solution.py:381
  172.1 2.4 %joined.1.old_ref = f32[384,2048]{1,0:T(8,128)S(1)} custom-call(f32[384,2048]{1,0:T(8,128)S(1)} %get-tuple-element.22.mine_ref, f32[384,2048]{1,0:T(8,128)} %collective-permute-done.26.given_ref), custom_call_target="tpu_custom_call", output_to_operand_aliasing={{}: (0, {})} | custom-call | flops 786432 | bytes 9437184 | tf_op jit(solution)/shard_map/joined/pallas_call | solution.py:396
  174.6 1.7 last_down.2.old_ref
  176.3 1.6 last_down.3
  177.9 1.2 copy-done.2
  179.1 0.8 all-to-all-done.1
  179.9 3.7 %all-to-all-start.3 = ((bf16[16,24,2048]{2,1,0:T(8,128)(2,1)}), bf16[16,24,2048]{2,1,0:T(8,128)(2,1)S(1)}, u32[]{:S(2)}, u32[]{:S(2)}) async-start(bf16[16,24,2048]{2,1,0:T(8,128)(2,1)} %bitcast.24), calls=%async_computation.3 | async-start | bytes 3145728 | tf_op jit(solution)/shard_map/all_to_all | solution.py:499
  183.6 3.8 %convolution_convert_fusion = bf16[128,2048]{1,0:T(8,128)(2,1)} fusion(bf16[1024,128]{1,0:T(8,128)(2,1)} %bitcast.5, bf16[1024,2048]{1,0:T(8,128)(2,1)} %param.22), kind=kOutput, calls=%fused_computation | convolution fusion | flops 537133056 | bytes 4980736 | tf_op jit(solution)/shard_map/dot_general | solution.py:221
  187.4 21.2 %all-to-all-done.3 = bf16[16,24,2048]{2,1,0:T(8,128)(2,1)S(1)} async-done(((bf16[16,24,2048]{2,1,0:T(8,128)(2,1)}), bf16[16,24,2048]{2,1,0:T(8,128)(2,1)S(1)}, u32[]{:S(2)}, u32[]{:S(2)}) %all-to-all-start.3) | async-done | bytes 1572896 | tf_op jit(solution)/shard_map/all_to_all | solution.py:499
  208.6 1.4 weighted_sum.1
  (40 shorter events, 0.1 us)
Async XLA Ops:
  1.3 10.7 %copy-start.3 = (bf16[1,2048,128]{2,1,0:T(8,128)(2,1)S(1)}, bf16[1,2048,128]{2,1,0:T(8,128)(2,1)}, u32[]{:S(2)}) copy-start(bf16[1,2048,128]{2,1,0:T(8,128)(2,1)} %param.27) | copy-start | bytes 1572868
  1.3 16.4 %copy-start.7 = (bf16[1,2048,128]{2,1,0:T(8,128)(2,1)S(1)}, bf16[1,2048,128]{2,1,0:T(8,128)(2,1)}, u32[]{:S(2)}) copy-start(bf16[1,2048,128]{2,1,0:T(8,128)(2,1)} %param.29) | copy-start | bytes 1572868
  1.3 17.8 %copy-start.5 = (bf16[1,2048,128]{2,1,0:T(8,128)(2,1)S(1)}, bf16[1,2048,128]{2,1,0:T(8,128)(2,1)}, u32[]{:S(2)}) copy-start(bf16[1,2048,128]{2,1,0:T(8,128)(2,1)} %param.28) | copy-start | bytes 1572868
  4.5 30.7 %all-to-all-start.2 = ((bf16[16,24,2048]{2,1,0:T(8,128)(2,1)}), bf16[16,24,2048]{2,1,0:T(8,128)(2,1)S(1)}, u32[]{:S(2)}, u32[]{:S(2)}) async-start(bf16[16,24,2048]{2,1,0:T(8,128)(2,1)} %bitcast.9), calls=%async_computation.2 | async-start | bytes 3145728 | tf_op jit(solution)/shard_map/all_to_all | solution.py:482
  12.0 15.8 %collective-permute-start.1 = (bf16[2048,128]{1,0:T(8,128)(2,1)S(1)}, bf16[2048,128]{1,0:T(8,128)(2,1)}, u32[]{:S(2)}, u32[]{:S(2)}) collective-permute-start(bf16[2048,128]{1,0:T(8,128)(2,1)S(1)} %bitcast.26), channel_id=1, source_target_pairs={{0,2},{1,15},{2,4},{3,1},{4,6},{5,3},{6,8},{7,5},{8,10},{9,7},{10,... | collective-permute-start | bytes 1572872 | tf_op jit(solution)/shard_map/ppermute | solution.py:30
  17.7 21.4 %collective-permute-start.11 = (bf16[2048,128]{1,0:T(8,128)(2,1)S(1)}, bf16[2048,128]{1,0:T(8,128)(2,1)}, u32[]{:S(2)}, u32[]{:S(2)}) collective-permute-start(bf16[2048,128]{1,0:T(8,128)(2,1)S(1)} %bitcast.32), channel_id=1, source_target_pairs={{0,2},{1,15},{2,4},{3,1},{4,6},{5,3},{6,8},{7,5},{8,10},{9,7},{10,... | collective-permute-start | bytes 1572872 | tf_op jit(solution)/shard_map/ppermute | solution.py:30
  18.4 24.7 %collective-permute-start.17 = (bf16[2048,128]{1,0:T(8,128)(2,1)S(1)}, bf16[2048,128]{1,0:T(8,128)(2,1)}, u32[]{:S(2)}, u32[]{:S(2)}) collective-permute-start(bf16[2048,128]{1,0:T(8,128)(2,1)S(1)} %bitcast.27), channel_id=1, source_target_pairs={{0,14},{1,3},{2,0},{3,5},{4,2},{5,7},{6,4},{7,9},{8,6},{9,11},{10,... | collective-permute-start | bytes 1572872 | tf_op jit(solution)/shard_map/ppermute | solution.py:30
  19.2 24.7 %collective-permute-start.20 = (bf16[2048,128]{1,0:T(8,128)(2,1)S(1)}, bf16[2048,128]{1,0:T(8,128)(2,1)}, u32[]{:S(2)}, u32[]{:S(2)}) collective-permute-start(bf16[2048,128]{1,0:T(8,128)(2,1)S(1)} %bitcast.29), channel_id=1, source_target_pairs={{0,14},{1,3},{2,0},{3,5},{4,2},{5,7},{6,4},{7,9},{8,6},{9,11},{10,... | collective-permute-start | bytes 1572872 | tf_op jit(solution)/shard_map/ppermute | solution.py:30
  19.2 31.0 %collective-permute-start.23 = (bf16[2048,128]{1,0:T(8,128)(2,1)S(1)}, bf16[2048,128]{1,0:T(8,128)(2,1)}, u32[]{:S(2)}, u32[]{:S(2)}) collective-permute-start(bf16[2048,128]{1,0:T(8,128)(2,1)S(1)} %bitcast.33), channel_id=1, source_target_pairs={{0,14},{1,3},{2,0},{3,5},{4,2},{5,7},{6,4},{7,9},{8,6},{9,11},{10,... | collective-permute-start | bytes 1572872 | tf_op jit(solution)/shard_map/ppermute | solution.py:30
  35.1 56.1 %copy-start = (bf16[16,24,2048]{2,1,0:T(8,128)(2,1)}, bf16[16,24,2048]{2,1,0:T(8,128)(2,1)S(1)}, u32[]{:S(2)}) copy-start(bf16[16,24,2048]{2,1,0:T(8,128)(2,1)S(1)} %all-to-all-done.2) | copy-start | bytes 4718596
  35.1 56.1 %collective-permute-start.16 = (bf16[384,2048]{1,0:T(8,128)(2,1)S(1)}, bf16[384,2048]{1,0:T(8,128)(2,1)S(1)}, u32[]{:S(2)}, u32[]{:S(2)}) collective-permute-start(bf16[384,2048]{1,0:T(8,128)(2,1)S(1)} %bitcast.18), channel_id=1, source_target_pairs={{0,1},{1,0},{2,3},{3,2},{4,5},{5,4},{6,7},{7,6},{8,9},{9,8},{10,11... | collective-permute-start | bytes 4718600 | tf_op jit(solution)/shard_map/ppermute | solution.py:35
  39.0 15.8 %collective-permute-start.5 = (bf16[2048,128]{1,0:T(8,128)(2,1)S(1)}, bf16[2048,128]{1,0:T(8,128)(2,1)S(1)}, u32[]{:S(2)}, u32[]{:S(2)}) collective-permute-start(bf16[2048,128]{1,0:T(8,128)(2,1)S(1)} %bitcast.30), channel_id=1, source_target_pairs={{0,2},{1,15},{2,4},{3,1},{4,6},{5,3},{6,8},{7,5},{8,10},{9,7},{10,... | collective-permute-start | bytes 1572872 | tf_op jit(solution)/shard_map/ppermute | solution.py:30
  43.1 22.6 %collective-permute-start.12 = (bf16[2048,128]{1,0:T(8,128)(2,1)}, bf16[2048,128]{1,0:T(8,128)(2,1)S(1)}, u32[]{:S(2)}, u32[]{:S(2)}) collective-permute-start(bf16[2048,128]{1,0:T(8,128)(2,1)} %collective-permute-done.11.refs_4_), channel_id=1, source_target_pairs={{0,2},{1,15},{2,4},{3,1},{4,6},{5,3},{6,8},{7,5},{8,10},{9,7},{10,... | collective-permute-start | bytes 1572872 | tf_op jit(solution)/shard_map/ppermute | solution.py:30
  43.8 25.1 %collective-permute-start.18 = (bf16[2048,128]{1,0:T(8,128)(2,1)}, bf16[2048,128]{1,0:T(8,128)(2,1)S(1)}, u32[]{:S(2)}, u32[]{:S(2)}) collective-permute-start(bf16[2048,128]{1,0:T(8,128)(2,1)} %collective-permute-done.17.refs_5_), channel_id=1, source_target_pairs={{0,14},{1,3},{2,0},{3,5},{4,2},{5,7},{6,4},{7,9},{8,6},{9,11},{10,... | collective-permute-start | bytes 1572872 | tf_op jit(solution)/shard_map/ppermute | solution.py:30
  50.2 25.5 %collective-permute-start.2 = (bf16[2048,128]{1,0:T(8,128)(2,1)}, bf16[2048,128]{1,0:T(8,128)(2,1)S(1)}, u32[]{:S(2)}, u32[]{:S(2)}) collective-permute-start(bf16[2048,128]{1,0:T(8,128)(2,1)} %collective-permute-done.1.refs_2_), channel_id=1, source_target_pairs={{0,2},{1,15},{2,4},{3,1},{4,6},{5,3},{6,8},{7,5},{8,10},{9,7},{10,... | collective-permute-start | bytes 1572872 | tf_op jit(solution)/shard_map/ppermute | solution.py:30
  54.8 24.1 %collective-permute-start.21 = (bf16[2048,128]{1,0:T(8,128)(2,1)}, bf16[2048,128]{1,0:T(8,128)(2,1)S(1)}, u32[]{:S(2)}, u32[]{:S(2)}) collective-permute-start(bf16[2048,128]{1,0:T(8,128)(2,1)} %collective-permute-done.20.refs_6_), channel_id=1, source_target_pairs={{0,14},{1,3},{2,0},{3,5},{4,2},{5,7},{6,4},{7,9},{8,6},{9,11},{10,... | collective-permute-start | bytes 1572872 | tf_op jit(solution)/shard_map/ppermute | solution.py:30
  65.6 20.0 %collective-permute-start.6 = (bf16[2048,128]{1,0:T(8,128)(2,1)S(1)}, bf16[2048,128]{1,0:T(8,128)(2,1)S(1)}, u32[]{:S(2)}, u32[]{:S(2)}) collective-permute-start(bf16[2048,128]{1,0:T(8,128)(2,1)S(1)} %collective-permute-done.5.refs_3_), channel_id=1, source_target_pairs={{0,2},{1,15},{2,4},{3,1},{4,6},{5,3},{6,8},{7,5},{8,10},{9,7},{10,... | collective-permute-start | bytes 1572872 | tf_op jit(solution)/shard_map/ppermute | solution.py:30
  68.9 19.8 %collective-permute-start.24 = (bf16[2048,128]{1,0:T(8,128)(2,1)}, bf16[2048,128]{1,0:T(8,128)(2,1)S(1)}, u32[]{:S(2)}, u32[]{:S(2)}) collective-permute-start(bf16[2048,128]{1,0:T(8,128)(2,1)} %collective-permute-done.23.refs_7_), channel_id=1, source_target_pairs={{0,14},{1,3},{2,0},{3,5},{4,2},{5,7},{6,4},{7,9},{8,6},{9,11},{10,... | collective-permute-start | bytes 1572872 | tf_op jit(solution)/shard_map/ppermute | solution.py:30
  75.7 15.6 %collective-permute-start.13 = (bf16[2048,128]{1,0:T(8,128)(2,1)S(1)}, bf16[2048,128]{1,0:T(8,128)(2,1)}, u32[]{:S(2)}, u32[]{:S(2)}) collective-permute-start(bf16[2048,128]{1,0:T(8,128)(2,1)S(1)} %collective-permute-done.12.refs_4_), channel_id=1, source_target_pairs={{0,2},{1,15},{2,4},{3,1},{4,6},{5,3},{6,8},{7,5},{8,10},{9,7},{10,... | collective-permute-start | bytes 1572872 | tf_op jit(solution)/shard_map/ppermute | solution.py:30
  79.0 29.4 %collective-permute-start.3 = (bf16[2048,128]{1,0:T(8,128)(2,1)S(1)}, bf16[2048,128]{1,0:T(8,128)(2,1)}, u32[]{:S(2)}, u32[]{:S(2)}) collective-permute-start(bf16[2048,128]{1,0:T(8,128)(2,1)S(1)} %collective-permute-done.2.refs_2_), channel_id=1, source_target_pairs={{0,2},{1,15},{2,4},{3,1},{4,6},{5,3},{6,8},{7,5},{8,10},{9,7},{10,... | collective-permute-start | bytes 1572872 | tf_op jit(solution)/shard_map/ppermute | solution.py:30
  85.6 27.5 %collective-permute-start.7 = (bf16[2048,128]{1,0:T(8,128)(2,1)S(1)}, bf16[2048,128]{1,0:T(8,128)(2,1)}, u32[]{:S(2)}, u32[]{:S(2)}) collective-permute-start(bf16[2048,128]{1,0:T(8,128)(2,1)S(1)} %collective-permute-done.6.refs_3_), channel_id=1, source_target_pairs={{0,2},{1,15},{2,4},{3,1},{4,6},{5,3},{6,8},{7,5},{8,10},{9,7},{10,... | collective-permute-start | bytes 1572872 | tf_op jit(solution)/shard_map/ppermute | solution.py:30
  88.7 24.4 %collective-permute-start.19 = (bf16[2048,128]{1,0:T(8,128)(2,1)S(1)}, bf16[2048,128]{1,0:T(8,128)(2,1)S(1)}, u32[]{:S(2)}, u32[]{:S(2)}) collective-permute-start(bf16[2048,128]{1,0:T(8,128)(2,1)S(1)} %collective-permute-done.18.refs_5_), channel_id=1, source_target_pairs={{0,14},{1,3},{2,0},{3,5},{4,2},{5,7},{6,4},{7,9},{8,6},{9,11},{10,... | collective-permute-start | bytes 1572872 | tf_op jit(solution)/shard_map/ppermute | solution.py:30
  91.2 24.0 %collective-permute-start.22 = (bf16[2048,128]{1,0:T(8,128)(2,1)S(1)}, bf16[2048,128]{1,0:T(8,128)(2,1)S(1)}, u32[]{:S(2)}, u32[]{:S(2)}) collective-permute-start(bf16[2048,128]{1,0:T(8,128)(2,1)S(1)} %collective-permute-done.21.refs_6_), channel_id=1, source_target_pairs={{0,14},{1,3},{2,0},{3,5},{4,2},{5,7},{6,4},{7,9},{8,6},{9,11},{10,... | collective-permute-start | bytes 1572872 | tf_op jit(solution)/shard_map/ppermute | solution.py:30
  91.2 1.2 copy-start.13
  91.3 29.7 %collective-permute-start.25 = (bf16[2048,128]{1,0:T(8,128)(2,1)S(1)}, bf16[2048,128]{1,0:T(8,128)(2,1)S(1)}, u32[]{:S(2)}, u32[]{:S(2)}) collective-permute-start(bf16[2048,128]{1,0:T(8,128)(2,1)S(1)} %collective-permute-done.24.refs_7_), channel_id=1, source_target_pairs={{0,14},{1,3},{2,0},{3,5},{4,2},{5,7},{6,4},{7,9},{8,6},{9,11},{10,... | collective-permute-start | bytes 1572872 | tf_op jit(solution)/shard_map/ppermute | solution.py:30
  92.4 1.0 copy-start.4
  93.4 1.0 copy-start.6
  94.5 1.0 copy-start.8
  126.3 45.8 %collective-permute-start.26 = (f32[384,2048]{1,0:T(8,128)}, f32[384,2048]{1,0:T(8,128)}, u32[]{:S(2)}, u32[]{:S(2)}) collective-permute-start(f32[384,2048]{1,0:T(8,128)} %get-tuple-element.23), channel_id=1, source_target_pairs={{0,1},{1,0},{2,3},{3,2},{4,5},{5,4},{6,7},{7,6},{8,9},{9,8},{10,11... | collective-permute-start | bytes 9437192 | tf_op jit(solution)/shard_map/ppermute | solution.py:35
  126.3 23.6 %collective-permute-start.8 = (bf16[2048,128]{1,0:T(8,128)(2,1)}, bf16[2048,128]{1,0:T(8,128)(2,1)}, u32[]{:S(2)}, u32[]{:S(2)}) collective-permute-start(bf16[2048,128]{1,0:T(8,128)(2,1)} %collective-permute-done.7.refs_3_), channel_id=1, source_target_pairs={{0,2},{1,15},{2,4},{3,1},{4,6},{5,3},{6,8},{7,5},{8,10},{9,7},{10,... | collective-permute-start | bytes 1572872 | tf_op jit(solution)/shard_map/ppermute | solution.py:30
  128.5 22.5 %collective-permute-start.4 = (bf16[2048,128]{1,0:T(8,128)(2,1)}, bf16[2048,128]{1,0:T(8,128)(2,1)}, u32[]{:S(2)}, u32[]{:S(2)}) collective-permute-start(bf16[2048,128]{1,0:T(8,128)(2,1)} %collective-permute-done.3.refs_2_), channel_id=1, source_target_pairs={{0,2},{1,15},{2,4},{3,1},{4,6},{5,3},{6,8},{7,5},{8,10},{9,7},{10,... | collective-permute-start | bytes 1572872 | tf_op jit(solution)/shard_map/ppermute | solution.py:30
  128.9 22.2 %collective-permute-start.14 = (bf16[2048,128]{1,0:T(8,128)(2,1)}, bf16[2048,128]{1,0:T(8,128)(2,1)}, u32[]{:S(2)}, u32[]{:S(2)}) collective-permute-start(bf16[2048,128]{1,0:T(8,128)(2,1)} %collective-permute-done.13.refs_4_), channel_id=1, source_target_pairs={{0,2},{1,15},{2,4},{3,1},{4,6},{5,3},{6,8},{7,5},{8,10},{9,7},{10,... | collective-permute-start | bytes 1572872 | tf_op jit(solution)/shard_map/ppermute | solution.py:30
  129.8 4.1 %collective-permute-start = (bf16[64,128]{1,0:T(8,128)(2,1)S(1)}, bf16[64,128]{1,0:T(8,128)(2,1)S(1)}, u32[]{:S(2)}, u32[]{:S(2)}) collective-permute-start(bf16[64,128]{1,0:T(8,128)(2,1)S(1)} %slice.3), channel_id=1, source_target_pairs={{0,16},{16,32},{32,48},{48,64},{64,80},{80,96},{96,112},{112,128},... | collective-permute-start | bytes 49160 | tf_op jit(solution)/shard_map/ppermute | solution.py:25
  140.9 0.8 copy-start.9
  141.7 0.8 copy-start.11
  142.5 13.9 %all-to-all-start = ((f32[16,8,128]{2,1,0:T(8,128)}), f32[16,8,128]{2,1,0:T(8,128)S(1)}, u32[]{:S(2)}, u32[]{:S(2)}) async-start(f32[16,8,128]{2,1,0:T(8,128)} %get-tuple-element.15), calls=%async_computation | async-start | bytes 131072 | tf_op jit(solution)/shard_map/all_to_all | solution.py:19
  149.9 18.3 %collective-permute-start.10 = (bf16[2048,128]{1,0:T(8,128)(2,1)}, bf16[2048,128]{1,0:T(8,128)(2,1)}, u32[]{:S(2)}, u32[]{:S(2)}) collective-permute-start(bf16[2048,128]{1,0:T(8,128)(2,1)} %collective-permute-done.8.refs_1_), channel_id=1, source_target_pairs={{0,1},{1,0},{2,3},{3,2},{4,5},{5,4},{6,7},{7,6},{8,9},{9,8},{10,11... | collective-permute-start | bytes 1572872 | tf_op jit(solution)/shard_map/ppermute | solution.py:35
  151.0 17.2 %collective-permute-start.9 = (bf16[2048,128]{1,0:T(8,128)(2,1)}, bf16[2048,128]{1,0:T(8,128)(2,1)}, u32[]{:S(2)}, u32[]{:S(2)}) collective-permute-start(bf16[2048,128]{1,0:T(8,128)(2,1)} %collective-permute-done.4.refs_0_), channel_id=1, source_target_pairs={{0,1},{1,0},{2,3},{3,2},{4,5},{5,4},{6,7},{7,6},{8,9},{9,8},{10,11... | collective-permute-start | bytes 1572872 | tf_op jit(solution)/shard_map/ppermute | solution.py:35
  151.1 25.2 %collective-permute-start.15 = (bf16[2048,128]{1,0:T(8,128)(2,1)}, bf16[2048,128]{1,0:T(8,128)(2,1)}, u32[]{:S(2)}, u32[]{:S(2)}) collective-permute-start(bf16[2048,128]{1,0:T(8,128)(2,1)} %collective-permute-done.14.down_ref), channel_id=1, source_target_pairs={{0,1},{1,0},{2,3},{3,2},{4,5},{5,4},{6,7},{7,6},{8,9},{9,8},{10,11... | collective-permute-start | bytes 1572872 | tf_op jit(solution)/shard_map/ppermute | solution.py:35
  156.4 1.0 copy-start.10
  157.5 1.0 copy-start.12
  160.5 19.4 %all-to-all-start.1 = ((bf16[16,64,128]{2,1,0:T(8,128)(2,1)}), bf16[16,64,128]{2,1,0:T(8,128)(2,1)}, u32[]{:S(2)}, u32[]{:S(2)}) async-start(bf16[16,64,128]{2,1,0:T(8,128)(2,1)} %gated_states.1), calls=%async_computation.1 | async-start | bytes 524288 | tf_op jit(solution)/shard_map/all_to_all | solution.py:220
  168.2 1.4 copy-start.1
  177.9 1.2 copy-start.2
  179.9 28.7 %all-to-all-start.3 = ((bf16[16,24,2048]{2,1,0:T(8,128)(2,1)}), bf16[16,24,2048]{2,1,0:T(8,128)(2,1)S(1)}, u32[]{:S(2)}, u32[]{:S(2)}) async-start(bf16[16,24,2048]{2,1,0:T(8,128)(2,1)} %bitcast.24), calls=%async_computation.3 | async-start | bytes 3145728 | tf_op jit(solution)/shard_map/all_to_all | solution.py:499
